TPU v7x, 128 devices: a whole 4x4x4 slice. The times are simulated.
128 devices in a mesh: fs: 32 (over z, y, core), tp: 4 (over x).
Axes of the slice: x: 4, y: 4, z: 4, core: 2. Of those that a mesh axis runs over, the one named last changes fastest.
Arguments:
- normed_input: bfloat16 [147456, 2048], P('fs'), may hold values from -12 to 12
- query_latent_cotangent: bfloat16 [147456, 768], P('fs', 'tp'), may hold values from -0.015625 to 0.015625
- key_value_latent_cotangent: bfloat16 [147456, 512], P('fs', 'tp'), may hold values from -0.015625 to 0.015625
- row_factor: bfloat16 [2048, 256], P('fs'), may hold values from -0.25 to 0.25
- query_down_weight: float32 [2048, 768], P('fs', 'tp'), may hold values from -6 to 6
- key_value_down_weight: float32 [2048, 512], P('fs', 'tp'), may hold values from -6 to 6
- query_first_moment: float32 [256, 768], P('fs', 'tp'), may hold values from -6 to 6
- key_value_first_moment: float32 [256, 512], P('fs', 'tp'), may hold values from -6 to 6
- query_second: float32 [256, 768], P('fs', 'tp'), may hold values from 0.5 to 2000
- latent_second: float32 [256, 512], P('fs', 'tp'), may hold values from 0.5 to 2000
Outputs:
- query_new: float32 [2048, 768], P('fs', 'tp')
- latent_new: float32 [2048, 512], P('fs', 'tp')
- query_step: float32 [2048, 768], P('fs', 'tp')
- latent_step: float32 [2048, 512], P('fs', 'tp')
- query_copy: bfloat16 [2048, 768], P(None, 'tp')
- latent_copy: bfloat16 [2048, 512], P(None, 'tp')
- query_first_new: float32 [256, 768], P('fs', 'tp')
- latent_first_new: float32 [256, 512], P('fs', 'tp')
- query_second_new: float32 [256, 768], P('fs', 'tp')
- latent_second_new: float32 [256, 512], P('fs', 'tp')
All inputs are finite; a program needn't handle non-finite values.
Results may differ from a plain program's by a relative error of at most 0.006.
Values may be sent and summed in bfloat16 or wider, within the bound.
No kernel may reach another device: no remote copies, remote signals or barrier semaphores. Data moves between devices by JAX's collectives and lax.ppermute only.
A program may use at most 64 MiB of HBM per device.

v0:
```python
import functools

import jax
import jax.numpy as jnp
from jax import lax
from jax.sharding import Mesh
from jax.sharding import PartitionSpec as P

FS = ("fs_0", "fs_1", "fs_2")
FS_TP = ("fs_0", "fs_1", "fs_2", "tp")


def from_everyone(array, axis):
    copies = jnp.broadcast_to(array, (lax.axis_size(axis), *array.shape))
    return lax.all_to_all(copies, axis, split_axis=0, concat_axis=0, tiled=True)


def in_order(tiles, dim):
    tiles = jnp.moveaxis(tiles, 0, dim)
    shape = tiles.shape
    return tiles.reshape(*shape[:dim], shape[dim] * shape[dim + 1], *shape[dim + 2 :])


def gather_directly(array, axis, dim):
    tiles = from_everyone(array, axis)
    return in_order(tiles, dim)


def split_up(array, dim, peers):
    shape = array.shape
    tiles = array.reshape(*shape[:dim], peers, shape[dim] // peers, *shape[dim + 1 :])
    return jnp.moveaxis(tiles, dim, 0)


def sent_and_summed(array, axis, dim):
    tiles = split_up(array, dim, lax.axis_size(axis))
    arrived = lax.all_to_all(tiles, axis, split_axis=0, concat_axis=0, tiled=True)
    return arrived.astype(jnp.float32).sum(axis=0)


def over_axes(array, axes):
    return functools.reduce(lax.psum, axes, array)


def in_one_piece(arrays, axis, dim, along):
    ends, at = ([], 0)
    for a in arrays[:-1]:
        at += a.shape[along]
        ends.append(at)
    both = jnp.concatenate(arrays, axis=along)
    return tuple(jnp.split(lax.all_gather(both, axis, axis=dim, tiled=True), ends, axis=along))


def token_sum(left, right):
    return lax.dot_general(
        left, right, (((0,), (0,)), ((), ())), preferred_element_type=jnp.float32
    )


def moment_update(projected, first, second):
    first_new = 0.8 * first + 0.2 * projected
    second_new = 0.9 * second + 0.1 * projected * projected
    direction = first_new / (jnp.sqrt(second_new) + 1e-08)
    return (first_new, second_new, direction)


def body(
    normed_input,
    query_latent_cotangent,
    key_value_latent_cotangent,
    row_factor,
    query_down_weight,
    key_value_down_weight,
    query_first_moment,
    key_value_first_moment,
    query_second,
    latent_second,
):
    fs_count = lax.axis_size(FS)
    tp_count = lax.axis_size("tp")
    query_width = query_latent_cotangent.shape[1]
    rank_rows = query_first_moment.shape[0]
    factor_whole = gather_directly(row_factor, FS, 0)
    latent_tokens = jnp.dot(normed_input, factor_whole, preferred_element_type=jnp.float32)
    upper_part = latent_tokens.astype(jnp.bfloat16)
    lower_part = (latent_tokens - upper_part.astype(jnp.float32)).astype(jnp.bfloat16)
    both_cotangents = jnp.concatenate([query_latent_cotangent, key_value_latent_cotangent], axis=1)
    projected = sent_and_summed(
        (token_sum(upper_part, both_cotangents) + token_sum(lower_part, both_cotangents)).astype(
            jnp.bfloat16
        ),
        FS,
        0,
    )
    query_first_new, query_second_new, query_dir = moment_update(
        projected[:, :query_width], query_first_moment, query_second
    )
    latent_first_new, latent_second_new, latent_dir = moment_update(
        projected[:, query_width:], key_value_first_moment, latent_second
    )
    query_sq, latent_sq = (
        over_axes(jnp.sum(query_dir * query_dir), FS_TP),
        over_axes(jnp.sum(latent_dir * latent_dir), FS_TP),
    )
    query_count = rank_rows * fs_count * query_width * tp_count
    latent_count = rank_rows * fs_count * key_value_latent_cotangent.shape[1] * tp_count
    query_scale = 0.5 * jnp.sqrt(jnp.float32(query_count)) / jnp.sqrt(query_sq + 1e-06)
    latent_scale = 0.5 * jnp.sqrt(jnp.float32(latent_count)) / jnp.sqrt(latent_sq + 1e-06)
    scaled = jnp.concatenate([query_scale * query_dir, latent_scale * latent_dir], axis=1)
    factor_rows = row_factor.astype(jnp.float32)
    steps = jnp.dot(factor_rows, gather_directly(scaled, FS, 0), preferred_element_type=jnp.float32)
    query_step = steps[:, :query_width]
    latent_step = steps[:, query_width:]
    query_new = query_down_weight - query_step
    latent_new = key_value_down_weight - latent_step
    query_copy, latent_copy = in_one_piece(
        (query_new.astype(jnp.bfloat16), latent_new.astype(jnp.bfloat16)), FS, 0, 1
    )
    return (
        query_new,
        latent_new,
        query_step,
        latent_step,
        query_copy,
        latent_copy,
        query_first_new,
        latent_first_new,
        query_second_new,
        latent_second_new,
    )


def solution(mesh):
    split = Mesh(mesh.devices.reshape(4, 4, 2, mesh.shape["tp"]), ("fs_0", "fs_1", "fs_2", "tp"))
    placed = (
        P(FS, None),
        P(FS, "tp"),
        P(FS, "tp"),
        P(FS, None),
        P(FS, "tp"),
        P(FS, "tp"),
        P(FS, "tp"),
        P(FS, "tp"),
        P(FS, "tp"),
        P(FS, "tp"),
    )
    return jax.shard_map(
        body,
        mesh=split,
        in_specs=placed,
        out_specs=(
            P(FS, "tp"),
            P(FS, "tp"),
            P(FS, "tp"),
            P(FS, "tp"),
            P(None, "tp"),
            P(None, "tp"),
            P(FS, "tp"),
            P(FS, "tp"),
            P(FS, "tp"),
            P(FS, "tp"),
        ),
        check_vma=False,
    )
```

profile of v0, /device:TPU:1, one launch (start us, length us, event | category | flops | bytes accessed | tf_op | source)
XLA Modules:
  0.0 159.6 jit_solution(15034981366741805355)
XLA Ops:
  7.2 0.0 copy-start
  7.2 1.9 %broadcast_in_dim.6 = bf16[32,64,256]{2,1,0:T(8,128)(2,1)} broadcast(bf16[64,256]{1,0:T(8,128)(2,1)} %param.13), dimensions={1,2} | broadcast | bytes 1081344 | tf_op jit(solution)/shard_map/broadcast_in_dim | solution.py:14
  9.1 9.6 %all-to-all-start = ((bf16[32,64,256]{2,1,0:T(8,128)(2,1)}), bf16[32,64,256]{2,1,0:T(8,128)(2,1)S(1)}, u32[]{:S(2)}, u32[]{:S(2)}) async-start(bf16[32,64,256]{2,1,0:T(8,128)(2,1)} %broadcast_in_dim.6), calls=%async_computation | async-start | bytes 2097152 | tf_op jit(solution)/shard_map/all_to_all | solution.py:15
  18.7 0.0 all-gather.2.cloned.1.call-start
  18.8 0.0 copy-done
  18.8 0.6 copy.22
  19.4 16.4 %all-to-all-done = bf16[32,64,256]{2,1,0:T(8,128)(2,1)S(1)} async-done(((bf16[32,64,256]{2,1,0:T(8,128)(2,1)}), bf16[32,64,256]{2,1,0:T(8,128)(2,1)S(1)}, u32[]{:S(2)}, u32[]{:S(2)}) %all-to-all-start) | async-done | bytes 1048608 | tf_op jit(solution)/shard_map/all_to_all | solution.py:15
  35.8 9.4 %fusion.19 = f32[4608,256]{1,0:T(8,128)S(1)} fusion(bf16[4608,2048]{1,0:T(8,128)(2,1)} %param.10, bf16[2048,256]{1,0:T(8,128)(2,1)S(1)} %bitcast.10), kind=kOutput, calls=%fused_computation.29 | convolution fusion | flops 4831838208 | bytes 24641536 | tf_op jit(solution)/shard_map/dot_general | solution.py:84
  45.2 0.0 copy-done.12
  45.2 1.0 fusion
  46.2 0.0 copy-start.8
  46.2 0.0 copy-start.9
  46.2 0.0 copy-start.10
  46.2 0.0 copy-start.11
  46.2 0.0 copy-start.1
  46.2 0.0 copy-start.2
  46.3 0.0 copy-start.3
  46.3 1.0 fusion.7
  47.2 0.2 copy.23
  47.4 11.8 %all_to_all.15 = bf16[32,8,320]{2,1,0:T(8,128)(2,1)S(1)} all-to-all(bf16[32,8,320]{2,1,0:T(8,128)(2,1)S(1)} %bitcast.11), channel_id=1, replica_groups=mesh['fs_0'=4,'fs_1'=4,'fs_2'=2,'tp'=4] {'fs_0','fs_1','fs_2'}, dimensions={0} | all-to-all | bytes 327680 | tf_op jit(solution)/shard_map/all_to_all | solution.py:37
  59.3 0.0 copy-done.8
  59.3 0.0 copy-done.9
  59.3 0.6 multiply_reduce_fusion
  59.9 0.0 copy-done.10
  59.9 0.0 copy-done.11
  59.9 0.7 multiply_reduce_fusion.1
  60.6 7.5 %all-reduce.2 = (f32[]{:T(128)}, f32[]{:T(128)}) all-reduce(f32[]{:T(128)} %get-tuple-element.47, f32[]{:T(128)} %get-tuple-element.44), channel_id=1, replica_groups=mesh['fs_0'=4,'fs_1'=4,'fs_2'=2,'tp'=4] {'fs_0'}, use_global_device_ids=true, to_apply=%region_7.0 | all-reduce | flops 2 | bytes 16 | tf_op jit(solution)/shard_map/psum | solution.py:42
  68.1 7.7 %all-reduce.1 = (f32[]{:T(128)}, f32[]{:T(128)}) all-reduce(f32[]{:T(128)} %get-tuple-element.34, f32[]{:T(128)} %get-tuple-element.35), channel_id=1, replica_groups=mesh['fs_0'=4,'fs_1'=4,'fs_2'=2,'tp'=4] {'fs_1'}, use_global_device_ids=true, to_apply=%region_8.0 | all-reduce | flops 2 | bytes 16 | tf_op jit(solution)/shard_map/psum | solution.py:42
  75.8 7.0 %all-reduce.3 = (f32[]{:T(128)}, f32[]{:T(128)}) all-reduce(f32[]{:T(128)} %get-tuple-element.32, f32[]{:T(128)} %get-tuple-element.33), channel_id=1, replica_groups=mesh['fs_0'=4,'fs_1'=4,'fs_2'=2,'tp'=4] {'fs_2'}, use_global_device_ids=true, to_apply=%region_9.0 | all-reduce | flops 2 | bytes 16 | tf_op jit(solution)/shard_map/psum | solution.py:42
  82.8 9.1 %all-reduce = (f32[]{:T(128)}, f32[]{:T(128)}) all-reduce(f32[]{:T(128)} %get-tuple-element.36, f32[]{:T(128)} %get-tuple-element.37), channel_id=1, replica_groups=mesh['fs_0'=4,'fs_1'=4,'fs_2'=2,'tp'=4] {'tp'}, use_global_device_ids=true, to_apply=%region_10.0 | all-reduce | flops 2 | bytes 16 | tf_op jit(solution)/shard_map/psum | solution.py:42
  93.3 0.1 pad_maximum_fusion.8
  93.4 13.3 %all_to_all.16 = bf16[32,8,320]{2,1,0:T(8,128)(2,1)S(1)} all-to-all(bf16[32,8,320]{2,1,0:T(8,128)(2,1)S(1)} %broadcast_in_dim.7), channel_id=1, replica_groups=mesh['fs_0'=4,'fs_1'=4,'fs_2'=2,'tp'=4] {'fs_0','fs_1','fs_2'}, dimensions={0} | all-to-all | bytes 327680 | tf_op jit(solution)/shard_map/all_to_all | solution.py:15
  106.8 0.0 copy-done.1
  106.8 0.2 convolution_bitcast_fusion
  106.9 0.0 copy-done.2
  106.9 0.7 fusion.15
  107.6 0.0 copy-done.3
  107.6 0.7 fusion.16
  108.3 0.7 pad_maximum_fusion.7
  109.0 0.0 all-gather.2.cloned.1.call-update
  109.0 38.9 %all-gather.2.cloned.1.call-done = bf16[2048,320]{1,0:T(8,128)(2,1)} async-done(((bf16[64,320]{1,0:T(8,128)(2,1)}), bf16[2048,320]{1,0:T(8,128)(2,1)}) %all-gather.2.cloned.1.call-update) | async-done | bytes 1310736 | tf_op jit(solution)/shard_map/all_gather | solution.py:51
  148.0 1.3 split.8
  149.2 1.2 copy.24
  150.5 2.2 %split.9 = bf16[2048,128]{1,0:T(8,128)(2,1)} slice(bf16[2048,320]{1,0:T(8,128)(2,1)} %all-gather.2.cloned.1.call-done), slice={[0:2048], [192:320]} | slice | bytes 1048576 | tf_op jit(solution)/shard_map/split | solution.py:51
  152.7 0.0 copy-done.4
  152.7 0.0 copy-done.5
  152.7 0.0 copy-done.6
  152.7 0.0 copy-done.7
  (9 shorter events, 0.1 us)
Async XLA Ops:
  7.2 11.6 %copy-start = (bf16[4608,128]{1,0:T(8,128)(2,1)S(1)}, bf16[4608,128]{1,0:T(8,128)(2,1)}, u32[]{:S(2)}) copy-start(bf16[4608,128]{1,0:T(8,128)(2,1)} %param.12) | copy-start | bytes 3538948
  9.1 26.6 %all-to-all-start = ((bf16[32,64,256]{2,1,0:T(8,128)(2,1)}), bf16[32,64,256]{2,1,0:T(8,128)(2,1)S(1)}, u32[]{:S(2)}, u32[]{:S(2)}) async-start(bf16[32,64,256]{2,1,0:T(8,128)(2,1)} %broadcast_in_dim.6), calls=%async_computation | async-start | bytes 2097152 | tf_op jit(solution)/shard_map/all_to_all | solution.py:15
  18.7 129.2 %all-gather.2.cloned.1.call-start = ((), (), s32[]{:S(2)}) async-start(), calls=%async_computation.3 | async-start | bytes 1622016 | tf_op jit(solution)/shard_map/all_gather | solution.py:51
  35.8 9.4 %copy-start.12 = (bf16[4608,192]{0,1:T(8,128)(2,1)S(1)}, bf16[4608,192]{0,1:T(8,128)(2,1)}, u32[]{:S(2)}) copy-start(bf16[4608,192]{0,1:T(8,128)(2,1)} %param.11) | copy-start | bytes 5308420
  46.2 13.1 %copy-start.8 = (f32[8,192]{1,0:T(8,128)S(1)}, f32[8,192]{1,0:T(8,128)}, u32[]{:S(2)}) copy-start(f32[8,192]{1,0:T(8,128)} %param.18) | copy-start | bytes 18436
  46.2 13.1 %copy-start.9 = (f32[8,192]{1,0:T(8,128)S(1)}, f32[8,192]{1,0:T(8,128)}, u32[]{:S(2)}) copy-start(f32[8,192]{1,0:T(8,128)} %param.16) | copy-start | bytes 18436
  46.2 13.7 %copy-start.10 = (f32[8,128]{1,0:T(8,128)S(1)}, f32[8,128]{1,0:T(8,128)}, u32[]{:S(2)}) copy-start(f32[8,128]{1,0:T(8,128)} %param.19) | copy-start | bytes 12292
  46.2 13.7 %copy-start.11 = (f32[8,128]{1,0:T(8,128)S(1)}, f32[8,128]{1,0:T(8,128)}, u32[]{:S(2)}) copy-start(f32[8,128]{1,0:T(8,128)} %param.17) | copy-start | bytes 12292
  46.2 60.5 %copy-start.1 = (bf16[64,256]{1,0:T(8,128)(2,1)S(1)}, bf16[64,256]{1,0:T(8,128)(2,1)}, u32[]{:S(2)}) copy-start(bf16[64,256]{1,0:T(8,128)(2,1)} %param.13) | copy-start | bytes 98308
  46.2 60.7 %copy-start.2 = (f32[64,192]{1,0:T(8,128)S(1)}, f32[64,192]{1,0:T(8,128)}, u32[]{:S(2)}) copy-start(f32[64,192]{1,0:T(8,128)} %param.14) | copy-start | bytes 147460
  46.3 61.3 %copy-start.3 = (f32[64,128]{1,0:T(8,128)S(1)}, f32[64,128]{1,0:T(8,128)}, u32[]{:S(2)}) copy-start(f32[64,128]{1,0:T(8,128)} %param.15) | copy-start | bytes 98308
  59.9 92.8 %copy-start.4 = (f32[8,192]{1,0:T(8,128)}, f32[8,192]{1,0:T(8,128)S(1)}, u32[]{:S(2)}) copy-start(f32[8,192]{1,0:T(8,128)S(1)} %get-tuple-element.45) | copy-start | bytes 18436
  59.9 92.8 %copy-start.5 = (f32[8,192]{1,0:T(8,128)}, f32[8,192]{1,0:T(8,128)S(1)}, u32[]{:S(2)}) copy-start(f32[8,192]{1,0:T(8,128)S(1)} %get-tuple-element.46) | copy-start | bytes 18436
  60.6 92.1 %copy-start.6 = (f32[8,128]{1,0:T(8,128)}, f32[8,128]{1,0:T(8,128)S(1)}, u32[]{:S(2)}) copy-start(f32[8,128]{1,0:T(8,128)S(1)} %get-tuple-element.48) | copy-start | bytes 12292
  60.6 92.1 %copy-start.7 = (f32[8,128]{1,0:T(8,128)}, f32[8,128]{1,0:T(8,128)S(1)}, u32[]{:S(2)}) copy-start(f32[8,128]{1,0:T(8,128)S(1)} %get-tuple-element.49) | copy-start | bytes 12292
Sparse Core Ops, SparseCore 0:
  109.1 38.7 all-gather.1
where the time goes:
time: 160 us
  blocking collectives  56.4 us (35%)
  waiting for transfers between devices  55.3 us (35%)
  between operations  15.6 us (10%)
  matrix products  11.5 us (7%)
  starting transfers between devices  9.63 us (6%)
  local copies, waits for them, and re-layouts  7.56 us (5%)
  other arithmetic  3.52 us (2%)
    all_gather x1, waiting for transfers between devices, in_one_piece(): lax.all_gather(both, axis, axis=dim, tiled=True)  38.9 us
    psum x4, blocking collectives, over_axes(): return functools.reduce(lax.psum, axes, array)  31.2 us
    all_to_all x1, waiting for transfers between devices, from_everyone(): return lax.all_to_all(copies, axis, split_axis=0, concat_axis=0, tiled=True)  16.4 us
    all_to_all x1, blocking collectives, from_everyone(): return lax.all_to_all(copies, axis, split_axis=0, concat_axis=0, tiled=True)  13.3 us
    all_to_all x1, blocking collectives, sent_and_summed(): lax.all_to_all(tiles, axis, split_axis=0, concat_axis=0, tiled=True)  11.8 us
    all_to_all x1, starting transfers between devices, from_everyone(): return lax.all_to_all(copies, axis, split_axis=0, concat_axis=0, tiled=True)  9.59 us
    dot_general x1, matrix products, body(): jnp.dot(normed_input, factor_whole, preferred_element_type=jnp.float32)  9.4 us
    split x2, local copies, waits for them, and re-layouts, in_one_piece(): jnp.split(lax.all_gather(both, axis, axis=dim, tiled=True), ends, axis=al...  3.52 us
  transfers between devices with their start and end apart: 2, of which 2 were waited for; matrix products, arithmetic and copies ran while one was open for 0% of the time, Pallas kernels for 0%

commit v1 on v0

v1 whole, which is shorter than its diff:
```python
import jax
import jax.numpy as jnp
from jax import lax
from jax.experimental import pallas as pl
from jax.experimental.pallas import tpu as pltpu
from jax.sharding import Mesh
from jax.sharding import PartitionSpec as P


FS = ("z", "y", "core")
ZY = ("z", "y")
BF16 = jnp.bfloat16
F32 = jnp.float32
VMEM = pl.BlockSpec(memory_space=pltpu.MemorySpace.VMEM)
SMEM = pl.BlockSpec(memory_space=pltpu.MemorySpace.SMEM)
HBM = pl.BlockSpec(memory_space=pltpu.MemorySpace.HBM)
PLACES = {id(VMEM): pltpu.MemorySpace.VMEM, id(HBM): pltpu.MemorySpace.HBM}


def near(dims, kind=F32):
    return pltpu.MemorySpace.VMEM(dims, kind)


def far(dims, kind=F32):
    return jax.ShapeDtypeStruct(dims, kind)


def run(kernel, specs, operands, out, scratch=(), flops=0, limit=8):
    operands = [
        pltpu.with_memory_space_constraint(o, PLACES[id(s)]) if id(s) in PLACES else o
        for s, o in zip(specs, operands)
    ]
    return pl.pallas_call(
        kernel,
        in_specs=list(specs),
        out_specs=[VMEM] * len(out),
        out_shape=list(out),
        scratch_shapes=list(scratch),
        compiler_params=pltpu.CompilerParams(vmem_limit_bytes=limit * 1024 * 1024),
        cost_estimate=pl.CostEstimate(flops=flops, bytes_accessed=0, transcendentals=0),
    )(*operands)


def exchange(tiles, axis):
    return lax.all_to_all(tiles, axis, split_axis=0, concat_axis=0, tiled=True)


def swapped(array, axis, bit):
    count = lax.axis_size(axis)
    return lax.ppermute(array, axis, [(i, i ^ bit) for i in range(count)])


def shifted(array, axis):
    count = lax.axis_size(axis)
    tiles = [array]
    for k in range(1, count):
        tiles.append(lax.ppermute(array, axis, [(i, (i + k) % count) for i in range(count)]))
    return tiles


def fetch(pairs, sems):
    copies = [pltpu.make_async_copy(a, b, sems.at[i]) for i, (a, b) in enumerate(pairs)]
    for copy in copies:
        copy.start()
    for copy in copies:
        copy.wait()


LANES = 128


def spread_kernel(factor_ref, q_ref, kv_ref, factor_out, weight_out, factor_buf, q_buf, kv_buf, sems):
    fetch(((factor_ref, factor_buf), (q_ref, q_buf), (kv_ref, kv_buf)), sems)
    rows = q_ref.shape[0]
    factor = factor_buf[...]
    q, kv = q_buf[...].astype(BF16), kv_buf[...].astype(BF16)
    for i in range(factor_out.shape[0]):
        factor_out[i] = factor
    weight_out[:rows, :LANES] = q[:, :LANES]
    weight_out[:rows, LANES:] = kv
    quarter = rows // 4
    rest = q[:, LANES:]
    for g in range(4):
        weight_out[rows:, 64 * g : 64 * (g + 1)] = rest[quarter * g : quarter * (g + 1)]


def spread(factor, q, kv, count):
    rows = factor.shape[0]
    return run(
        spread_kernel,
        [HBM] * 3,
        (factor, q, kv),
        [near((count, *factor.shape), BF16), near((rows + rows // 4, 2 * LANES), BF16)],
        [
            pltpu.VMEM(factor.shape, BF16),
            pltpu.VMEM(q.shape, F32),
            pltpu.VMEM(kv.shape, F32),
            pltpu.SemaphoreType.DMA((3,)),
        ],
    )


def stack_kernel(*refs):
    for i, ref in enumerate(refs[:-1]):
        refs[-1][i] = ref[...]


def stacked(tiles):
    return run(
        stack_kernel, [VMEM] * len(tiles), tiles, [near((len(tiles), *tiles[0].shape), BF16)]
    )[0]


def gradient_kernel(block, depth):
    def kernel(q_ref, kv_ref, x_ref, out_ref, q_buf, kv_buf, x_buf, sems):
        tokens = x_ref.shape[0]
        steps = tokens // block

        def copies(k):
            at, slot = pl.ds(k * block, block), k % depth
            return (
                pltpu.make_async_copy(q_ref.at[:, at], q_buf.at[slot], sems.at[slot, 0]),
                pltpu.make_async_copy(kv_ref.at[at, :], kv_buf.at[slot], sems.at[slot, 1]),
                pltpu.make_async_copy(x_ref.at[at, :], x_buf.at[slot], sems.at[slot, 2]),
            )

        for k in range(depth):
            for copy in copies(k):
                copy.start()
        for k in range(steps):
            slot = k % depth
            for copy in copies(k):
                copy.wait()
            left = jnp.concatenate([q_buf[slot], kv_buf[slot].T], axis=0)
            piece = jnp.dot(left, x_buf[slot], preferred_element_type=F32)
            if k == 0:
                out_ref[...] = piece
            else:
                out_ref[...] += piece
            if k + depth < steps:
                for copy in copies(k + depth):
                    copy.start()

    return kernel


def gradients(q_turned, kv, x, block=512, depth=4):
    q_width, kv_width = q_turned.shape[0], kv.shape[1]
    width = q_width + kv_width
    tokens, model = x.shape
    return run(
        gradient_kernel(block, depth),
        [HBM] * 3,
        (q_turned, kv, x),
        [near((width, model))],
        [
            pltpu.VMEM((depth, q_width, block), BF16),
            pltpu.VMEM((depth, block, kv_width), BF16),
            pltpu.VMEM((depth, block, model), BF16),
            pltpu.SemaphoreType.DMA((depth, 3)),
        ],
        2 * width * tokens * model,
        20,
    )[0]


def assemble(place_ref, mine_ref, other_ref, factor_ref):
    core = place_ref[2]
    for i in range(mine_ref.shape[0]):
        factor_ref[i, core] = mine_ref[i]
        factor_ref[i, 1 - core] = other_ref[i]
    count, pair, rows, rank = factor_ref.shape
    return factor_ref[...].reshape(count * pair * rows, rank)


def whole_factor(mine):
    count, rows, rank = mine.shape
    return pltpu.VMEM((count, 2, rows, rank), BF16)


def project_kernel(place_ref, mine_ref, other_ref, grad_ref, out_ref, factor_ref):
    factor = assemble(place_ref, mine_ref, other_ref, factor_ref)
    grad = grad_ref[...]
    upper = grad.astype(BF16)
    lower = (grad - upper.astype(F32)).astype(BF16)
    turned = jnp.dot(upper, factor, preferred_element_type=F32) + jnp.dot(
        lower, factor, preferred_element_type=F32
    )
    out_ref[...] = turned.T.astype(BF16)


def project(place, mine, other, grad):
    return run(
        project_kernel,
        [SMEM, VMEM, VMEM, VMEM],
        (place, mine, other, grad),
        [near((mine.shape[2], grad.shape[0]), BF16)],
        [whole_factor(mine)],
    )[0]


def updated(parts_ref, qm_ref, km_ref, qs_ref, ks_ref):
    projected = jnp.sum(parts_ref[...].astype(F32), axis=0)
    q_width = qm_ref.shape[1]
    for value, first_ref, second_ref in (
        (projected[:, :q_width], qm_ref, qs_ref),
        (projected[:, q_width:], km_ref, ks_ref),
    ):
        first = 0.8 * first_ref[...] + 0.2 * value
        second = 0.9 * second_ref[...] + 0.1 * value * value
        yield first, second


def direction_kernel(parts_ref, qm_ref, km_ref, qs_ref, ks_ref, dir_ref):
    at = 0
    for first, second in updated(parts_ref, qm_ref, km_ref, qs_ref, ks_ref):
        direction = (first / (jnp.sqrt(second) + 1e-08)).astype(BF16)
        width = direction.shape[1]
        for i in range(dir_ref.shape[0]):
            dir_ref[i, :, at : at + width] = direction
        at += width


def direction_tiles(parts, moments):
    return run(direction_kernel, [VMEM] * 5, (parts, *moments), [near(parts.shape, BF16)])[0]


def keep_kernel(parts_ref, qm_ref, km_ref, qs_ref, ks_ref, qm_out, km_out, qs_out, ks_out):
    outs = ((qm_out, qs_out), (km_out, ks_out))
    values = updated(parts_ref, qm_ref, km_ref, qs_ref, ks_ref)
    for (first, second), (first_out, second_out) in zip(values, outs):
        first_out[...] = first
        second_out[...] = second


def keep(parts, moments):
    return run(keep_kernel, [VMEM] * 5, (parts, *moments), [far(m.shape) for m in moments])


def stats_kernel(q_width):
    def kernel(dir_ref, out_ref):
        values = dir_ref[...].astype(F32)
        squares = jnp.sum(values * values, axis=0, keepdims=True)
        out_ref[0:1, :] = jnp.broadcast_to(jnp.sum(squares[:, :q_width], axis=1, keepdims=True), (1, 128))
        out_ref[1:2, :] = jnp.broadcast_to(jnp.sum(squares[:, q_width:], axis=1, keepdims=True), (1, 128))
        out_ref[2:, :] = jnp.zeros((6, 128), F32)

    return kernel


def stats(directions, q_width):
    return run(stats_kernel(q_width), [VMEM], (directions,), [near((8, 128))])[0]


def weights_kernel(place_ref, *refs):
    tiles, (q_ref, kv_ref, first_ref, rest_ref) = refs[:-4], refs[-4:]
    z, y, core = place_ref[0], place_ref[1], place_ref[2]
    count = len(tiles) // 2
    rows = first_ref.shape[3]
    quarter = rows // 4
    for t, tile in enumerate(tiles):
        c = core if t < count else 1 - core
        zi = lax.rem(z + count - t % count, count)
        for k in range(count):
            yi = lax.rem(y + count - k, count)
            first_ref[zi, yi, c] = tile[k, :rows, :LANES]
            kv_ref[zi, yi, c] = tile[k, :rows, LANES:]
            for g in range(4):
                rest_ref[zi, yi, c, quarter * g : quarter * (g + 1), :64] = tile[
                    k, rows:, 64 * g : 64 * (g + 1)
                ]
    model = q_ref.shape[1]
    q_ref[:LANES] = first_ref[...].reshape(model, LANES).T
    q_ref[LANES:] = rest_ref[...].reshape(model, LANES).T[:64]


def weights(place, mine, other, rows, q_width, kv_width):
    count = len(mine)
    blocks = (count, count, 2, rows)
    model = count * count * 2 * rows
    q_turned, kv = run(
        weights_kernel,
        [SMEM] + [VMEM] * (2 * count),
        (place, *mine, *other),
        [near((q_width, model), BF16), near((*blocks, kv_width), BF16)],
        [pltpu.VMEM((*blocks, LANES), BF16), pltpu.VMEM((*blocks, LANES), BF16)],
    )
    return q_turned, kv.reshape(model, kv_width)


NT = (((1,), (1,)), ((), ()))


def steps_kernel(place_ref, dir_ref, mine_ref, other_ref, own_ref, q_ref, kv_ref, own_out, factor_ref):
    q_width = q_ref.shape[0]
    factor = assemble(place_ref, mine_ref, other_ref, factor_ref)
    directions = dir_ref[...]
    turned = directions[:, :q_width].T
    q_ref[...] = lax.dot_general(turned, factor, NT, preferred_element_type=F32)
    kv_ref[...] = jnp.dot(factor, directions[:, q_width:], preferred_element_type=F32)
    own_out[...] = jnp.dot(own_ref[...], directions, preferred_element_type=F32)


def unscaled_steps(place, directions, mine, other, own, q_width):
    count, rows, rank = mine.shape
    model, width = 2 * count * rows, directions.shape[1]
    return run(
        steps_kernel,
        [SMEM] + [VMEM] * 4,
        (place, directions, mine, other, own),
        [near((q_width, model)), near((model, width - q_width)), near((own.shape[0], width))],
        [whole_factor(mine)],
        2 * width * rank * model,
    )


def finish_kernel(q_count, kv_count):
    def kernel(
        sums_ref, q_step_ref, kv_step_ref, own_ref, q_whole_ref, kv_whole_ref, q_ref, kv_ref,
        q_new, kv_new, q_step, kv_step, q_copy, kv_copy,
    ):
        q_width = q_ref.shape[1]
        sums = sums_ref[...]
        q_scale = 0.5 * jnp.sqrt(F32(q_count)) * lax.rsqrt(sums[0:1, 0:1] + 1e-06)
        kv_scale = 0.5 * jnp.sqrt(F32(kv_count)) * lax.rsqrt(sums[1:2, 0:1] + 1e-06)
        own = own_ref[...]
        step = q_scale * own[:, :q_width]
        q_step[...] = step
        q_new[...] = q_ref[...] - step
        step = kv_scale * own[:, q_width:]
        kv_step[...] = step
        kv_new[...] = kv_ref[...] - step
        q_copy[...] = (q_whole_ref[...].astype(F32) - q_scale * q_step_ref[...]).astype(BF16)
        kv_copy[...] = (kv_whole_ref[...].astype(F32) - kv_scale * kv_step_ref[...]).astype(BF16)

    return kernel


def finish(sums, q_steps, kv_steps, own, q_whole, kv_whole, q_own, kv_own, q_count, kv_count):
    return run(
        finish_kernel(q_count, kv_count),
        [VMEM] * 8,
        (sums, q_steps, kv_steps, own, q_whole, kv_whole, q_own, kv_own),
        [
            far(q_own.shape),
            far(kv_own.shape),
            far(q_own.shape),
            far(kv_own.shape),
            far(q_whole.shape, BF16),
            far(kv_whole.shape, BF16),
        ],
    )


def body(x, q_cot, kv_cot, row_factor, q_weight, kv_weight, qm, km, qs, ks):
    fs_count = lax.axis_size(FS)
    q_width, kv_width = q_cot.shape[1], kv_cot.shape[1]
    width, rank_rows = q_width + kv_width, qm.shape[0]
    place = jnp.stack([lax.axis_index(a) for a in ("z", "y", "core")]).astype(jnp.int32)
    factor_tiles, weight_rows = spread(row_factor, q_weight, kv_weight, lax.axis_size(ZY))
    mine = exchange(factor_tiles, ZY)
    grad = gradients(q_cot.T, kv_cot, x)
    other = swapped(mine, "core", 1)
    partial = project(place, mine, other, grad)
    parts = exchange(partial.reshape(fs_count, rank_rows, width), FS)
    weight_rows = stacked(shifted(weight_rows, "y"))
    to_send = direction_tiles(parts, (qm, km, qs, ks))
    qm_new, km_new, qs_new, ks_new = keep(parts, (qm, km, qs, ks))
    directions = exchange(to_send, FS).reshape(fs_count * rank_rows, width)
    weight_mine = shifted(weight_rows, "z")
    weight_other = [swapped(w, "core", 1) for w in weight_mine]
    q_whole, kv_whole = weights(
        place, weight_mine, weight_other, q_weight.shape[0], q_width, kv_width
    )
    squares = stats(directions, q_width)
    squares = squares + swapped(squares, "tp", 1)
    squares = squares + swapped(squares, "tp", 2)
    q_steps, kv_steps, own = unscaled_steps(
        place, directions, mine, other, row_factor, q_width
    )
    count = rank_rows * fs_count * lax.axis_size("tp")
    q_new, kv_new, q_step, kv_step, q_copy, kv_copy = finish(
        squares, q_steps, kv_steps, own, q_whole, kv_whole, q_weight, kv_weight,
        count * q_width, count * kv_width,
    )
    return (q_new, kv_new, q_step, kv_step, q_copy.T, kv_copy, qm_new, km_new, qs_new, ks_new)


def solution(mesh):
    split = Mesh(mesh.devices.reshape(4, 4, 2, mesh.shape["tp"]), ("z", "y", "core", "tp"))
    rows, tiles = P(FS, None), P(FS, "tp")
    return jax.shard_map(
        body,
        mesh=split,
        in_specs=(rows, tiles, tiles, rows, tiles, tiles, tiles, tiles, tiles, tiles),
        out_specs=(tiles, tiles, tiles, tiles, P(None, "tp"), P(None, "tp"), tiles, tiles, tiles, tiles),
        check_vma=False,
    )
```

time: 160 us -> 75 us (0.47)
  blocking collectives: 56.4 us -> 12 us
  waiting for transfers between devices: 55.3 us -> 13.7 us
  Pallas kernels: 0 us -> 19.7 us
  starting transfers between devices: 9.63 us -> 28.1 us
  between operations: 15.6 us -> 0.83 us
  matrix products: 11.5 us -> 0 us
  local copies, waits for them, and re-layouts: 7.56 us -> 0.03 us
  other arithmetic: 3.52 us -> 0.08 us
    all_gather x1 -> x0, waiting for transfers between devices: 38.9 us -> none  [in_one_piece(): lax.all_gather(both, axis, axis=dim, tiled=True)]
    psum x4 -> x0, blocking collectives: 31.2 us -> none  [over_axes(): return functools.reduce(lax.psum, axes, array)]
    pallas_call x0 -> x10, Pallas kernels: none -> 19.7 us  [run(): pl.pallas_call(kernel, in_specs=list(specs), out_specs=[VMEM] * len(out),...]
    ppermute x0 -> x13, starting transfers between devices: none -> 13.3 us  [the longest x7 7.99 us: swapped(): return lax.ppermute(array, axis, [(i, i ^ bit) for i in range(count)])]
    all_to_all x2 -> x1, blocking collectives: 25.2 us -> 12 us  [exchange(): return lax.all_to_all(tiles, axis, split_axis=0, concat_axis=0, tiled=True)]
    dot_general x4 -> x0, matrix products: 11.5 us -> none  [the longest x1 9.4 us: body(): jnp.dot(normed_input, factor_whole, preferred_element_type=jnp.float32)]
    all_to_all x1 -> x2, starting transfers between devices: 9.59 us -> 14.9 us  [exchange(): return lax.all_to_all(tiles, axis, split_axis=0, concat_axis=0, tiled=True)]
    split x2 -> x0, local copies, waits for them, and re-layouts: 3.52 us -> none  [in_one_piece(): jnp.split(lax.all_gather(both, axis, axis=dim, tiled=True), ends, axis=al...]
  transfers between devices with their start and end apart: 2 -> 15, of which waited for: 2 -> 3; matrix products, arithmetic and copies ran while one was open for 0% -> 0% of each run, Pallas kernels for 0% -> 22%
where the time goes in v1:
time: 75 us; the launch traced here: 74.4 us
  starting transfers between devices  28.1 us (37%)
  Pallas kernels  19.7 us (26%)
  waiting for transfers between devices  13.7 us (18%)
  blocking collectives  12 us (16%)
  between operations  0.83 us (1%)
    pallas_call x10, Pallas kernels, run(): pl.pallas_call(kernel, in_specs=list(specs), out_specs=[VMEM] * len(out),...  19.7 us
    all_to_all x2, starting transfers between devices, exchange(): return lax.all_to_all(tiles, axis, split_axis=0, concat_axis=0, tiled=True)  14.9 us
    all_to_all x2, waiting for transfers between devices, exchange(): return lax.all_to_all(tiles, axis, split_axis=0, concat_axis=0, tiled=True)  13.2 us
    all_to_all x1, blocking collectives, exchange(): return lax.all_to_all(tiles, axis, split_axis=0, concat_axis=0, tiled=True)  12 us
    ppermute x7, starting transfers between devices, swapped(): return lax.ppermute(array, axis, [(i, i ^ bit) for i in range(count)])  7.99 us
    ppermute x6, starting transfers between devices, shifted(): lax.ppermute(array, axis, [(i, (i + k) % count) for i in range(count)])  5.27 us
  transfers between devices with their start and end apart: 15, of which 3 were waited for; matrix products, arithmetic and copies ran while one was open for 0% of the time, Pallas kernels for 22%

profile of v1, /device:TPU:1, one launch (start us, length us, event | category | flops | bytes accessed | tf_op | source)
XLA Modules:
  0.0 74.4 jit_solution(18010885384963316836)
XLA Ops:
  0.6 1.7 %shard_map.177 = (bf16[16,64,256]{2,1,0:T(8,128)(2,1)}, bf16[80,256]{1,0:T(8,128)(2,1)S(1)}) custom-call(bf16[64,256]{1,0:T(8,128)(2,1)} %own_ref.1, f32[64,192]{1,0:T(8,128)} %q_ref.3, f32[64,128]{1,0:T(8,128)} %kv_ref.5), custom_call_target="tpu_custom_call" | custom-call | tf_op jit(solution)/shard_map/pallas_call | solution.py:33
  2.4 8.6 %all-to-all-start = ((bf16[16,64,256]{2,1,0:T(8,128)(2,1)}), bf16[16,64,256]{2,1,0:T(8,128)(2,1)S(1)}, u32[]{:S(2)}, u32[]{:S(2)}) async-start(bf16[16,64,256]{2,1,0:T(8,128)(2,1)} %get-tuple-element.27), calls=%async_computation | async-start | bytes 1048576 | tf_op jit(solution)/shard_map/all_to_all | solution.py:45
  11.0 2.6 %collective-permute-start.5 = (bf16[80,256]{1,0:T(8,128)(2,1)S(1)}, bf16[80,256]{1,0:T(8,128)(2,1)S(1)}, u32[]{:S(2)}, u32[]{:S(2)}) collective-permute-start(bf16[80,256]{1,0:T(8,128)(2,1)S(1)} %get-tuple-element.31.refs_0_), channel_id=1, source_target_pairs={{0,24},{8,0},{16,8},{24,16},{1,25},{9,1},{17,9},{25,17},{2,26},{10... | collective-permute-start | bytes 122888 | tf_op jit(solution)/shard_map/ppermute | solution.py:57
  13.6 0.6 collective-permute-start.4
  14.1 0.6 collective-permute-start.3
  14.7 6.7 %all-to-all-done.mine_ref = bf16[16,64,256]{2,1,0:T(8,128)(2,1)S(1)} async-done(((bf16[16,64,256]{2,1,0:T(8,128)(2,1)}), bf16[16,64,256]{2,1,0:T(8,128)(2,1)S(1)}, u32[]{:S(2)}, u32[]{:S(2)}) %all-to-all-start) | async-done | bytes 524320 | tf_op jit(solution)/shard_map/all_to_all | solution.py:45
  21.4 2.9 %collective-permute-start = (bf16[16,64,256]{2,1,0:T(8,128)(2,1)S(1)}, bf16[16,64,256]{2,1,0:T(8,128)(2,1)}, u32[]{:S(2)}, u32[]{:S(2)}) collective-permute-start(bf16[16,64,256]{2,1,0:T(8,128)(2,1)S(1)} %all-to-all-done.mine_ref), channel_id=1, source_target_pairs={{0,4},{4,0},{1,5},{5,1},{2,6},{6,2},{3,7},{7,3},{8,12},{12,8},{9,1... | collective-permute-start | bytes 1572872 | tf_op jit(solution)/shard_map/ppermute | solution.py:50
  24.3 9.1 %shard_map.178.grad_ref = f32[320,2048]{1,0:T(8,128)S(1)} custom-call(bf16[192,4608]{1,0:T(8,128)(2,1)} %bitcast.11, bf16[4608,128]{1,0:T(8,128)(2,1)} %kv_ref.4, bf16[4608,2048]{1,0:T(8,128)(2,1)} %x_ref.1), custom_call_target="tpu_custom_call" | custom-call | flops 6039797760 | tf_op jit(solution)/shard_map/pallas_call | solution.py:33
  33.4 0.0 collective-permute-done.5.refs_3_
  33.4 0.0 collective-permute-done.4.refs_2_
  33.5 0.0 collective-permute-done.3.refs_1_
  33.5 0.6 collective-permute-start.8
  34.1 0.3 collective-permute-start.7
  34.4 0.6 collective-permute-start.6
  35.0 0.1 pad_add_fusion.place_ref
  35.1 0.0 collective-permute-done.other_ref
  35.1 2.8 %shard_map.179 = bf16[256,320]{1,0:T(8,128)(2,1)} custom-call(s32[3]{0:T(128)S(1)} %pad_add_fusion.place_ref, bf16[16,64,256]{2,1,0:T(8,128)(2,1)S(1)} %all-to-all-done.mine_ref, bf16[16,64,256]{2,1,0:T(8,128)(2,1)} %collective-permute-done.other_ref, f32[320,2048]{1,0:T(8,128)S(1)} %shard_map.178.grad_ref), custom_call_target="tpu_custom_call" | custom-call | tf_op jit(solution)/shard_map/pallas_call | solution.py:33
  37.9 6.3 %all-to-all-start.1 = ((bf16[32,8,320]{2,1,0:T(8,128)(2,1)}), bf16[32,8,320]{2,1,0:T(8,128)(2,1)S(1)}, u32[]{:S(2)}, u32[]{:S(2)}) async-start(bf16[32,8,320]{2,1,0:T(8,128)(2,1)} %bitcast.4), calls=%async_computation.1 | async-start | bytes 393216 | tf_op jit(solution)/shard_map/all_to_all | solution.py:45
  44.2 0.3 collective-permute-start.9
  44.5 0.0 collective-permute-done.8.refs_3_
  44.5 0.3 collective-permute-start.12
  44.8 0.0 collective-permute-done.7.refs_2_
  44.8 0.2 collective-permute-start.11
  45.0 0.4 collective-permute-done.6.refs_1_
  45.4 0.5 collective-permute-start.10
  45.9 6.5 %all-to-all-done.1.parts_ref = bf16[32,8,320]{2,1,0:T(8,128)(2,1)S(1)} async-done(((bf16[32,8,320]{2,1,0:T(8,128)(2,1)}), bf16[32,8,320]{2,1,0:T(8,128)(2,1)S(1)}, u32[]{:S(2)}, u32[]{:S(2)}) %all-to-all-start.1) | async-done | bytes 163872 | tf_op jit(solution)/shard_map/all_to_all | solution.py:45
  52.4 0.0 copy-done.3
  52.4 0.0 copy-done.4
  52.4 0.0 copy-done.5
  52.4 0.0 copy-done.6
  52.4 0.2 shard_map.180
  52.6 0.0 copy-start
  52.7 0.0 copy-start.1
  52.7 12.0 %all_to_all.15 = bf16[32,8,320]{2,1,0:T(8,128)(2,1)S(1)} all-to-all(bf16[32,8,320]{2,1,0:T(8,128)(2,1)S(1)} %shard_map.180), channel_id=1, replica_groups=mesh['z'=4,'y'=4,'core'=2,'tp'=4] {'z','y','core'}, dimensions={0} | all-to-all | bytes 327680 | tf_op jit(solution)/shard_map/all_to_all | solution.py:45
  64.6 0.2 shard_map.181
  64.8 1.2 %collective-permute-start.1 = (f32[8,128]{1,0:T(8,128)S(1)}, f32[8,128]{1,0:T(8,128)S(1)}, u32[]{:S(2)}, u32[]{:S(2)}) collective-permute-start(f32[8,128]{1,0:T(8,128)S(1)} %shard_map.181), channel_id=1, source_target_pairs={{0,1},{1,0},{2,3},{3,2},{4,5},{5,4},{6,7},{7,6},{8,9},{9,8},{10,11... | collective-permute-start | bytes 12296 | tf_op jit(solution)/shard_map/ppermute | solution.py:50
  66.1 0.0 collective-permute-done.9.refs_4_
  66.1 0.0 collective-permute-done.12.refs_7_
  66.1 0.0 collective-permute-done.11.refs_6_
  66.1 0.0 collective-permute-done.10.refs_5_
  66.1 1.6 %shard_map.184 = (bf16[192,2048]{1,0:T(8,128)(2,1)S(1)}, bf16[4,4,2,64,128]{4,3,2,1,0:T(8,128)(2,1)S(1)}) custom-call(s32[3]{0:T(128)S(1)} %pad_add_fusion.place_ref, bf16[4,80,256]{2,1,0:T(8,128)(2,1)S(1)} %shard_map.183.refs_0_, bf16[4,80,256]{2,1,0:T(8,128)(2,1)} %collective-permute-done.6.refs_1_, bf16[4,80,256]{2,1,0:T(8,128)(2,1)} %collective-permute-done.7.refs_2_, ...), custom_call_target="tpu_custom_call" | custom-call | tf_op jit(solution)/shard_map/pallas_call | solution.py:33
  67.7 0.7 shard_map.186
  68.4 0.0 collective-permute-done.1
  68.4 2.5 %collective-permute-start.2 = (f32[8,128]{1,0:T(8,128)S(1)}, f32[8,128]{1,0:T(8,128)S(1)}, u32[]{:S(2)}, u32[]{:S(2)}) collective-permute-start(f32[8,128]{1,0:T(8,128)S(1)} %add.6), channel_id=1, source_target_pairs={{0,2},{1,3},{2,0},{3,1},{4,6},{5,7},{6,4},{7,5},{8,10},{9,11},{10,... | collective-permute-start | bytes 12296 | tf_op jit(solution)/shard_map/ppermute | solution.py:50
  70.9 0.0 copy-done.2
  70.9 1.9 %shard_map.182 = (f32[192,2048]{1,0:T(8,128)S(1)}, f32[2048,128]{1,0:T(8,128)S(1)}, f32[64,320]{1,0:T(8,128)S(1)}) custom-call(s32[3]{0:T(128)S(1)} %pad_add_fusion.place_ref, bf16[256,320]{1,0:T(8,128)(2,1)S(1)} %bitcast.9, bf16[16,64,256]{2,1,0:T(8,128)(2,1)S(1)} %all-to-all-done.mine_ref, bf16[16,64,256]{2,1,0:T(8,128)(2,1)} %collective-permute-done.other_ref, ...), custom_call_target="tpu_custom_call" | custom-call | flops 335544320 | tf_op jit(solution)/shard_map/pallas_call | solution.py:33
  72.9 0.0 collective-permute-done.2
  72.9 1.5 %shard_map.185 = (f32[64,192]{1,0:T(8,128)}, f32[64,128]{1,0:T(8,128)}, f32[64,192]{1,0:T(8,128)}, f32[64,128]{1,0:T(8,128)}, bf16[192,2048]{1,0:T(8,128)(2,1)}, /*index=5*/bf16[2048,128]{1,0:T(8,128)(2,1)}) custom-call(f32[8,128]{1,0:T(8,128)S(1)} %add.7.sums_ref, f32[192,2048]{1,0:T(8,128)S(1)} %get-tuple-element.28.q_step_ref, ...), custom_call_target="tpu_custom_call" | custom-call | tf_op jit(solution)/shard_map/pallas_call | solution.py:33
  (10 shorter events, 0.0 us)
Async XLA Ops:
  2.4 19.0 %all-to-all-start = ((bf16[16,64,256]{2,1,0:T(8,128)(2,1)}), bf16[16,64,256]{2,1,0:T(8,128)(2,1)S(1)}, u32[]{:S(2)}, u32[]{:S(2)}) async-start(bf16[16,64,256]{2,1,0:T(8,128)(2,1)} %get-tuple-element.27), calls=%async_computation | async-start | bytes 1048576 | tf_op jit(solution)/shard_map/all_to_all | solution.py:45
  11.0 22.5 %collective-permute-start.5 = (bf16[80,256]{1,0:T(8,128)(2,1)S(1)}, bf16[80,256]{1,0:T(8,128)(2,1)S(1)}, u32[]{:S(2)}, u32[]{:S(2)}) collective-permute-start(bf16[80,256]{1,0:T(8,128)(2,1)S(1)} %get-tuple-element.31.refs_0_), channel_id=1, source_target_pairs={{0,24},{8,0},{16,8},{24,16},{1,25},{9,1},{17,9},{25,17},{2,26},{10... | collective-permute-start | bytes 122888 | tf_op jit(solution)/shard_map/ppermute | solution.py:57
  13.6 19.9 %collective-permute-start.4 = (bf16[80,256]{1,0:T(8,128)(2,1)S(1)}, bf16[80,256]{1,0:T(8,128)(2,1)S(1)}, u32[]{:S(2)}, u32[]{:S(2)}) collective-permute-start(bf16[80,256]{1,0:T(8,128)(2,1)S(1)} %get-tuple-element.31.refs_0_), channel_id=1, source_target_pairs={{0,16},{8,24},{16,0},{24,8},{1,17},{9,25},{17,1},{25,9},{2,18},{10... | collective-permute-start | bytes 122888 | tf_op jit(solution)/shard_map/ppermute | solution.py:57
  14.1 19.3 %collective-permute-start.3 = (bf16[80,256]{1,0:T(8,128)(2,1)S(1)}, bf16[80,256]{1,0:T(8,128)(2,1)S(1)}, u32[]{:S(2)}, u32[]{:S(2)}) collective-permute-start(bf16[80,256]{1,0:T(8,128)(2,1)S(1)} %get-tuple-element.31.refs_0_), channel_id=1, source_target_pairs={{0,8},{8,16},{16,24},{24,0},{1,9},{9,17},{17,25},{25,1},{2,10},{10... | collective-permute-start | bytes 122888 | tf_op jit(solution)/shard_map/ppermute | solution.py:57
  21.4 13.7 %collective-permute-start = (bf16[16,64,256]{2,1,0:T(8,128)(2,1)S(1)}, bf16[16,64,256]{2,1,0:T(8,128)(2,1)}, u32[]{:S(2)}, u32[]{:S(2)}) collective-permute-start(bf16[16,64,256]{2,1,0:T(8,128)(2,1)S(1)} %all-to-all-done.mine_ref), channel_id=1, source_target_pairs={{0,4},{4,0},{1,5},{5,1},{2,6},{6,2},{3,7},{7,3},{8,12},{12,8},{9,1... | collective-permute-start | bytes 1572872 | tf_op jit(solution)/shard_map/ppermute | solution.py:50
  33.5 11.0 %collective-permute-start.8 = (bf16[4,80,256]{2,1,0:T(8,128)(2,1)S(1)}, bf16[4,80,256]{2,1,0:T(8,128)(2,1)S(1)}, u32[]{:S(2)}, u32[]{:S(2)}) collective-permute-start(bf16[4,80,256]{2,1,0:T(8,128)(2,1)S(1)} %shard_map.183.refs_0_), channel_id=1, source_target_pairs={{0,96},{32,0},{64,32},{96,64},{1,97},{33,1},{65,33},{97,65},{2,98}... | collective-permute-start | bytes 491528 | tf_op jit(solution)/shard_map/ppermute | solution.py:57
  34.1 10.6 %collective-permute-start.7 = (bf16[4,80,256]{2,1,0:T(8,128)(2,1)S(1)}, bf16[4,80,256]{2,1,0:T(8,128)(2,1)}, u32[]{:S(2)}, u32[]{:S(2)}) collective-permute-start(bf16[4,80,256]{2,1,0:T(8,128)(2,1)S(1)} %shard_map.183.refs_0_), channel_id=1, source_target_pairs={{0,64},{32,96},{64,0},{96,32},{1,65},{33,97},{65,1},{97,33},{2,66}... | collective-permute-start | bytes 491528 | tf_op jit(solution)/shard_map/ppermute | solution.py:57
  34.4 11.0 %collective-permute-start.6 = (bf16[4,80,256]{2,1,0:T(8,128)(2,1)S(1)}, bf16[4,80,256]{2,1,0:T(8,128)(2,1)}, u32[]{:S(2)}, u32[]{:S(2)}) collective-permute-start(bf16[4,80,256]{2,1,0:T(8,128)(2,1)S(1)} %shard_map.183.refs_0_), channel_id=1, source_target_pairs={{0,32},{32,64},{64,96},{96,0},{1,33},{33,65},{65,97},{97,1},{2,34}... | collective-permute-start | bytes 491528 | tf_op jit(solution)/shard_map/ppermute | solution.py:57
  35.1 17.3 %copy-start.3 = (f32[8,192]{1,0:T(8,128)S(1)}, f32[8,192]{1,0:T(8,128)}, u32[]{:S(2)}) copy-start(f32[8,192]{1,0:T(8,128)} %qm_ref.3) | copy-start | bytes 18436
  35.1 17.3 %copy-start.4 = (f32[8,192]{1,0:T(8,128)S(1)}, f32[8,192]{1,0:T(8,128)}, u32[]{:S(2)}) copy-start(f32[8,192]{1,0:T(8,128)} %qs_ref.3) | copy-start | bytes 18436
  35.1 17.3 %copy-start.5 = (f32[8,128]{1,0:T(8,128)S(1)}, f32[8,128]{1,0:T(8,128)}, u32[]{:S(2)}) copy-start(f32[8,128]{1,0:T(8,128)} %km_ref.3) | copy-start | bytes 12292
  35.1 17.3 %copy-start.6 = (f32[8,128]{1,0:T(8,128)S(1)}, f32[8,128]{1,0:T(8,128)}, u32[]{:S(2)}) copy-start(f32[8,128]{1,0:T(8,128)} %ks_ref.3) | copy-start | bytes 12292
  37.9 33.0 %copy-start.2 = (bf16[64,256]{1,0:T(8,128)(2,1)S(1)}, bf16[64,256]{1,0:T(8,128)(2,1)}, u32[]{:S(2)}) copy-start(bf16[64,256]{1,0:T(8,128)(2,1)} %own_ref.1) | copy-start | bytes 98308
  37.9 14.5 %all-to-all-start.1 = ((bf16[32,8,320]{2,1,0:T(8,128)(2,1)}), bf16[32,8,320]{2,1,0:T(8,128)(2,1)S(1)}, u32[]{:S(2)}, u32[]{:S(2)}) async-start(bf16[32,8,320]{2,1,0:T(8,128)(2,1)} %bitcast.4), calls=%async_computation.1 | async-start | bytes 393216 | tf_op jit(solution)/shard_map/all_to_all | solution.py:45
  44.2 21.9 %collective-permute-start.9 = (bf16[4,80,256]{2,1,0:T(8,128)(2,1)S(1)}, bf16[4,80,256]{2,1,0:T(8,128)(2,1)S(1)}, u32[]{:S(2)}, u32[]{:S(2)}) collective-permute-start(bf16[4,80,256]{2,1,0:T(8,128)(2,1)S(1)} %shard_map.183.refs_0_), channel_id=1, source_target_pairs={{0,4},{4,0},{1,5},{5,1},{2,6},{6,2},{3,7},{7,3},{8,12},{12,8},{9,1... | collective-permute-start | bytes 491528 | tf_op jit(solution)/shard_map/ppermute | solution.py:50
  44.5 21.6 %collective-permute-start.12 = (bf16[4,80,256]{2,1,0:T(8,128)(2,1)S(1)}, bf16[4,80,256]{2,1,0:T(8,128)(2,1)S(1)}, u32[]{:S(2)}, u32[]{:S(2)}) collective-permute-start(bf16[4,80,256]{2,1,0:T(8,128)(2,1)S(1)} %collective-permute-done.8.refs_3_), channel_id=1, source_target_pairs={{0,4},{4,0},{1,5},{5,1},{2,6},{6,2},{3,7},{7,3},{8,12},{12,8},{9,1... | collective-permute-start | bytes 491528 | tf_op jit(solution)/shard_map/ppermute | solution.py:50
  44.8 21.3 %collective-permute-start.11 = (bf16[4,80,256]{2,1,0:T(8,128)(2,1)}, bf16[4,80,256]{2,1,0:T(8,128)(2,1)S(1)}, u32[]{:S(2)}, u32[]{:S(2)}) collective-permute-start(bf16[4,80,256]{2,1,0:T(8,128)(2,1)} %collective-permute-done.7.refs_2_), channel_id=1, source_target_pairs={{0,4},{4,0},{1,5},{5,1},{2,6},{6,2},{3,7},{7,3},{8,12},{12,8},{9,1... | collective-permute-start | bytes 491528 | tf_op jit(solution)/shard_map/ppermute | solution.py:50
  45.4 20.7 %collective-permute-start.10 = (bf16[4,80,256]{2,1,0:T(8,128)(2,1)}, bf16[4,80,256]{2,1,0:T(8,128)(2,1)S(1)}, u32[]{:S(2)}, u32[]{:S(2)}) collective-permute-start(bf16[4,80,256]{2,1,0:T(8,128)(2,1)} %collective-permute-done.6.refs_1_), channel_id=1, source_target_pairs={{0,4},{4,0},{1,5},{5,1},{2,6},{6,2},{3,7},{7,3},{8,12},{12,8},{9,1... | collective-permute-start | bytes 491528 | tf_op jit(solution)/shard_map/ppermute | solution.py:50
  52.6 20.2 %copy-start = (f32[64,192]{1,0:T(8,128)S(1)}, f32[64,192]{1,0:T(8,128)}, u32[]{:S(2)}) copy-start(f32[64,192]{1,0:T(8,128)} %q_ref.3) | copy-start | bytes 147460
  52.7 20.2 %copy-start.1 = (f32[64,128]{1,0:T(8,128)S(1)}, f32[64,128]{1,0:T(8,128)}, u32[]{:S(2)}) copy-start(f32[64,128]{1,0:T(8,128)} %kv_ref.5) | copy-start | bytes 98308
  64.8 3.6 %collective-permute-start.1 = (f32[8,128]{1,0:T(8,128)S(1)}, f32[8,128]{1,0:T(8,128)S(1)}, u32[]{:S(2)}, u32[]{:S(2)}) collective-permute-start(f32[8,128]{1,0:T(8,128)S(1)} %shard_map.181), channel_id=1, source_target_pairs={{0,1},{1,0},{2,3},{3,2},{4,5},{5,4},{6,7},{7,6},{8,9},{9,8},{10,11... | collective-permute-start | bytes 12296 | tf_op jit(solution)/shard_map/ppermute | solution.py:50
  68.4 4.5 %collective-permute-start.2 = (f32[8,128]{1,0:T(8,128)S(1)}, f32[8,128]{1,0:T(8,128)S(1)}, u32[]{:S(2)}, u32[]{:S(2)}) collective-permute-start(f32[8,128]{1,0:T(8,128)S(1)} %add.6), channel_id=1, source_target_pairs={{0,2},{1,3},{2,0},{3,1},{4,6},{5,7},{6,4},{7,5},{8,10},{9,11},{10,... | collective-permute-start | bytes 12296 | tf_op jit(solution)/shard_map/ppermute | solution.py:50

commit v2 on v1

v2 whole, which is shorter than its diff:
```python
import jax
import jax.numpy as jnp
from jax import lax
from jax.experimental import pallas as pl
from jax.experimental.pallas import tpu as pltpu
from jax.sharding import Mesh
from jax.sharding import PartitionSpec as P


FS = ("z", "y", "core")
ZY = ("z", "y")
BF16 = jnp.bfloat16
F32 = jnp.float32
VMEM = pl.BlockSpec(memory_space=pltpu.MemorySpace.VMEM)
HBM = pl.BlockSpec(memory_space=pltpu.MemorySpace.HBM)
PLACES = {id(VMEM): pltpu.MemorySpace.VMEM, id(HBM): pltpu.MemorySpace.HBM}


def near(dims, kind=F32):
    return pltpu.MemorySpace.VMEM(dims, kind)


def far(dims, kind=F32):
    return jax.ShapeDtypeStruct(dims, kind)


def run(kernel, specs, operands, out, scratch=(), flops=0, limit=8, outs=None):
    operands = [
        pltpu.with_memory_space_constraint(o, PLACES[id(s)]) if id(s) in PLACES else o
        for s, o in zip(specs, operands)
    ]
    return pl.pallas_call(
        kernel,
        in_specs=list(specs),
        out_specs=outs or [VMEM] * len(out),
        out_shape=list(out),
        scratch_shapes=list(scratch),
        compiler_params=pltpu.CompilerParams(vmem_limit_bytes=limit * 1024 * 1024),
        cost_estimate=pl.CostEstimate(flops=flops, bytes_accessed=0, transcendentals=0),
    )(*operands)


def exchange(tiles, axis):
    return lax.all_to_all(tiles, axis, split_axis=0, concat_axis=0, tiled=True)


def swapped(array, axis, bit):
    count = lax.axis_size(axis)
    return lax.ppermute(array, axis, [(i, i ^ bit) for i in range(count)])


def shifted(array, axis, k):
    count = lax.axis_size(axis)
    return lax.ppermute(array, axis, [(i, (i + k) % count) for i in range(count)])


def fetch(pairs, sems):
    copies = [pltpu.make_async_copy(a, b, sems.at[i]) for i, (a, b) in enumerate(pairs)]
    for copy in copies:
        copy.start()
    for copy in copies:
        copy.wait()


LANES = 128
HALF = LANES // 2


def spread_kernel(
    factor_ref, q_ref, kv_ref, qm_ref, km_ref, qs_ref, ks_ref, factor_out, rows_out, moments_out,
    factor_buf, q_buf, kv_buf, qm_buf, km_buf, qs_buf, ks_buf, sems,
):
    fetch(
        (
            (factor_ref, factor_buf),
            (q_ref, q_buf),
            (kv_ref, kv_buf),
            (qm_ref, qm_buf),
            (km_ref, km_buf),
            (qs_ref, qs_buf),
            (ks_ref, ks_buf),
        ),
        sems,
    )
    factor = factor_buf[...]
    for i in range(factor_out.shape[0]):
        factor_out[i] = factor
    q_width = q_ref.shape[1]
    moments_out[0, :, :q_width] = qm_buf[...]
    moments_out[0, :, q_width:] = km_buf[...]
    moments_out[1, :, :q_width] = qs_buf[...]
    moments_out[1, :, q_width:] = ks_buf[...]
    rows = q_ref.shape[0]
    quarter = rows // 4
    q = q_buf[...].astype(BF16)
    rows_out[0, :rows, :LANES] = q[:, :LANES]
    rows_out[0, :rows, LANES:] = kv_buf[...].astype(BF16)
    for g in range(4):
        rows_out[0, rows:, HALF * g : HALF * (g + 1)] = q[quarter * g : quarter * (g + 1), LANES:]


def spread(factor, q, kv, qm, km, qs, ks, count):
    rows, width = q.shape[0], q.shape[1] + kv.shape[1]
    operands = (factor, q, kv, qm, km, qs, ks)
    return run(
        spread_kernel,
        [HBM] * 7,
        operands,
        [
            near((count, *factor.shape), BF16),
            near((1, rows + rows // 4, 2 * LANES), BF16),
            near((2, qm.shape[0], width)),
        ],
        [pltpu.VMEM(o.shape, o.dtype) for o in operands] + [pltpu.SemaphoreType.DMA((7,))],
    )


def stack_kernel(*refs):
    at = 0
    for ref in refs[:-1]:
        count = ref.shape[0]
        refs[-1][at : at + count] = ref[...]
        at += count


def stacked(tiles):
    count = sum(t.shape[0] for t in tiles)
    return run(
        stack_kernel, [VMEM] * len(tiles), tiles, [near((count, *tiles[0].shape[1:]), BF16)]
    )[0]


def gradient_kernel(q_ref, kv_ref, x_ref, out_ref, sum_ref, q_buf, kv_buf, x_buf, sems):
    depth, block, _ = x_buf.shape
    steps = x_ref.shape[0] // block

    def copies(k):
        at, slot = pl.ds(k * block, block), k % depth
        return (
            pltpu.make_async_copy(q_ref.at[:, at], q_buf.at[slot], sems.at[slot, 0]),
            pltpu.make_async_copy(kv_ref.at[at, :], kv_buf.at[slot], sems.at[slot, 1]),
            pltpu.make_async_copy(x_ref.at[at, :], x_buf.at[slot], sems.at[slot, 2]),
        )

    for k in range(depth):
        for copy in copies(k):
            copy.start()
    for k in range(steps):
        slot = k % depth
        for copy in copies(k):
            copy.wait()
        left = jnp.concatenate([q_buf[slot], kv_buf[slot].T], axis=0)
        piece = jnp.dot(left, x_buf[slot], preferred_element_type=F32)
        if k == 0:
            sum_ref[...] = piece
        elif k < steps - 1:
            sum_ref[...] += piece
        else:
            out_ref[...] = (sum_ref[...] + piece).astype(BF16)
        if k + depth < steps:
            for copy in copies(k + depth):
                copy.start()


def gradients(q_turned, kv, x, block=512, depth=4):
    q_width, kv_width = q_turned.shape[0], kv.shape[1]
    width = q_width + kv_width
    tokens, model = x.shape
    return run(
        gradient_kernel,
        [HBM] * 3,
        (q_turned, kv, x),
        [near((width, model), BF16)],
        [
            pltpu.VMEM((width, model), F32),
            pltpu.VMEM((depth, q_width, block), BF16),
            pltpu.VMEM((depth, block, kv_width), BF16),
            pltpu.VMEM((depth, block, model), BF16),
            pltpu.SemaphoreType.DMA((depth, 3)),
        ],
        2 * width * tokens * model,
        24,
    )[0]


def project_kernel(mine_ref, other_ref, grad_ref, out_ref, factor_ref):
    core = lax.axis_index("core")
    count, pair, rows, rank = factor_ref.shape
    for i in range(count):
        factor_ref[i, core] = mine_ref[i]
        factor_ref[i, 1 - core] = other_ref[i]
    factor = factor_ref[...].reshape(count * pair * rows, rank)
    out_ref[...] = jnp.dot(grad_ref[...], factor, preferred_element_type=F32).T.astype(BF16)


def project(mine, other, grad):
    count, rows, rank = mine.shape
    partial, factor = run(
        project_kernel,
        [VMEM] * 3,
        (mine, other, grad),
        [near((rank, grad.shape[0]), BF16), near((count, 2, rows, rank), BF16)],
    )
    return partial, factor.reshape(count * 2 * rows, rank)


def pair_kernel(parts_ref, moments_ref, out_ref):
    rows = parts_ref.shape[1]
    half = rows // 2
    out_ref[:rows] = jnp.sum(parts_ref[...].astype(F32), axis=0)
    out_ref[rows : rows + half] = moments_ref[0]
    out_ref[rows + half :] = moments_ref[1]


def pair_sums(parts, moments):
    rows, width = parts.shape[1:]
    return run(pair_kernel, [VMEM] * 2, (parts, moments), [near((2 * rows, width))])[0]


def update(value, first, second):
    return 0.8 * first + 0.2 * value, 0.9 * second + 0.1 * value * value


def direction_kernel(mine_ref, other_ref, out_ref, moments_ref):
    core = lax.axis_index("core")
    count, rows, _ = out_ref.shape
    half = rows // 2
    for ref, at in ((mine_ref, core * half), (other_ref, (1 - core) * half)):
        at = pl.ds(pl.multiple_of(at, half), half)
        moments_ref[0, at, :] = ref[rows : rows + half]
        moments_ref[1, at, :] = ref[rows + half :]
    value = mine_ref[:rows] + other_ref[:rows]
    first, second = update(value, moments_ref[0], moments_ref[1])
    direction = (first / (jnp.sqrt(second) + 1e-08)).astype(BF16)
    for i in range(count):
        out_ref[i] = direction


def direction_tiles(mine, other, count):
    rows, width = mine.shape[0] // 2, mine.shape[1]
    return run(
        direction_kernel,
        [VMEM] * 2,
        (mine, other),
        [near((count, rows, width), BF16)],
        [pltpu.VMEM((2, rows, width), F32)],
    )[0]


def keep_kernel(mine_ref, other_ref, qm_out, km_out, qs_out, ks_out):
    half, q_width = qm_out.shape
    rows = 2 * half
    at = pl.ds(pl.multiple_of(lax.axis_index("core") * half, half), half)
    value = mine_ref[at, :] + other_ref[at, :]
    first, second = update(value, mine_ref[rows : rows + half], mine_ref[rows + half :])
    qm_out[...] = first[:, :q_width]
    km_out[...] = first[:, q_width:]
    qs_out[...] = second[:, :q_width]
    ks_out[...] = second[:, q_width:]


def keep(mine, other, outs):
    return run(keep_kernel, [VMEM] * 2, (mine, other), [far(o.shape) for o in outs])


def stats_kernel(q_width):
    def kernel(dir_ref, out_ref):
        values = dir_ref[...].astype(F32)
        squares = jnp.sum(values * values, axis=0, keepdims=True)
        out_ref[0:1, :] = jnp.broadcast_to(jnp.sum(squares[:, :q_width], axis=1, keepdims=True), (1, 128))
        out_ref[1:2, :] = jnp.broadcast_to(jnp.sum(squares[:, q_width:], axis=1, keepdims=True), (1, 128))
        out_ref[2:, :] = jnp.zeros((6, 128), F32)

    return kernel


def stats(directions, q_width):
    return run(stats_kernel(q_width), [VMEM], (directions,), [near((8, 128))])[0]


def weights_kernel(*refs):
    tiles, (q_ref, kv_ref, first_ref, rest_ref) = refs[:-4], refs[-4:]
    z, y, core = (lax.axis_index(a) for a in ("z", "y", "core"))
    count = first_ref.shape[0]
    rows = first_ref.shape[3]
    quarter = rows // 4
    pieces = len(tiles) // 2
    half = count // 2
    origins = ((0, 0), (count - 1, 0), (1, 0), (half, 0), (half, half))
    for t, tile in enumerate(tiles):
        c = core if t < pieces else 1 - core
        dz, dy = origins[t % pieces]
        zi = lax.rem(z + dz, count)
        for k in range(tile.shape[0]):
            yi = lax.rem(y + count - dy - k, count)
            first_ref[zi, yi, c] = tile[k, :rows, :LANES]
            kv_ref[zi, yi, c] = tile[k, :rows, LANES:]
            for g in range(4):
                rest_ref[zi, yi, c, quarter * g : quarter * (g + 1), :HALF] = tile[
                    k, rows:, HALF * g : HALF * (g + 1)
                ]
    model = q_ref.shape[1]
    q_ref[:LANES] = first_ref[...].reshape(model, LANES).T
    q_ref[LANES:] = rest_ref[...].reshape(model, LANES).T[:HALF]


def weights(mine, other, rows, q_width, kv_width):
    count = mine[0].shape[0]
    blocks = (count, count, 2, rows)
    model = count * count * 2 * rows
    q_turned, kv = run(
        weights_kernel,
        [VMEM] * (2 * len(mine)),
        (*mine, *other),
        [near((q_width, model), BF16), near((*blocks, kv_width), BF16)],
        [pltpu.VMEM((*blocks, LANES), BF16), pltpu.VMEM((*blocks, LANES), BF16)],
    )
    return q_turned, kv.reshape(model, kv_width)


NT = (((1,), (1,)), ((), ()))


def steps_kernel(dir_ref, factor_ref, own_ref, q_ref, kv_ref, own_out):
    q_width = q_ref.shape[0]
    directions = dir_ref[...]
    factor = factor_ref[...]
    turned = directions[:, :q_width].T
    q_ref[...] = lax.dot_general(turned, factor, NT, preferred_element_type=F32)
    kv_ref[...] = jnp.dot(factor, directions[:, q_width:], preferred_element_type=F32)
    own_out[...] = jnp.dot(own_ref[...], directions, preferred_element_type=F32)


def unscaled_steps(directions, factor, own, q_width):
    model, width = factor.shape[0], directions.shape[1]
    return run(
        steps_kernel,
        [VMEM] * 3,
        (directions, factor, own),
        [near((q_width, model)), near((model, width - q_width)), near((own.shape[0], width))],
        flops=2 * width * directions.shape[0] * model,
    )


def finish_kernel(q_count, kv_count):
    def kernel(
        squares_0, squares_1, squares_2, squares_3, q_step_ref, kv_step_ref, own_ref, q_whole_ref, kv_whole_ref, q_ref, kv_ref,
        q_new, kv_new, q_step, kv_step, q_copy, kv_copy,
    ):
        q_width = q_ref.shape[1]
        sums = squares_0[...] + squares_1[...] + squares_2[...] + squares_3[...]
        q_scale = 0.5 * jnp.sqrt(F32(q_count)) * lax.rsqrt(sums[0:1, 0:1] + 1e-06)
        kv_scale = 0.5 * jnp.sqrt(F32(kv_count)) * lax.rsqrt(sums[1:2, 0:1] + 1e-06)
        own = own_ref[...]
        step = q_scale * own[:, :q_width]
        q_step[...] = step
        q_new[...] = q_ref[...] - step
        step = kv_scale * own[:, q_width:]
        kv_step[...] = step
        kv_new[...] = kv_ref[...] - step
        q_copy[...] = (q_whole_ref[...].astype(F32) - q_scale * q_step_ref[...]).astype(BF16)
        kv_copy[...] = (kv_whole_ref[...].astype(F32) - kv_scale * kv_step_ref[...]).astype(BF16)

    return kernel


def finish(squares, q_steps, kv_steps, own, q_whole, kv_whole, q_own, kv_own, q_count, kv_count):
    return run(
        finish_kernel(q_count, kv_count),
        [VMEM] * 11,
        (*squares, q_steps, kv_steps, own, q_whole, kv_whole, q_own, kv_own),
        [
            far(q_own.shape),
            far(kv_own.shape),
            far(q_own.shape),
            far(kv_own.shape),
            far(q_whole.shape, BF16),
            far(kv_whole.shape, BF16),
        ],
    )


def body(x, q_cot, kv_cot, row_factor, q_weight, kv_weight, qm, km, qs, ks):
    fs_count = lax.axis_size(FS)
    q_width, kv_width = q_cot.shape[1], kv_cot.shape[1]
    width, rank_rows = q_width + kv_width, qm.shape[0]
    chips = lax.axis_size(ZY)
    factor_tiles, weight_rows, moments = spread(
        row_factor, q_weight, kv_weight, qm, km, qs, ks, chips
    )
    mine = exchange(factor_tiles, ZY)
    grad = gradients(q_cot.T, kv_cot, x)
    mine, weight_rows, moments, grad = lax.optimization_barrier((mine, weight_rows, moments, grad))
    other = swapped(mine, "core", 1)
    weight_near = [shifted(weight_rows, "y", k) for k in (1, 2, 3)]
    partial, factor = project(mine, other, grad)
    parts = exchange(partial.reshape(chips, 2 * rank_rows, width), ZY)
    weight_stack = stacked((weight_rows, *weight_near))
    sums = pair_sums(parts, moments)
    more = swapped(sums, "core", 1)
    to_send = direction_tiles(sums, more, chips)
    qm_new, km_new, qs_new, ks_new = keep(sums, more, (qm, km, qs, ks))
    directions = exchange(to_send, ZY).reshape(fs_count * rank_rows, width)
    below = shifted(weight_stack, "z", 1)
    above = shifted(weight_stack, "z", 3)
    middle = weight_stack.shape[0] // 2
    weight_mine = (
        weight_stack, below, above, shifted(below[:middle], "z", 1), shifted(above[middle:], "z", 3)
    )
    weight_other = [swapped(w, "core", 1) for w in weight_mine]
    q_whole, kv_whole = weights(
        weight_mine, weight_other, q_weight.shape[0], q_width, kv_width
    )
    squares = stats(directions, q_width)
    squares = [squares] + [shifted(squares, "tp", k) for k in (2, 1, 3)]
    q_steps, kv_steps, own = unscaled_steps(directions, factor, row_factor, q_width)
    count = rank_rows * fs_count * lax.axis_size("tp")
    q_new, kv_new, q_step, kv_step, q_copy, kv_copy = finish(
        squares, q_steps, kv_steps, own, q_whole, kv_whole, q_weight, kv_weight,
        count * q_width, count * kv_width,
    )
    return (q_new, kv_new, q_step, kv_step, q_copy.T, kv_copy, qm_new, km_new, qs_new, ks_new)


def solution(mesh):
    split = Mesh(mesh.devices.reshape(4, 4, 2, mesh.shape["tp"]), ("z", "y", "core", "tp"))
    rows, tiles = P(FS, None), P(FS, "tp")
    return jax.shard_map(
        body,
        mesh=split,
        in_specs=(rows, tiles, tiles, rows, tiles, tiles, tiles, tiles, tiles, tiles),
        out_specs=(tiles, tiles, tiles, tiles, P(None, "tp"), P(None, "tp"), tiles, tiles, tiles, tiles),
        check_vma=False,
    )
```

time: 75 us -> 69.8 us (0.931)
  the two profiles are of different devices: /device:TPU:1 before, /device:TPU:6 now
where the time goes in v2:
time: 69.8 us; the launch traced here: 69.4 us
  starting transfers between devices  33.7 us (48%)
  waiting for transfers between devices  17.2 us (25%)
  Pallas kernels  16.8 us (24%)
  local copies, waits for them, and re-layouts  0.91 us (1%)
  between operations  0.83 us (1%)
    all_to_all x3, starting transfers between devices, exchange(): return lax.all_to_all(tiles, axis, split_axis=0, concat_axis=0, tiled=True)  20.3 us
    pallas_call x11, Pallas kernels, run(): pl.pallas_call(kernel, in_specs=list(specs), out_specs=outs or [VMEM] * l...  16.8 us
    all_to_all x3, waiting for transfers between devices, exchange(): return lax.all_to_all(tiles, axis, split_axis=0, concat_axis=0, tiled=True)  12.1 us
    ppermute x10, starting transfers between devices, shifted(): lax.ppermute(array, axis, [(i, (i + k) % count) for i in range(count)])  11.6 us
    ppermute x10, waiting for transfers between devices, shifted(): lax.ppermute(array, axis, [(i, (i + k) % count) for i in range(count)])  4.12 us
    ppermute x7, starting transfers between devices, swapped(): return lax.ppermute(array, axis, [(i, i ^ bit) for i in range(count)])  1.74 us
  transfers between devices with their start and end apart: 20, of which 7 were waited for; matrix products, arithmetic and copies ran while one was open for 0% of the time, Pallas kernels for 19%

profile of v2, /device:TPU:6, one launch (start us, length us, event | category | flops | bytes accessed | tf_op | source)
XLA Modules:
  0.0 69.4 jit_solution(7202348767581976399)
XLA Ops:
  0.6 1.8 %shard_map.177 = (bf16[16,64,256]{2,1,0:T(8,128)(2,1)}, bf16[1,80,256]{2,1,0:T(8,128)(2,1)S(1)}, f32[2,8,320]{2,1,0:T(8,128)S(1)}) custom-call(bf16[64,256]{1,0:T(8,128)(2,1)} %own_ref.1, f32[64,192]{1,0:T(8,128)} %q_ref.3, f32[64,128]{1,0:T(8,128)} %kv_ref.5, f32[8,192]{1,0:T(8,128)} %qm_ref.1, f32[8,128]{1,0:T(8,128)} %km_ref.1, f32[8,192]{1,0:T(8,128)} %qs_ref.1, ...), custom_call_target="tpu_custom_call" | custom-call | tf_op jit(solution)/shard_map/pallas_call | solution.py:32
  2.4 8.1 %all-to-all-start = ((bf16[16,64,256]{2,1,0:T(8,128)(2,1)}), bf16[16,64,256]{2,1,0:T(8,128)(2,1)S(1)}, u32[]{:S(2)}, u32[]{:S(2)}) async-start(bf16[16,64,256]{2,1,0:T(8,128)(2,1)} %get-tuple-element.34), calls=%async_computation | async-start | bytes 1048576 | tf_op jit(solution)/shard_map/all_to_all | solution.py:44
  10.5 9.1 %shard_map.178.grad_ref = bf16[320,2048]{1,0:T(8,128)(2,1)S(1)} custom-call(bf16[192,4608]{1,0:T(8,128)(2,1)} %bitcast.10, bf16[4608,128]{1,0:T(8,128)(2,1)} %kv_ref.4, bf16[4608,2048]{1,0:T(8,128)(2,1)} %x_ref.1), custom_call_target="tpu_custom_call" | custom-call | flops 6039797760 | tf_op jit(solution)/shard_map/pallas_call | solution.py:32
  19.6 2.4 %all-to-all-done.mine_ref = bf16[16,64,256]{2,1,0:T(8,128)(2,1)S(1)} async-done(((bf16[16,64,256]{2,1,0:T(8,128)(2,1)}), bf16[16,64,256]{2,1,0:T(8,128)(2,1)S(1)}, u32[]{:S(2)}, u32[]{:S(2)}) %all-to-all-start) | async-done | bytes 524320 | tf_op jit(solution)/shard_map/all_to_all | solution.py:44
  22.0 0.0 collective-permute-start
  22.0 0.9 %collective-permute-start.7 = (bf16[1,80,256]{2,1,0:T(8,128)(2,1)S(1)}, bf16[1,80,256]{2,1,0:T(8,128)(2,1)S(1)}, u32[]{:S(2)}, u32[]{:S(2)}) collective-permute-start(bf16[1,80,256]{2,1,0:T(8,128)(2,1)S(1)} %get-tuple-element.45.refs_0_), channel_id=1, source_target_pairs={{0,24},{8,0},{16,8},{24,16},{1,25},{9,1},{17,9},{25,17},{2,26},{10... | collective-permute-start | bytes 122888 | tf_op jit(solution)/shard_map/ppermute | solution.py:54
  22.9 1.7 %collective-permute-start.6 = (bf16[1,80,256]{2,1,0:T(8,128)(2,1)S(1)}, bf16[1,80,256]{2,1,0:T(8,128)(2,1)S(1)}, u32[]{:S(2)}, u32[]{:S(2)}) collective-permute-start(bf16[1,80,256]{2,1,0:T(8,128)(2,1)S(1)} %get-tuple-element.45.refs_0_), channel_id=1, source_target_pairs={{0,16},{8,24},{16,0},{24,8},{1,17},{9,25},{17,1},{25,9},{2,18},{10... | collective-permute-start | bytes 122888 | tf_op jit(solution)/shard_map/ppermute | solution.py:54
  24.7 0.0 collective-permute-start.5
  24.7 0.0 collective-permute-done.other_ref
  24.7 1.3 %shard_map.179 = (bf16[256,320]{1,0:T(8,128)(2,1)}, bf16[16,2,64,256]{3,2,1,0:T(8,128)(2,1)S(1)}) custom-call(bf16[16,64,256]{2,1,0:T(8,128)(2,1)S(1)} %all-to-all-done.mine_ref, bf16[16,64,256]{2,1,0:T(8,128)(2,1)S(1)} %collective-permute-done.other_ref, bf16[320,2048]{1,0:T(8,128)(2,1)S(1)} %shard_map.178.grad_ref), custom_call_target="tpu_custom_call" | custom-call | tf_op jit(solution)/shard_map/pallas_call | solution.py:32
  26.0 6.1 %all-to-all-start.1 = ((bf16[16,16,320]{2,1,0:T(8,128)(2,1)}), bf16[16,16,320]{2,1,0:T(8,128)(2,1)S(1)}, u32[]{:S(2)}, u32[]{:S(2)}) async-start(bf16[16,16,320]{2,1,0:T(8,128)(2,1)} %bitcast.1), calls=%async_computation.1 | async-start | bytes 393216 | tf_op jit(solution)/shard_map/all_to_all | solution.py:44
  32.1 0.0 copy-start.4
  32.2 0.0 collective-permute-done.7.refs_3_
  32.2 0.0 collective-permute-done.6.refs_2_
  32.2 0.0 collective-permute-done.5.refs_1_
  32.2 3.2 %collective-permute-start.9 = (bf16[4,80,256]{2,1,0:T(8,128)(2,1)S(1)}, bf16[4,80,256]{2,1,0:T(8,128)(2,1)S(1)}, u32[]{:S(2)}, u32[]{:S(2)}) collective-permute-start(bf16[4,80,256]{2,1,0:T(8,128)(2,1)S(1)} %shard_map.184.refs_0_), channel_id=1, source_target_pairs={{0,96},{32,0},{64,32},{96,64},{1,97},{33,1},{65,33},{97,65},{2,98}... | collective-permute-start | bytes 491528 | tf_op jit(solution)/shard_map/ppermute | solution.py:54
  35.4 5.1 %all-to-all-done.1.parts_ref = bf16[16,16,320]{2,1,0:T(8,128)(2,1)S(1)} async-done(((bf16[16,16,320]{2,1,0:T(8,128)(2,1)}), bf16[16,16,320]{2,1,0:T(8,128)(2,1)S(1)}, u32[]{:S(2)}, u32[]{:S(2)}) %all-to-all-start.1) | async-done | bytes 163872 | tf_op jit(solution)/shard_map/all_to_all | solution.py:44
  40.5 0.1 collective-permute-start.1
  40.6 0.5 collective-permute-start.12
  41.1 0.0 collective-permute-done.9.refs_2_
  41.1 2.2 %collective-permute-start.11 = (bf16[2,80,256]{2,1,0:T(8,128)(2,1)S(1)}, bf16[2,80,256]{2,1,0:T(8,128)(2,1)S(1)}, u32[]{:S(2)}, u32[]{:S(2)}) collective-permute-start(bf16[2,80,256]{2,1,0:T(8,128)(2,1)S(1)} %slice.9), channel_id=1, source_target_pairs={{0,96},{32,0},{64,32},{96,64},{1,97},{33,1},{65,33},{97,65},{2,98}... | collective-permute-start | bytes 245768 | tf_op jit(solution)/shard_map/ppermute | solution.py:54
  43.3 0.0 collective-permute-done.8.refs_1_
  43.4 0.1 collective-permute-start.10
  43.4 0.1 collective-permute-start.14
  43.5 0.5 collective-permute-start.13
  44.0 0.7 %shard_map.181 = bf16[16,16,320]{2,1,0:T(8,128)(2,1)} custom-call(f32[32,320]{1,0:T(8,128)S(1)} %shard_map.180.mine_ref, f32[32,320]{1,0:T(8,128)S(1)} %collective-permute-done.1.other_ref), custom_call_target="tpu_custom_call" | custom-call | tf_op jit(solution)/shard_map/pallas_call | solution.py:32
  44.8 6.1 %all-to-all-start.2 = ((bf16[16,16,320]{2,1,0:T(8,128)(2,1)}), bf16[16,16,320]{2,1,0:T(8,128)(2,1)S(1)}, u32[]{:S(2)}, u32[]{:S(2)}) async-start(bf16[16,16,320]{2,1,0:T(8,128)(2,1)} %shard_map.181), calls=%async_computation.2 | async-start | bytes 393216 | tf_op jit(solution)/shard_map/all_to_all | solution.py:44
  50.9 0.0 collective-permute-done.11.refs_4_
  50.9 0.1 collective-permute-start.16
  51.0 0.5 collective-permute-start.15
  51.5 0.0 collective-permute-done.12.refs_5_
  51.5 0.8 %collective-permute-done.16.refs_9_ = bf16[2,80,256]{2,1,0:T(8,128)(2,1)S(1)} collective-permute-done((bf16[2,80,256]{2,1,0:T(8,128)(2,1)S(1)}, bf16[2,80,256]{2,1,0:T(8,128)(2,1)S(1)}, u32[]{:S(2)}, u32[]{:S(2)}) %collective-permute-start.16) | collective-permute-done | bytes 81952 | tf_op jit(solution)/shard_map/ppermute | solution.py:49
  52.3 0.0 collective-permute-done.14.refs_7_
  52.3 0.2 collective-permute-done.15.refs_8_
  52.4 0.0 collective-permute-done.13.refs_6_
  52.4 0.6 shard_map.185
  53.0 0.0 copy-start
  53.1 0.9 %copy-done = bf16[192,2048]{1,0:T(8,128)(2,1)} copy-done((bf16[192,2048]{1,0:T(8,128)(2,1)}, bf16[192,2048]{1,0:T(8,128)(2,1)S(1)}, u32[]{:S(2)}) %copy-start) | copy-done | bytes 786456
  53.9 0.7 shard_map.187
  54.6 4.6 %all-to-all-done.2 = bf16[16,16,320]{2,1,0:T(8,128)(2,1)S(1)} async-done(((bf16[16,16,320]{2,1,0:T(8,128)(2,1)}), bf16[16,16,320]{2,1,0:T(8,128)(2,1)S(1)}, u32[]{:S(2)}, u32[]{:S(2)}) %all-to-all-start.2) | async-done | bytes 163872 | tf_op jit(solution)/shard_map/all_to_all | solution.py:44
  59.3 0.2 shard_map.182.squares_0
  59.4 0.8 %collective-permute-start.4 = (f32[8,128]{1,0:T(8,128)S(1)}, f32[8,128]{1,0:T(8,128)S(1)}, u32[]{:S(2)}, u32[]{:S(2)}) collective-permute-start(f32[8,128]{1,0:T(8,128)S(1)} %shard_map.182.squares_0), channel_id=1, source_target_pairs={{0,3},{1,0},{2,1},{3,2},{4,7},{5,4},{6,5},{7,6},{8,11},{9,8},{10,9... | collective-permute-start | bytes 12296 | tf_op jit(solution)/shard_map/ppermute | solution.py:54
  60.3 2.4 %collective-permute-start.3 = (f32[8,128]{1,0:T(8,128)S(1)}, f32[8,128]{1,0:T(8,128)S(1)}, u32[]{:S(2)}, u32[]{:S(2)}) collective-permute-start(f32[8,128]{1,0:T(8,128)S(1)} %shard_map.182.squares_0), channel_id=1, source_target_pairs={{0,1},{1,2},{2,3},{3,0},{4,5},{5,6},{6,7},{7,4},{8,9},{9,10},{10,1... | collective-permute-start | bytes 12296 | tf_op jit(solution)/shard_map/ppermute | solution.py:54
  62.7 0.2 collective-permute-start.2
  62.9 0.8 %shard_map.183 = (f32[192,2048]{1,0:T(8,128)S(1)}, f32[2048,128]{1,0:T(8,128)S(1)}, f32[64,320]{1,0:T(8,128)S(1)}) custom-call(bf16[256,320]{1,0:T(8,128)(2,1)S(1)} %bitcast.7, bf16[2048,256]{1,0:T(8,128)(2,1)S(1)} %bitcast.8, bf16[64,256]{1,0:T(8,128)(2,1)S(1)} %copy-done.4), custom_call_target="tpu_custom_call" | custom-call | flops 335544320 | tf_op jit(solution)/shard_map/pallas_call | solution.py:32
  63.7 0.6 collective-permute-done.4.squares_3
  64.3 3.5 %collective-permute-done.2.squares_1 = f32[8,128]{1,0:T(8,128)S(1)} collective-permute-done((f32[8,128]{1,0:T(8,128)S(1)}, f32[8,128]{1,0:T(8,128)S(1)}, u32[]{:S(2)}, u32[]{:S(2)}) %collective-permute-start.2) | collective-permute-done | bytes 4128 | tf_op jit(solution)/shard_map/ppermute | solution.py:54
  67.8 1.5 %shard_map.186 = (f32[64,192]{1,0:T(8,128)}, f32[64,128]{1,0:T(8,128)}, f32[64,192]{1,0:T(8,128)}, f32[64,128]{1,0:T(8,128)}, bf16[192,2048]{1,0:T(8,128)(2,1)}, /*index=5*/bf16[2048,128]{1,0:T(8,128)(2,1)}) custom-call(f32[8,128]{1,0:T(8,128)S(1)} %shard_map.182.squares_0, f32[8,128]{1,0:T(8,128)S(1)} %collective-permute-done.2.squares_1, ...), custom_call_target="tpu_custom_call" | custom-call | tf_op jit(solution)/shard_map/pallas_call | solution.py:32
  (15 shorter events, 0.1 us)
Async XLA Ops:
  2.4 19.6 %all-to-all-start = ((bf16[16,64,256]{2,1,0:T(8,128)(2,1)}), bf16[16,64,256]{2,1,0:T(8,128)(2,1)S(1)}, u32[]{:S(2)}, u32[]{:S(2)}) async-start(bf16[16,64,256]{2,1,0:T(8,128)(2,1)} %get-tuple-element.34), calls=%async_computation | async-start | bytes 1048576 | tf_op jit(solution)/shard_map/all_to_all | solution.py:44
  22.0 2.6 %collective-permute-start = (bf16[16,64,256]{2,1,0:T(8,128)(2,1)S(1)}, bf16[16,64,256]{2,1,0:T(8,128)(2,1)S(1)}, u32[]{:S(2)}, u32[]{:S(2)}) collective-permute-start(bf16[16,64,256]{2,1,0:T(8,128)(2,1)S(1)} %all-to-all-done.mine_ref), channel_id=1, source_target_pairs={{0,4},{4,0},{1,5},{5,1},{2,6},{6,2},{3,7},{7,3},{8,12},{12,8},{9,1... | collective-permute-start | bytes 1572872 | tf_op jit(solution)/shard_map/ppermute | solution.py:49
  22.0 10.1 %collective-permute-start.7 = (bf16[1,80,256]{2,1,0:T(8,128)(2,1)S(1)}, bf16[1,80,256]{2,1,0:T(8,128)(2,1)S(1)}, u32[]{:S(2)}, u32[]{:S(2)}) collective-permute-start(bf16[1,80,256]{2,1,0:T(8,128)(2,1)S(1)} %get-tuple-element.45.refs_0_), channel_id=1, source_target_pairs={{0,24},{8,0},{16,8},{24,16},{1,25},{9,1},{17,9},{25,17},{2,26},{10... | collective-permute-start | bytes 122888 | tf_op jit(solution)/shard_map/ppermute | solution.py:54
  22.9 9.3 %collective-permute-start.6 = (bf16[1,80,256]{2,1,0:T(8,128)(2,1)S(1)}, bf16[1,80,256]{2,1,0:T(8,128)(2,1)S(1)}, u32[]{:S(2)}, u32[]{:S(2)}) collective-permute-start(bf16[1,80,256]{2,1,0:T(8,128)(2,1)S(1)} %get-tuple-element.45.refs_0_), channel_id=1, source_target_pairs={{0,16},{8,24},{16,0},{24,8},{1,17},{9,25},{17,1},{25,9},{2,18},{10... | collective-permute-start | bytes 122888 | tf_op jit(solution)/shard_map/ppermute | solution.py:54
  24.7 7.5 %collective-permute-start.5 = (bf16[1,80,256]{2,1,0:T(8,128)(2,1)S(1)}, bf16[1,80,256]{2,1,0:T(8,128)(2,1)S(1)}, u32[]{:S(2)}, u32[]{:S(2)}) collective-permute-start(bf16[1,80,256]{2,1,0:T(8,128)(2,1)S(1)} %get-tuple-element.45.refs_0_), channel_id=1, source_target_pairs={{0,8},{8,16},{16,24},{24,0},{1,9},{9,17},{17,25},{25,1},{2,10},{10... | collective-permute-start | bytes 122888 | tf_op jit(solution)/shard_map/ppermute | solution.py:54
  26.0 14.5 %all-to-all-start.1 = ((bf16[16,16,320]{2,1,0:T(8,128)(2,1)}), bf16[16,16,320]{2,1,0:T(8,128)(2,1)S(1)}, u32[]{:S(2)}, u32[]{:S(2)}) async-start(bf16[16,16,320]{2,1,0:T(8,128)(2,1)} %bitcast.1), calls=%async_computation.1 | async-start | bytes 393216 | tf_op jit(solution)/shard_map/all_to_all | solution.py:44
  32.1 30.7 %copy-start.4 = (bf16[64,256]{1,0:T(8,128)(2,1)S(1)}, bf16[64,256]{1,0:T(8,128)(2,1)}, u32[]{:S(2)}) copy-start(bf16[64,256]{1,0:T(8,128)(2,1)} %own_ref.1) | copy-start | bytes 98308
  32.2 8.9 %collective-permute-start.9 = (bf16[4,80,256]{2,1,0:T(8,128)(2,1)S(1)}, bf16[4,80,256]{2,1,0:T(8,128)(2,1)S(1)}, u32[]{:S(2)}, u32[]{:S(2)}) collective-permute-start(bf16[4,80,256]{2,1,0:T(8,128)(2,1)S(1)} %shard_map.184.refs_0_), channel_id=1, source_target_pairs={{0,96},{32,0},{64,32},{96,64},{1,97},{33,1},{65,33},{97,65},{2,98}... | collective-permute-start | bytes 491528 | tf_op jit(solution)/shard_map/ppermute | solution.py:54
  35.4 7.9 %collective-permute-start.8 = (bf16[4,80,256]{2,1,0:T(8,128)(2,1)S(1)}, bf16[4,80,256]{2,1,0:T(8,128)(2,1)S(1)}, u32[]{:S(2)}, u32[]{:S(2)}) collective-permute-start(bf16[4,80,256]{2,1,0:T(8,128)(2,1)S(1)} %shard_map.184.refs_0_), channel_id=1, source_target_pairs={{0,32},{32,64},{64,96},{96,0},{1,33},{33,65},{65,97},{97,1},{2,34}... | collective-permute-start | bytes 491528 | tf_op jit(solution)/shard_map/ppermute | solution.py:54
  40.5 3.0 %collective-permute-start.1 = (f32[32,320]{1,0:T(8,128)S(1)}, f32[32,320]{1,0:T(8,128)S(1)}, u32[]{:S(2)}, u32[]{:S(2)}) collective-permute-start(f32[32,320]{1,0:T(8,128)S(1)} %shard_map.180.mine_ref), channel_id=1, source_target_pairs={{0,4},{4,0},{1,5},{5,1},{2,6},{6,2},{3,7},{7,3},{8,12},{12,8},{9,1... | collective-permute-start | bytes 122888 | tf_op jit(solution)/shard_map/ppermute | solution.py:49
  40.6 10.9 %collective-permute-start.12 = (bf16[4,80,256]{2,1,0:T(8,128)(2,1)S(1)}, bf16[4,80,256]{2,1,0:T(8,128)(2,1)S(1)}, u32[]{:S(2)}, u32[]{:S(2)}) collective-permute-start(bf16[4,80,256]{2,1,0:T(8,128)(2,1)S(1)} %shard_map.184.refs_0_), channel_id=1, source_target_pairs={{0,4},{4,0},{1,5},{5,1},{2,6},{6,2},{3,7},{7,3},{8,12},{12,8},{9,1... | collective-permute-start | bytes 491528 | tf_op jit(solution)/shard_map/ppermute | solution.py:49
  41.1 9.8 %collective-permute-start.11 = (bf16[2,80,256]{2,1,0:T(8,128)(2,1)S(1)}, bf16[2,80,256]{2,1,0:T(8,128)(2,1)S(1)}, u32[]{:S(2)}, u32[]{:S(2)}) collective-permute-start(bf16[2,80,256]{2,1,0:T(8,128)(2,1)S(1)} %slice.9), channel_id=1, source_target_pairs={{0,96},{32,0},{64,32},{96,64},{1,97},{33,1},{65,33},{97,65},{2,98}... | collective-permute-start | bytes 245768 | tf_op jit(solution)/shard_map/ppermute | solution.py:54
  43.4 7.7 %collective-permute-start.10 = (bf16[2,80,256]{2,1,0:T(8,128)(2,1)S(1)}, bf16[2,80,256]{2,1,0:T(8,128)(2,1)S(1)}, u32[]{:S(2)}, u32[]{:S(2)}) collective-permute-start(bf16[2,80,256]{2,1,0:T(8,128)(2,1)S(1)} %slice.8), channel_id=1, source_target_pairs={{0,32},{32,64},{64,96},{96,0},{1,33},{33,65},{65,97},{97,1},{2,34}... | collective-permute-start | bytes 245768 | tf_op jit(solution)/shard_map/ppermute | solution.py:54
  43.4 8.8 %collective-permute-start.14 = (bf16[4,80,256]{2,1,0:T(8,128)(2,1)S(1)}, bf16[4,80,256]{2,1,0:T(8,128)(2,1)S(1)}, u32[]{:S(2)}, u32[]{:S(2)}) collective-permute-start(bf16[4,80,256]{2,1,0:T(8,128)(2,1)S(1)} %collective-permute-done.9.refs_2_), channel_id=1, source_target_pairs={{0,4},{4,0},{1,5},{5,1},{2,6},{6,2},{3,7},{7,3},{8,12},{12,8},{9,1... | collective-permute-start | bytes 491528 | tf_op jit(solution)/shard_map/ppermute | solution.py:49
  43.5 8.9 %collective-permute-start.13 = (bf16[4,80,256]{2,1,0:T(8,128)(2,1)S(1)}, bf16[4,80,256]{2,1,0:T(8,128)(2,1)S(1)}, u32[]{:S(2)}, u32[]{:S(2)}) collective-permute-start(bf16[4,80,256]{2,1,0:T(8,128)(2,1)S(1)} %collective-permute-done.8.refs_1_), channel_id=1, source_target_pairs={{0,4},{4,0},{1,5},{5,1},{2,6},{6,2},{3,7},{7,3},{8,12},{12,8},{9,1... | collective-permute-start | bytes 491528 | tf_op jit(solution)/shard_map/ppermute | solution.py:49
  44.8 23.0 %copy-start.2 = (f32[64,192]{1,0:T(8,128)S(1)}, f32[64,192]{1,0:T(8,128)}, u32[]{:S(2)}) copy-start(f32[64,192]{1,0:T(8,128)} %q_ref.3) | copy-start | bytes 147460
  44.8 23.0 %copy-start.3 = (f32[64,128]{1,0:T(8,128)S(1)}, f32[64,128]{1,0:T(8,128)}, u32[]{:S(2)}) copy-start(f32[64,128]{1,0:T(8,128)} %kv_ref.5) | copy-start | bytes 98308
  44.8 14.5 %all-to-all-start.2 = ((bf16[16,16,320]{2,1,0:T(8,128)(2,1)}), bf16[16,16,320]{2,1,0:T(8,128)(2,1)S(1)}, u32[]{:S(2)}, u32[]{:S(2)}) async-start(bf16[16,16,320]{2,1,0:T(8,128)(2,1)} %shard_map.181), calls=%async_computation.2 | async-start | bytes 393216 | tf_op jit(solution)/shard_map/all_to_all | solution.py:44
  50.9 1.4 %collective-permute-start.16 = (bf16[2,80,256]{2,1,0:T(8,128)(2,1)S(1)}, bf16[2,80,256]{2,1,0:T(8,128)(2,1)S(1)}, u32[]{:S(2)}, u32[]{:S(2)}) collective-permute-start(bf16[2,80,256]{2,1,0:T(8,128)(2,1)S(1)} %collective-permute-done.11.refs_4_), channel_id=1, source_target_pairs={{0,4},{4,0},{1,5},{5,1},{2,6},{6,2},{3,7},{7,3},{8,12},{12,8},{9,1... | collective-permute-start | bytes 245768 | tf_op jit(solution)/shard_map/ppermute | solution.py:49
  51.0 1.4 %collective-permute-start.15 = (bf16[2,80,256]{2,1,0:T(8,128)(2,1)S(1)}, bf16[2,80,256]{2,1,0:T(8,128)(2,1)S(1)}, u32[]{:S(2)}, u32[]{:S(2)}) collective-permute-start(bf16[2,80,256]{2,1,0:T(8,128)(2,1)S(1)} %collective-permute-done.10.refs_3_), channel_id=1, source_target_pairs={{0,4},{4,0},{1,5},{5,1},{2,6},{6,2},{3,7},{7,3},{8,12},{12,8},{9,1... | collective-permute-start | bytes 245768 | tf_op jit(solution)/shard_map/ppermute | solution.py:49
  53.0 0.9 %copy-start = (bf16[192,2048]{1,0:T(8,128)(2,1)}, bf16[192,2048]{1,0:T(8,128)(2,1)S(1)}, u32[]{:S(2)}) copy-start(bf16[192,2048]{1,0:T(8,128)(2,1)S(1)} %get-tuple-element.46.q_whole_ref) | copy-start | bytes 2359300
  59.3 8.6 %copy-start.1 = (bf16[192,2048]{1,0:T(8,128)(2,1)S(1)}, bf16[192,2048]{1,0:T(8,128)(2,1)}, u32[]{:S(2)}) copy-start(bf16[192,2048]{1,0:T(8,128)(2,1)} %copy-done) | copy-start | bytes 2359300
  59.4 4.8 %collective-permute-start.4 = (f32[8,128]{1,0:T(8,128)S(1)}, f32[8,128]{1,0:T(8,128)S(1)}, u32[]{:S(2)}, u32[]{:S(2)}) collective-permute-start(f32[8,128]{1,0:T(8,128)S(1)} %shard_map.182.squares_0), channel_id=1, source_target_pairs={{0,3},{1,0},{2,1},{3,2},{4,7},{5,4},{6,5},{7,6},{8,11},{9,8},{10,9... | collective-permute-start | bytes 12296 | tf_op jit(solution)/shard_map/ppermute | solution.py:54
  60.3 4.0 %collective-permute-start.3 = (f32[8,128]{1,0:T(8,128)S(1)}, f32[8,128]{1,0:T(8,128)S(1)}, u32[]{:S(2)}, u32[]{:S(2)}) collective-permute-start(f32[8,128]{1,0:T(8,128)S(1)} %shard_map.182.squares_0), channel_id=1, source_target_pairs={{0,1},{1,2},{2,3},{3,0},{4,5},{5,6},{6,7},{7,4},{8,9},{9,10},{10,1... | collective-permute-start | bytes 12296 | tf_op jit(solution)/shard_map/ppermute | solution.py:54
  62.7 5.1 %collective-permute-start.2 = (f32[8,128]{1,0:T(8,128)S(1)}, f32[8,128]{1,0:T(8,128)S(1)}, u32[]{:S(2)}, u32[]{:S(2)}) collective-permute-start(f32[8,128]{1,0:T(8,128)S(1)} %shard_map.182.squares_0), channel_id=1, source_target_pairs={{0,2},{1,3},{2,0},{3,1},{4,6},{5,7},{6,4},{7,5},{8,10},{9,11},{10,... | collective-permute-start | bytes 12296 | tf_op jit(solution)/shard_map/ppermute | solution.py:54

commit v3 on v2

v3 whole, which is shorter than its diff:
```python
import jax
import jax.numpy as jnp
from jax import lax
from jax.experimental import pallas as pl
from jax.experimental.pallas import tpu as pltpu
from jax.sharding import Mesh
from jax.sharding import PartitionSpec as P


FS = ("z", "y", "core")
ZY = ("z", "y")
BF16 = jnp.bfloat16
F32 = jnp.float32
VMEM = pl.BlockSpec(memory_space=pltpu.MemorySpace.VMEM)
HBM = pl.BlockSpec(memory_space=pltpu.MemorySpace.HBM)
PLACES = {id(VMEM): pltpu.MemorySpace.VMEM, id(HBM): pltpu.MemorySpace.HBM}


def near(dims, kind=F32):
    return pltpu.MemorySpace.VMEM(dims, kind)


def far(dims, kind=F32):
    return jax.ShapeDtypeStruct(dims, kind)


def run(kernel, specs, operands, out, scratch=(), flops=0, limit=8, outs=None):
    operands = [
        pltpu.with_memory_space_constraint(o, PLACES[id(s)]) if id(s) in PLACES else o
        for s, o in zip(specs, operands)
    ]
    return pl.pallas_call(
        kernel,
        in_specs=list(specs),
        out_specs=outs or [VMEM] * len(out),
        out_shape=list(out),
        scratch_shapes=list(scratch),
        compiler_params=pltpu.CompilerParams(vmem_limit_bytes=limit * 1024 * 1024),
        cost_estimate=pl.CostEstimate(flops=flops, bytes_accessed=0, transcendentals=0),
    )(*operands)


def exchange(tiles, axis):
    return lax.all_to_all(tiles, axis, split_axis=0, concat_axis=0, tiled=True)


def swapped(array, axis, bit):
    count = lax.axis_size(axis)
    return lax.ppermute(array, axis, [(i, i ^ bit) for i in range(count)])


def shifted(array, axis, k):
    count = lax.axis_size(axis)
    return lax.ppermute(array, axis, [(i, (i + k) % count) for i in range(count)])


def turned(array, axis):
    sizes = [lax.axis_size(a) for a in FS]
    at = FS.index(axis)
    pairs = []
    for z in range(sizes[0]):
        for y in range(sizes[1]):
            for core in range(sizes[2]):
                here, there = [z, y, core], [z, y, core]
                there[at] = (there[at] + 2 * core - 1) % sizes[at]
                pairs.append(
                    tuple((p[0] * sizes[1] + p[1]) * sizes[2] + p[2] for p in (here, there))
                )
    return lax.ppermute(array, FS, pairs)


LANES = 128
HALF = LANES // 2


def spread_kernel(factor_ref, out_ref, buf_ref, sems):
    count = out_ref.shape[0]
    arrival = pltpu.make_async_copy(factor_ref, buf_ref, sems.at[count])
    arrival.start()
    arrival.wait()
    copies = [pltpu.make_async_copy(buf_ref, out_ref.at[i], sems.at[i]) for i in range(count)]
    for copy in copies:
        copy.start()
    for copy in copies:
        copy.wait()


def spread(factor, count):
    return run(
        spread_kernel,
        [HBM],
        (factor,),
        [far((count, *factor.shape), BF16)],
        [pltpu.VMEM(factor.shape, BF16), pltpu.SemaphoreType.DMA((count + 1,))],
        outs=[HBM],
    )[0]


def fold(q_ref, kv_ref, out_ref):
    rows = q_ref.shape[0]
    quarter = rows // 4
    q = q_ref[...].astype(BF16)
    out_ref[0, :rows, :LANES] = q[:, :LANES]
    out_ref[0, :rows, LANES:] = kv_ref[...].astype(BF16)
    for g in range(4):
        out_ref[0, rows:, HALF * g : HALF * (g + 1)] = q[quarter * g : quarter * (g + 1), LANES:]


def stack_kernel(*refs):
    at = 0
    for ref in refs[:-1]:
        count = ref.shape[0]
        refs[-1][at : at + count] = ref[...]
        at += count


def stacked(tiles):
    count = sum(t.shape[0] for t in tiles)
    return run(
        stack_kernel, [VMEM] * len(tiles), tiles, [near((count, *tiles[0].shape[1:]), BF16)]
    )[0]


def gradient_kernel(
    q_ref, kv_ref, x_ref, qw_ref, kvw_ref, qm_ref, km_ref, qs_ref, ks_ref,
    out_ref, rows_ref, moments_ref, sum_ref, q_buf, kv_buf, x_buf,
    qw_buf, kvw_buf, qm_buf, km_buf, qs_buf, ks_buf, sems, small_sems,
):
    depth, block, _ = x_buf.shape
    steps = x_ref.shape[0] // block
    q_width = q_ref.shape[0]

    def copies(k):
        at, slot = pl.ds(k * block, block), k % depth
        return (
            pltpu.make_async_copy(q_ref.at[:, at], q_buf.at[slot], sems.at[slot, 0]),
            pltpu.make_async_copy(kv_ref.at[at, :], kv_buf.at[slot], sems.at[slot, 1]),
            pltpu.make_async_copy(x_ref.at[at, :], x_buf.at[slot], sems.at[slot, 2]),
        )

    small = [
        pltpu.make_async_copy(a, b, small_sems.at[i])
        for i, (a, b) in enumerate(
            (
                (qw_ref, qw_buf),
                (kvw_ref, kvw_buf),
                (qm_ref, qm_buf),
                (km_ref, km_buf),
                (qs_ref, qs_buf),
                (ks_ref, ks_buf),
            )
        )
    ]
    for k in range(depth):
        for copy in copies(k):
            copy.start()
    for copy in small:
        copy.start()
    for k in range(steps):
        slot = k % depth
        for copy in copies(k):
            copy.wait()
        left = jnp.concatenate([q_buf[slot], kv_buf[slot].T], axis=0)
        piece = jnp.dot(left, x_buf[slot], preferred_element_type=F32)
        if k == 0:
            sum_ref[...] = piece
        elif k < steps - 1:
            sum_ref[...] += piece
        else:
            out_ref[...] = (sum_ref[...] + piece).astype(BF16)
        if k + depth < steps:
            for copy in copies(k + depth):
                copy.start()
        if k == depth:
            for copy in small:
                copy.wait()
            fold(qw_buf, kvw_buf, rows_ref)
            moments_ref[0, :, :q_width] = qm_buf[...]
            moments_ref[0, :, q_width:] = km_buf[...]
            moments_ref[1, :, :q_width] = qs_buf[...]
            moments_ref[1, :, q_width:] = ks_buf[...]


def gradients(q_turned, kv, x, small, block=512, depth=4):
    q_width, kv_width = q_turned.shape[0], kv.shape[1]
    width = q_width + kv_width
    tokens, model = x.shape
    rows, half = small[0].shape[0], small[2].shape[0]
    return run(
        gradient_kernel,
        [HBM] * (3 + len(small)),
        (q_turned, kv, x, *small),
        [
            near((width, model), BF16),
            near((1, rows + rows // 4, 2 * LANES), BF16),
            near((2, half, width)),
        ],
        [
            pltpu.VMEM((width, model), F32),
            pltpu.VMEM((depth, q_width, block), BF16),
            pltpu.VMEM((depth, block, kv_width), BF16),
            pltpu.VMEM((depth, block, model), BF16),
        ]
        + [pltpu.VMEM(a.shape, F32) for a in small]
        + [pltpu.SemaphoreType.DMA((depth, 3)), pltpu.SemaphoreType.DMA((len(small),))],
        2 * width * tokens * model,
        24,
    )


def project_kernel(mine_ref, other_ref, grad_ref, out_ref, factor_ref):
    core = lax.axis_index("core")
    count, pair, rows, rank = factor_ref.shape
    for i in range(count):
        factor_ref[i, core] = mine_ref[i]
        factor_ref[i, 1 - core] = other_ref[i]
    factor = factor_ref[...].reshape(count * pair * rows, rank)
    out_ref[...] = jnp.dot(grad_ref[...], factor, preferred_element_type=F32).T.astype(BF16)


def project(mine, other, grad):
    count, rows, rank = mine.shape
    partial, factor = run(
        project_kernel,
        [VMEM] * 3,
        (mine, other, grad),
        [near((rank, grad.shape[0]), BF16), near((count, 2, rows, rank), BF16)],
    )
    return partial, factor.reshape(count * 2 * rows, rank)


def pair_kernel(parts_ref, moments_ref, out_ref):
    rows = parts_ref.shape[1]
    half = rows // 2
    out_ref[:rows] = jnp.sum(parts_ref[...].astype(F32), axis=0)
    out_ref[rows : rows + half] = moments_ref[0]
    out_ref[rows + half :] = moments_ref[1]


def pair_sums(parts, moments):
    rows, width = parts.shape[1:]
    return run(pair_kernel, [VMEM] * 2, (parts, moments), [near((2 * rows, width))])[0]


def update(value, first, second):
    return 0.8 * first + 0.2 * value, 0.9 * second + 0.1 * value * value


def direction_kernel(mine_ref, other_ref, out_ref, moments_ref):
    core = lax.axis_index("core")
    count, rows, _ = out_ref.shape
    half = rows // 2
    for ref, at in ((mine_ref, core * half), (other_ref, (1 - core) * half)):
        at = pl.ds(pl.multiple_of(at, half), half)
        moments_ref[0, at, :] = ref[rows : rows + half]
        moments_ref[1, at, :] = ref[rows + half :]
    value = mine_ref[:rows] + other_ref[:rows]
    first, second = update(value, moments_ref[0], moments_ref[1])
    direction = (first / (jnp.sqrt(second) + 1e-08)).astype(BF16)
    for i in range(count):
        out_ref[i] = direction


def direction_tiles(mine, other, count):
    rows, width = mine.shape[0] // 2, mine.shape[1]
    return run(
        direction_kernel,
        [VMEM] * 2,
        (mine, other),
        [near((count, rows, width), BF16)],
        [pltpu.VMEM((2, rows, width), F32)],
    )[0]


def stats_kernel(q_width):
    def kernel(dir_ref, out_ref):
        values = dir_ref[...].astype(F32)
        squares = jnp.sum(values * values, axis=0, keepdims=True)
        out_ref[0:1, :] = jnp.broadcast_to(jnp.sum(squares[:, :q_width], axis=1, keepdims=True), (1, 128))
        out_ref[1:2, :] = jnp.broadcast_to(jnp.sum(squares[:, q_width:], axis=1, keepdims=True), (1, 128))
        out_ref[2:, :] = jnp.zeros((6, 128), F32)

    return kernel


def stats(directions, q_width):
    return run(stats_kernel(q_width), [VMEM], (directions,), [near((8, 128))])[0]


def weights_kernel(here_ref, near_ref, over_ref, far_ref, last_ref, q_ref, kv_ref, first_ref, rest_ref):
    z, y, core = (lax.axis_index(a) for a in FS)
    count, _, _, rows, _ = first_ref.shape
    quarter = rows // 4
    turn = 2 * core - 1

    def around(value):
        return lax.rem(value + count, count)

    def pieces(c):
        t = 2 * c - 1
        return [(y, c), (around(y - t), c), (around(y - t), 1 - c), (around(y + count // 2), c)]

    mine, other = pieces(core), pieces(1 - core)
    for ref, zi, order in (
        (here_ref, z, mine + other),
        (near_ref, around(z - turn), mine + other),
        (over_ref, around(z + turn), other + mine),
        (far_ref, around(z + count // 2), mine),
        (last_ref, around(z + count // 2), other),
    ):
        for k, (yi, c) in enumerate(order):
            first_ref[zi, yi, c] = ref[k, :rows, :LANES]
            kv_ref[zi, yi, c] = ref[k, :rows, LANES:]
            for g in range(4):
                rest_ref[zi, yi, c, quarter * g : quarter * (g + 1), :HALF] = ref[
                    k, rows:, HALF * g : HALF * (g + 1)
                ]
    model = q_ref.shape[1]
    q_ref[:LANES] = first_ref[...].reshape(model, LANES).T
    q_ref[LANES:] = rest_ref[...].reshape(model, LANES).T[:HALF]


def weights(pieces, count, rows, q_width, kv_width):
    blocks = (count, count, 2, rows)
    model = count * count * 2 * rows
    q_turned, kv = run(
        weights_kernel,
        [VMEM] * len(pieces),
        pieces,
        [near((q_width, model), BF16), near((*blocks, kv_width), BF16)],
        [pltpu.VMEM((*blocks, LANES), BF16), pltpu.VMEM((*blocks, LANES), BF16)],
    )
    return q_turned, kv.reshape(model, kv_width)


NT = (((1,), (1,)), ((), ()))


def steps_kernel(
    dir_ref, factor_ref, own_ref, mine_ref, other_ref,
    q_ref, kv_ref, own_out, qm_out, km_out, qs_out, ks_out, qm_buf, km_buf, qs_buf, ks_buf, sems,
):
    half, q_width = qm_buf.shape
    rows = 2 * half
    at = pl.ds(pl.multiple_of(lax.axis_index("core") * half, half), half)
    value = mine_ref[at, :] + other_ref[at, :]
    first, second = update(value, mine_ref[rows : rows + half], mine_ref[rows + half :])
    qm_buf[...] = first[:, :q_width]
    km_buf[...] = first[:, q_width:]
    qs_buf[...] = second[:, :q_width]
    ks_buf[...] = second[:, q_width:]
    saved = [
        pltpu.make_async_copy(a, b, sems.at[i])
        for i, (a, b) in enumerate(
            ((qm_buf, qm_out), (km_buf, km_out), (qs_buf, qs_out), (ks_buf, ks_out))
        )
    ]
    for copy in saved:
        copy.start()
    directions = dir_ref[...]
    factor = factor_ref[...]
    turned = directions[:, :q_width].T
    q_ref[...] = lax.dot_general(turned, factor, NT, preferred_element_type=F32)
    kv_ref[...] = jnp.dot(factor, directions[:, q_width:], preferred_element_type=F32)
    own_out[...] = jnp.dot(own_ref[...], directions, preferred_element_type=F32)
    for copy in saved:
        copy.wait()


def unscaled_steps(directions, factor, own, mine, other, kept):
    model, width = factor.shape[0], directions.shape[1]
    q_width = kept[0].shape[1]
    return run(
        steps_kernel,
        [VMEM] * 5,
        (directions, factor, own, mine, other),
        [near((q_width, model)), near((model, width - q_width)), near((own.shape[0], width))]
        + [far(k.shape) for k in kept],
        [pltpu.VMEM(k.shape, F32) for k in kept] + [pltpu.SemaphoreType.DMA((len(kept),))],
        2 * width * directions.shape[0] * model,
        outs=[VMEM] * 3 + [HBM] * 4,
    )


PARTS = 2


def finish_kernel(q_count, kv_count):
    def kernel(
        squares_0, squares_1, squares_2, squares_3, q_step_ref, kv_step_ref, own_ref, q_whole_ref,
        kv_whole_ref, q_ref, kv_ref, q_new, kv_new, q_step, kv_step, q_copy, kv_copy,
        q_new_buf, kv_new_buf, q_step_buf, kv_step_buf, q_buf, kv_buf, sems,
    ):
        copies = []

        def save(source, target):
            copy = pltpu.make_async_copy(source, target, sems.at[len(copies)])
            copy.start()
            copies.append(copy)

        q_width, model = q_buf.shape
        piece = model // PARTS
        sums = squares_0[...] + squares_1[...] + squares_2[...] + squares_3[...]
        q_scale = 0.5 * jnp.sqrt(F32(q_count)) * lax.rsqrt(sums[0:1, 0:1] + 1e-06)
        kv_scale = 0.5 * jnp.sqrt(F32(kv_count)) * lax.rsqrt(sums[1:2, 0:1] + 1e-06)
        own = own_ref[...]
        step = q_scale * own[:, :q_width]
        q_step_buf[...] = step
        q_new_buf[...] = q_ref[...] - step
        step = kv_scale * own[:, q_width:]
        kv_step_buf[...] = step
        kv_new_buf[...] = kv_ref[...] - step
        save(q_step_buf, q_step)
        save(q_new_buf, q_new)
        save(kv_step_buf, kv_step)
        save(kv_new_buf, kv_new)
        for p in range(PARTS):
            at = slice(p * piece, (p + 1) * piece)
            q_buf[:, at] = (q_whole_ref[:, at].astype(F32) - q_scale * q_step_ref[:, at]).astype(BF16)
            save(q_buf.at[:, at], q_copy.at[:, at])
        for p in range(PARTS):
            at = slice(p * piece, (p + 1) * piece)
            kv_buf[at] = (kv_whole_ref[at].astype(F32) - kv_scale * kv_step_ref[at]).astype(BF16)
            save(kv_buf.at[at], kv_copy.at[at])
        for copy in copies:
            copy.wait()

    return kernel


def finish(squares, q_steps, kv_steps, own, q_whole, kv_whole, q_own, kv_own, q_count, kv_count):
    made = [
        (q_own.shape, F32),
        (kv_own.shape, F32),
        (q_own.shape, F32),
        (kv_own.shape, F32),
        (q_whole.shape, BF16),
        (kv_whole.shape, BF16),
    ]
    return run(
        finish_kernel(q_count, kv_count),
        [VMEM] * 11,
        (*squares, q_steps, kv_steps, own, q_whole, kv_whole, q_own, kv_own),
        [far(*m) for m in made],
        [pltpu.VMEM(*m) for m in made] + [pltpu.SemaphoreType.DMA((4 + 2 * PARTS,))],
        outs=[HBM] * 6,
    )


def body(x, q_cot, kv_cot, row_factor, q_weight, kv_weight, qm, km, qs, ks):
    fs_count = lax.axis_size(FS)
    q_width, kv_width = q_cot.shape[1], kv_cot.shape[1]
    width, rank_rows = q_width + kv_width, qm.shape[0]
    chips = lax.axis_size(ZY)
    mine = exchange(spread(row_factor, chips), ZY)
    grad, weight_rows, moments = gradients(
        q_cot.T, kv_cot, x, (q_weight, kv_weight, qm, km, qs, ks)
    )
    mine, grad, weight_rows, moments = lax.optimization_barrier((mine, grad, weight_rows, moments))
    weight_more = swapped(weight_rows, "core", 1)
    other = swapped(mine, "core", 1)
    weight_across = shifted(weight_rows, "y", lax.axis_size("y") // 2)
    weight_both = stacked((weight_rows, weight_more))
    weight_beside = turned(weight_both, "y")
    partial, factor = project(mine, other, grad)
    parts = exchange(partial.reshape(chips, 2 * rank_rows, width), ZY)
    weight_part = stacked((weight_rows, weight_beside, weight_across))
    weight_row = stacked((weight_part, swapped(weight_part, "core", 1)))
    weight_near = turned(weight_row, "z")
    sums = pair_sums(parts, moments)
    more = swapped(sums, "core", 1)
    to_send = direction_tiles(sums, more, chips)
    directions = exchange(to_send, ZY).reshape(fs_count * rank_rows, width)
    weight_over = swapped(weight_near, "core", 1)
    weight_far = shifted(weight_part, "z", lax.axis_size("z") // 2)
    weight_last = swapped(weight_far, "core", 1)
    q_whole, kv_whole = weights(
        (weight_row, weight_near, weight_over, weight_far, weight_last),
        lax.axis_size("z"), q_weight.shape[0], q_width, kv_width,
    )
    squares = stats(directions, q_width)
    squares = [squares] + [shifted(squares, "tp", k) for k in (2, 1, 3)]
    q_steps, kv_steps, own, *kept = unscaled_steps(
        directions, factor, row_factor, sums, more, (qm, km, qs, ks)
    )
    count = rank_rows * fs_count * lax.axis_size("tp")
    q_new, kv_new, q_step, kv_step, q_copy, kv_copy = finish(
        squares, q_steps, kv_steps, own, q_whole, kv_whole, q_weight, kv_weight,
        count * q_width, count * kv_width,
    )
    return (q_new, kv_new, q_step, kv_step, q_copy.T, kv_copy, *kept)


def solution(mesh):
    split = Mesh(mesh.devices.reshape(4, 4, 2, mesh.shape["tp"]), ("z", "y", "core", "tp"))
    rows, tiles = P(FS, None), P(FS, "tp")
    return jax.shard_map(
        body,
        mesh=split,
        in_specs=(rows, tiles, tiles, rows, tiles, tiles, tiles, tiles, tiles, tiles),
        out_specs=(tiles, tiles, tiles, tiles, P(None, "tp"), P(None, "tp"), tiles, tiles, tiles, tiles),
        check_vma=False,
    )
```

time: 69.8 us -> 72 us (1.032)
  the two profiles are of different devices: /device:TPU:6 before, /device:TPU:1 now
where the time goes in v3:
time: 72 us; the launch traced here: 70.6 us
  starting transfers between devices  35.3 us (49%)
  Pallas kernels  16.9 us (23%)
  waiting for transfers between devices  16.9 us (23%)
  between operations  0.81 us (1%)
    pallas_call x12, Pallas kernels, run(): pl.pallas_call(kernel, in_specs=list(specs), out_specs=outs or [VMEM] * l...  16.9 us
    all_to_all x3, starting transfers between devices, exchange(): return lax.all_to_all(tiles, axis, split_axis=0, concat_axis=0, tiled=True)  16.3 us
    all_to_all x3, waiting for transfers between devices, exchange(): return lax.all_to_all(tiles, axis, split_axis=0, concat_axis=0, tiled=True)  11.1 us
    ppermute x6, starting transfers between devices, swapped(): return lax.ppermute(array, axis, [(i, i ^ bit) for i in range(count)])  8.74 us
    ppermute x5, starting transfers between devices, shifted(): lax.ppermute(array, axis, [(i, (i + k) % count) for i in range(count)])  8.66 us
    ppermute x5, waiting for transfers between devices, shifted(): lax.ppermute(array, axis, [(i, (i + k) % count) for i in range(count)])  2.9 us
    ppermute x6, waiting for transfers between devices, swapped(): return lax.ppermute(array, axis, [(i, i ^ bit) for i in range(count)])  2.78 us
    ppermute x2, starting transfers between devices, turned(): return lax.ppermute(array, FS, pairs)  1.54 us
  transfers between devices with their start and end apart: 16, of which 8 were waited for; matrix products, arithmetic and copies ran while one was open for 0% of the time, Pallas kernels for 20%

profile of v3, /device:TPU:1, one launch (start us, length us, event | category | flops | bytes accessed | tf_op | source)
XLA Modules:
  0.0 70.6 jit_solution(6424621280346975043)
XLA Ops:
  0.6 1.7 %shard_map.177 = bf16[16,64,256]{2,1,0:T(8,128)(2,1)} custom-call(bf16[64,256]{1,0:T(8,128)(2,1)} %own_ref.1), custom_call_target="tpu_custom_call" | custom-call | tf_op jit(solution)/shard_map/pallas_call | solution.py:32
  2.3 8.6 %all-to-all-start = ((bf16[16,64,256]{2,1,0:T(8,128)(2,1)}), bf16[16,64,256]{2,1,0:T(8,128)(2,1)S(1)}, u32[]{:S(2)}, u32[]{:S(2)}) async-start(bf16[16,64,256]{2,1,0:T(8,128)(2,1)} %shard_map.177), calls=%async_computation | async-start | bytes 1048576 | tf_op jit(solution)/shard_map/all_to_all | solution.py:44
  10.9 9.3 %shard_map.178 = (bf16[320,2048]{1,0:T(8,128)(2,1)S(1)}, bf16[1,80,256]{2,1,0:T(8,128)(2,1)S(1)}, f32[2,8,320]{2,1,0:T(8,128)S(1)}) custom-call(bf16[192,4608]{1,0:T(8,128)(2,1)} %bitcast.11, bf16[4608,128]{1,0:T(8,128)(2,1)} %kv_ref.2, bf16[4608,2048]{1,0:T(8,128)(2,1)} %x_ref.1, f32[64,192]{1,0:T(8,128)} %q_ref.1, f32[64,128]{1,0:T(8,128)} %kv_ref.3, ...), custom_call_target="tpu_custom_call" | custom-call | flops 6039797760 | tf_op jit(solution)/shard_map/pallas_call | solution.py:32
  20.2 1.2 %all-to-all-done.mine_ref = bf16[16,64,256]{2,1,0:T(8,128)(2,1)S(1)} async-done(((bf16[16,64,256]{2,1,0:T(8,128)(2,1)}), bf16[16,64,256]{2,1,0:T(8,128)(2,1)S(1)}, u32[]{:S(2)}, u32[]{:S(2)}) %all-to-all-start) | async-done | bytes 524320 | tf_op jit(solution)/shard_map/all_to_all | solution.py:44
  21.4 2.1 %collective-permute-start.5 = (bf16[1,80,256]{2,1,0:T(8,128)(2,1)S(1)}, bf16[1,80,256]{2,1,0:T(8,128)(2,1)S(1)}, u32[]{:S(2)}, u32[]{:S(2)}) collective-permute-start(bf16[1,80,256]{2,1,0:T(8,128)(2,1)S(1)} %get-tuple-element.45.refs_0_), channel_id=1, source_target_pairs={{0,4},{4,0},{1,5},{5,1},{2,6},{6,2},{3,7},{7,3},{8,12},{12,8},{9,1... | collective-permute-start | bytes 122888 | tf_op jit(solution)/shard_map/ppermute | solution.py:49
  23.4 0.0 collective-permute-start
  23.4 0.9 %collective-permute-done.5.refs_1_ = bf16[1,80,256]{2,1,0:T(8,128)(2,1)S(1)} collective-permute-done((bf16[1,80,256]{2,1,0:T(8,128)(2,1)S(1)}, bf16[1,80,256]{2,1,0:T(8,128)(2,1)S(1)}, u32[]{:S(2)}, u32[]{:S(2)}) %collective-permute-start.5) | collective-permute-done | bytes 40992 | tf_op jit(solution)/shard_map/ppermute | solution.py:49
  24.3 0.3 collective-permute-start.6
  24.6 1.6 %collective-permute-start.7 = (bf16[1,80,256]{2,1,0:T(8,128)(2,1)S(1)}, bf16[1,80,256]{2,1,0:T(8,128)(2,1)S(1)}, u32[]{:S(2)}, u32[]{:S(2)}) collective-permute-start(bf16[1,80,256]{2,1,0:T(8,128)(2,1)S(1)} %get-tuple-element.45.refs_0_), channel_id=1, source_target_pairs={{0,16},{8,24},{16,0},{24,8},{1,17},{9,25},{17,1},{25,9},{2,18},{10... | collective-permute-start | bytes 122888 | tf_op jit(solution)/shard_map/ppermute | solution.py:54
  26.2 2.9 %collective-permute-done.7.refs_2_ = bf16[1,80,256]{2,1,0:T(8,128)(2,1)S(1)} collective-permute-done((bf16[1,80,256]{2,1,0:T(8,128)(2,1)S(1)}, bf16[1,80,256]{2,1,0:T(8,128)(2,1)S(1)}, u32[]{:S(2)}, u32[]{:S(2)}) %collective-permute-start.7) | collective-permute-done | bytes 40992 | tf_op jit(solution)/shard_map/ppermute | solution.py:54
  29.0 0.2 collective-permute-done.6.refs_1_
  29.3 1.9 %collective-permute-start.8 = (bf16[4,80,256]{2,1,0:T(8,128)(2,1)S(1)}, bf16[4,80,256]{2,1,0:T(8,128)(2,1)S(1)}, u32[]{:S(2)}, u32[]{:S(2)}) collective-permute-start(bf16[4,80,256]{2,1,0:T(8,128)(2,1)S(1)} %shard_map.185.refs_0_), channel_id=1, source_target_pairs={{0,4},{4,0},{1,5},{5,1},{2,6},{6,2},{3,7},{7,3},{8,12},{12,8},{9,1... | collective-permute-start | bytes 491528 | tf_op jit(solution)/shard_map/ppermute | solution.py:49
  31.2 1.0 %collective-permute-done.8.refs_1_ = bf16[4,80,256]{2,1,0:T(8,128)(2,1)S(1)} collective-permute-done((bf16[4,80,256]{2,1,0:T(8,128)(2,1)S(1)}, bf16[4,80,256]{2,1,0:T(8,128)(2,1)S(1)}, u32[]{:S(2)}, u32[]{:S(2)}) %collective-permute-start.8) | collective-permute-done | bytes 163872 | tf_op jit(solution)/shard_map/ppermute | solution.py:49
  32.3 0.0 copy-start.1
  32.3 1.3 %collective-permute-start.9 = (bf16[8,80,256]{2,1,0:T(8,128)(2,1)S(1)}, bf16[8,80,256]{2,1,0:T(8,128)(2,1)}, u32[]{:S(2)}, u32[]{:S(2)}) collective-permute-start(bf16[8,80,256]{2,1,0:T(8,128)(2,1)S(1)} %shard_map.186.here_ref), channel_id=1, source_target_pairs={{0,96},{4,36},{8,104},{12,44},{16,112},{20,52},{24,120},{28,60},{3... | collective-permute-start | bytes 983048 | tf_op jit(solution)/shard_map/ppermute | solution.py:69
  33.5 0.0 collective-permute-done.other_ref
  33.5 0.7 shard_map.179
  34.2 0.0 copy-start
  34.2 0.7 copy-done
  34.9 4.1 %all-to-all-start.1 = ((bf16[16,16,320]{2,1,0:T(8,128)(2,1)}), bf16[16,16,320]{2,1,0:T(8,128)(2,1)S(1)}, u32[]{:S(2)}, u32[]{:S(2)}) async-start(bf16[16,16,320]{2,1,0:T(8,128)(2,1)} %bitcast.10), calls=%async_computation.1 | async-start | bytes 393216 | tf_op jit(solution)/shard_map/all_to_all | solution.py:44
  39.0 2.9 %collective-permute-start.11 = (bf16[4,80,256]{2,1,0:T(8,128)(2,1)S(1)}, bf16[4,80,256]{2,1,0:T(8,128)(2,1)S(1)}, u32[]{:S(2)}, u32[]{:S(2)}) collective-permute-start(bf16[4,80,256]{2,1,0:T(8,128)(2,1)S(1)} %shard_map.185.refs_0_), channel_id=1, source_target_pairs={{0,64},{32,96},{64,0},{96,32},{1,65},{33,97},{65,1},{97,33},{2,66}... | collective-permute-start | bytes 491528 | tf_op jit(solution)/shard_map/ppermute | solution.py:54
  41.8 0.0 collective-permute-done.9.near_ref
  41.8 1.8 %collective-permute-start.10 = (bf16[8,80,256]{2,1,0:T(8,128)(2,1)}, bf16[8,80,256]{2,1,0:T(8,128)(2,1)S(1)}, u32[]{:S(2)}, u32[]{:S(2)}) collective-permute-start(bf16[8,80,256]{2,1,0:T(8,128)(2,1)} %collective-permute-done.9.near_ref), channel_id=1, source_target_pairs={{0,4},{4,0},{1,5},{5,1},{2,6},{6,2},{3,7},{7,3},{8,12},{12,8},{9,1... | collective-permute-start | bytes 983048 | tf_op jit(solution)/shard_map/ppermute | solution.py:49
  43.6 2.6 %all-to-all-done.1.parts_ref = bf16[16,16,320]{2,1,0:T(8,128)(2,1)S(1)} async-done(((bf16[16,16,320]{2,1,0:T(8,128)(2,1)}), bf16[16,16,320]{2,1,0:T(8,128)(2,1)S(1)}, u32[]{:S(2)}, u32[]{:S(2)}) %all-to-all-start.1) | async-done | bytes 163872 | tf_op jit(solution)/shard_map/all_to_all | solution.py:44
  46.3 2.5 %collective-permute-start.1 = (f32[32,320]{1,0:T(8,128)S(1)}, f32[32,320]{1,0:T(8,128)S(1)}, u32[]{:S(2)}, u32[]{:S(2)}) collective-permute-start(f32[32,320]{1,0:T(8,128)S(1)} %shard_map.180.mine_ref), channel_id=1, source_target_pairs={{0,4},{4,0},{1,5},{5,1},{2,6},{6,2},{3,7},{7,3},{8,12},{12,8},{9,1... | collective-permute-start | bytes 122888 | tf_op jit(solution)/shard_map/ppermute | solution.py:49
  48.8 0.9 %collective-permute-done.1.other_ref = f32[32,320]{1,0:T(8,128)S(1)} collective-permute-done((f32[32,320]{1,0:T(8,128)S(1)}, f32[32,320]{1,0:T(8,128)S(1)}, u32[]{:S(2)}, u32[]{:S(2)}) %collective-permute-start.1) | collective-permute-done | bytes 40992 | tf_op jit(solution)/shard_map/ppermute | solution.py:49
  49.7 0.7 %shard_map.181 = bf16[16,16,320]{2,1,0:T(8,128)(2,1)} custom-call(f32[32,320]{1,0:T(8,128)S(1)} %shard_map.180.mine_ref, f32[32,320]{1,0:T(8,128)S(1)} %collective-permute-done.1.other_ref), custom_call_target="tpu_custom_call" | custom-call | tf_op jit(solution)/shard_map/pallas_call | solution.py:32
  50.4 0.0 copy-start.2
  50.4 0.0 copy-start.3
  50.4 3.7 %all-to-all-start.2 = ((bf16[16,16,320]{2,1,0:T(8,128)(2,1)}), bf16[16,16,320]{2,1,0:T(8,128)(2,1)S(1)}, u32[]{:S(2)}, u32[]{:S(2)}) async-start(bf16[16,16,320]{2,1,0:T(8,128)(2,1)} %shard_map.181), calls=%async_computation.2 | async-start | bytes 393216 | tf_op jit(solution)/shard_map/all_to_all | solution.py:44
  54.1 0.0 collective-permute-done.11.far_ref
  54.1 0.4 collective-permute-start.12
  54.5 7.2 %all-to-all-done.2 = bf16[16,16,320]{2,1,0:T(8,128)(2,1)S(1)} async-done(((bf16[16,16,320]{2,1,0:T(8,128)(2,1)}), bf16[16,16,320]{2,1,0:T(8,128)(2,1)S(1)}, u32[]{:S(2)}, u32[]{:S(2)}) %all-to-all-start.2) | async-done | bytes 163872 | tf_op jit(solution)/shard_map/all_to_all | solution.py:44
  61.8 0.2 shard_map.182.squares_0
  62.0 2.5 %collective-permute-start.4 = (f32[8,128]{1,0:T(8,128)S(1)}, f32[8,128]{1,0:T(8,128)S(1)}, u32[]{:S(2)}, u32[]{:S(2)}) collective-permute-start(f32[8,128]{1,0:T(8,128)S(1)} %shard_map.182.squares_0), channel_id=1, source_target_pairs={{0,3},{1,0},{2,1},{3,2},{4,7},{5,4},{6,5},{7,6},{8,11},{9,8},{10,9... | collective-permute-start | bytes 12296 | tf_op jit(solution)/shard_map/ppermute | solution.py:54
  64.5 0.0 collective-permute-start.3
  64.5 1.7 %collective-permute-start.2 = (f32[8,128]{1,0:T(8,128)S(1)}, f32[8,128]{1,0:T(8,128)S(1)}, u32[]{:S(2)}, u32[]{:S(2)}) collective-permute-start(f32[8,128]{1,0:T(8,128)S(1)} %shard_map.182.squares_0), channel_id=1, source_target_pairs={{0,2},{1,3},{2,0},{3,1},{4,6},{5,7},{6,4},{7,5},{8,10},{9,11},{10,... | collective-permute-start | bytes 12296 | tf_op jit(solution)/shard_map/ppermute | solution.py:54
  66.2 0.0 copy-done.1
  66.2 1.4 %shard_map.183 = (f32[192,2048]{1,0:T(8,128)S(1)}, f32[2048,128]{1,0:T(8,128)S(1)}, f32[64,320]{1,0:T(8,128)S(1)}, f32[8,192]{1,0:T(8,128)}, f32[8,128]{1,0:T(8,...) custom-call(bf16[256,320]{1,0:T(8,128)(2,1)S(1)} %bitcast.7, bf16[2048,256]{1,0:T(8,128)(2,1)S(1)} %bitcast.8, ...), custom_call_target="tpu_custom_call" | custom-call | flops 335544320 | tf_op jit(solution)/shard_map/pallas_call | solution.py:32
  67.6 0.0 collective-permute-done.12.last_ref
  67.6 0.0 collective-permute-done.10.over_ref
  67.6 1.6 %shard_map.187 = (bf16[192,2048]{1,0:T(8,128)(2,1)S(1)}, bf16[4,4,2,64,128]{4,3,2,1,0:T(8,128)(2,1)S(1)}) custom-call(bf16[8,80,256]{2,1,0:T(8,128)(2,1)S(1)} %shard_map.186.here_ref, bf16[8,80,256]{2,1,0:T(8,128)(2,1)} %collective-permute-done.9.near_ref, bf16[8,80,256]{2,1,0:T(8,128)(2,1)S(1)} %collective-permute-done.10.over_ref, ...), custom_call_target="tpu_custom_call" | custom-call | tf_op jit(solution)/shard_map/pallas_call | solution.py:32
  69.1 0.0 collective-permute-done.4.squares_3
  69.2 0.0 collective-permute-done.3.squares_2
  69.2 0.0 collective-permute-done.2.squares_1
  69.2 0.0 copy-done.2
  69.2 0.0 copy-done.3
  69.2 1.4 %shard_map.188 = (f32[64,192]{1,0:T(8,128)}, f32[64,128]{1,0:T(8,128)}, f32[64,192]{1,0:T(8,128)}, f32[64,128]{1,0:T(8,128)}, bf16[192,2048]{1,0:T(8,128)(2,1)}, /*index=5*/bf16[2048,128]{1,0:T(8,128)(2,1)}) custom-call(f32[8,128]{1,0:T(8,128)S(1)} %shard_map.182.squares_0, f32[8,128]{1,0:T(8,128)S(1)} %collective-permute-done.2.squares_1, ...), custom_call_target="tpu_custom_call" | custom-call | tf_op jit(solution)/shard_map/pallas_call | solution.py:32
  (4 shorter events, 0.1 us)
Async XLA Ops:
  2.3 19.0 %all-to-all-start = ((bf16[16,64,256]{2,1,0:T(8,128)(2,1)}), bf16[16,64,256]{2,1,0:T(8,128)(2,1)S(1)}, u32[]{:S(2)}, u32[]{:S(2)}) async-start(bf16[16,64,256]{2,1,0:T(8,128)(2,1)} %shard_map.177), calls=%async_computation | async-start | bytes 1048576 | tf_op jit(solution)/shard_map/all_to_all | solution.py:44
  21.4 2.9 %collective-permute-start.5 = (bf16[1,80,256]{2,1,0:T(8,128)(2,1)S(1)}, bf16[1,80,256]{2,1,0:T(8,128)(2,1)S(1)}, u32[]{:S(2)}, u32[]{:S(2)}) collective-permute-start(bf16[1,80,256]{2,1,0:T(8,128)(2,1)S(1)} %get-tuple-element.45.refs_0_), channel_id=1, source_target_pairs={{0,4},{4,0},{1,5},{5,1},{2,6},{6,2},{3,7},{7,3},{8,12},{12,8},{9,1... | collective-permute-start | bytes 122888 | tf_op jit(solution)/shard_map/ppermute | solution.py:49
  23.4 10.1 %collective-permute-start = (bf16[16,64,256]{2,1,0:T(8,128)(2,1)S(1)}, bf16[16,64,256]{2,1,0:T(8,128)(2,1)S(1)}, u32[]{:S(2)}, u32[]{:S(2)}) collective-permute-start(bf16[16,64,256]{2,1,0:T(8,128)(2,1)S(1)} %all-to-all-done.mine_ref), channel_id=1, source_target_pairs={{0,4},{4,0},{1,5},{5,1},{2,6},{6,2},{3,7},{7,3},{8,12},{12,8},{9,1... | collective-permute-start | bytes 1572872 | tf_op jit(solution)/shard_map/ppermute | solution.py:49
  24.3 4.9 %collective-permute-start.6 = (bf16[2,80,256]{2,1,0:T(8,128)(2,1)S(1)}, bf16[2,80,256]{2,1,0:T(8,128)(2,1)S(1)}, u32[]{:S(2)}, u32[]{:S(2)}) collective-permute-start(bf16[2,80,256]{2,1,0:T(8,128)(2,1)S(1)} %shard_map.184), channel_id=1, source_target_pairs={{0,24},{4,12},{8,0},{12,20},{16,8},{20,28},{24,16},{28,4},{32,56},... | collective-permute-start | bytes 245768 | tf_op jit(solution)/shard_map/ppermute | solution.py:69
  24.6 4.5 %collective-permute-start.7 = (bf16[1,80,256]{2,1,0:T(8,128)(2,1)S(1)}, bf16[1,80,256]{2,1,0:T(8,128)(2,1)S(1)}, u32[]{:S(2)}, u32[]{:S(2)}) collective-permute-start(bf16[1,80,256]{2,1,0:T(8,128)(2,1)S(1)} %get-tuple-element.45.refs_0_), channel_id=1, source_target_pairs={{0,16},{8,24},{16,0},{24,8},{1,17},{9,25},{17,1},{25,9},{2,18},{10... | collective-permute-start | bytes 122888 | tf_op jit(solution)/shard_map/ppermute | solution.py:54
  29.3 3.0 %collective-permute-start.8 = (bf16[4,80,256]{2,1,0:T(8,128)(2,1)S(1)}, bf16[4,80,256]{2,1,0:T(8,128)(2,1)S(1)}, u32[]{:S(2)}, u32[]{:S(2)}) collective-permute-start(bf16[4,80,256]{2,1,0:T(8,128)(2,1)S(1)} %shard_map.185.refs_0_), channel_id=1, source_target_pairs={{0,4},{4,0},{1,5},{5,1},{2,6},{6,2},{3,7},{7,3},{8,12},{12,8},{9,1... | collective-permute-start | bytes 491528 | tf_op jit(solution)/shard_map/ppermute | solution.py:49
  32.3 33.9 %copy-start.1 = (bf16[64,256]{1,0:T(8,128)(2,1)S(1)}, bf16[64,256]{1,0:T(8,128)(2,1)}, u32[]{:S(2)}) copy-start(bf16[64,256]{1,0:T(8,128)(2,1)} %own_ref.1) | copy-start | bytes 98308
  32.3 9.6 %collective-permute-start.9 = (bf16[8,80,256]{2,1,0:T(8,128)(2,1)S(1)}, bf16[8,80,256]{2,1,0:T(8,128)(2,1)}, u32[]{:S(2)}, u32[]{:S(2)}) collective-permute-start(bf16[8,80,256]{2,1,0:T(8,128)(2,1)S(1)} %shard_map.186.here_ref), channel_id=1, source_target_pairs={{0,96},{4,36},{8,104},{12,44},{16,112},{20,52},{24,120},{28,60},{3... | collective-permute-start | bytes 983048 | tf_op jit(solution)/shard_map/ppermute | solution.py:69
  34.2 0.7 copy-start
  34.9 11.4 %all-to-all-start.1 = ((bf16[16,16,320]{2,1,0:T(8,128)(2,1)}), bf16[16,16,320]{2,1,0:T(8,128)(2,1)S(1)}, u32[]{:S(2)}, u32[]{:S(2)}) async-start(bf16[16,16,320]{2,1,0:T(8,128)(2,1)} %bitcast.10), calls=%async_computation.1 | async-start | bytes 393216 | tf_op jit(solution)/shard_map/all_to_all | solution.py:44
  39.0 15.1 %collective-permute-start.11 = (bf16[4,80,256]{2,1,0:T(8,128)(2,1)S(1)}, bf16[4,80,256]{2,1,0:T(8,128)(2,1)S(1)}, u32[]{:S(2)}, u32[]{:S(2)}) collective-permute-start(bf16[4,80,256]{2,1,0:T(8,128)(2,1)S(1)} %shard_map.185.refs_0_), channel_id=1, source_target_pairs={{0,64},{32,96},{64,0},{96,32},{1,65},{33,97},{65,1},{97,33},{2,66}... | collective-permute-start | bytes 491528 | tf_op jit(solution)/shard_map/ppermute | solution.py:54
  41.8 25.7 %collective-permute-start.10 = (bf16[8,80,256]{2,1,0:T(8,128)(2,1)}, bf16[8,80,256]{2,1,0:T(8,128)(2,1)S(1)}, u32[]{:S(2)}, u32[]{:S(2)}) collective-permute-start(bf16[8,80,256]{2,1,0:T(8,128)(2,1)} %collective-permute-done.9.near_ref), channel_id=1, source_target_pairs={{0,4},{4,0},{1,5},{5,1},{2,6},{6,2},{3,7},{7,3},{8,12},{12,8},{9,1... | collective-permute-start | bytes 983048 | tf_op jit(solution)/shard_map/ppermute | solution.py:49
  46.3 3.4 %collective-permute-start.1 = (f32[32,320]{1,0:T(8,128)S(1)}, f32[32,320]{1,0:T(8,128)S(1)}, u32[]{:S(2)}, u32[]{:S(2)}) collective-permute-start(f32[32,320]{1,0:T(8,128)S(1)} %shard_map.180.mine_ref), channel_id=1, source_target_pairs={{0,4},{4,0},{1,5},{5,1},{2,6},{6,2},{3,7},{7,3},{8,12},{12,8},{9,1... | collective-permute-start | bytes 122888 | tf_op jit(solution)/shard_map/ppermute | solution.py:49
  50.4 18.8 %copy-start.2 = (f32[64,192]{1,0:T(8,128)S(1)}, f32[64,192]{1,0:T(8,128)}, u32[]{:S(2)}) copy-start(f32[64,192]{1,0:T(8,128)} %q_ref.1) | copy-start | bytes 147460
  50.4 18.8 %copy-start.3 = (f32[64,128]{1,0:T(8,128)S(1)}, f32[64,128]{1,0:T(8,128)}, u32[]{:S(2)}) copy-start(f32[64,128]{1,0:T(8,128)} %kv_ref.3) | copy-start | bytes 98308
  50.4 11.4 %all-to-all-start.2 = ((bf16[16,16,320]{2,1,0:T(8,128)(2,1)}), bf16[16,16,320]{2,1,0:T(8,128)(2,1)S(1)}, u32[]{:S(2)}, u32[]{:S(2)}) async-start(bf16[16,16,320]{2,1,0:T(8,128)(2,1)} %shard_map.181), calls=%async_computation.2 | async-start | bytes 393216 | tf_op jit(solution)/shard_map/all_to_all | solution.py:44
  54.1 13.4 %collective-permute-start.12 = (bf16[4,80,256]{2,1,0:T(8,128)(2,1)S(1)}, bf16[4,80,256]{2,1,0:T(8,128)(2,1)S(1)}, u32[]{:S(2)}, u32[]{:S(2)}) collective-permute-start(bf16[4,80,256]{2,1,0:T(8,128)(2,1)S(1)} %collective-permute-done.11.far_ref), channel_id=1, source_target_pairs={{0,4},{4,0},{1,5},{5,1},{2,6},{6,2},{3,7},{7,3},{8,12},{12,8},{9,1... | collective-permute-start | bytes 491528 | tf_op jit(solution)/shard_map/ppermute | solution.py:49
  62.0 7.2 %collective-permute-start.4 = (f32[8,128]{1,0:T(8,128)S(1)}, f32[8,128]{1,0:T(8,128)S(1)}, u32[]{:S(2)}, u32[]{:S(2)}) collective-permute-start(f32[8,128]{1,0:T(8,128)S(1)} %shard_map.182.squares_0), channel_id=1, source_target_pairs={{0,3},{1,0},{2,1},{3,2},{4,7},{5,4},{6,5},{7,6},{8,11},{9,8},{10,9... | collective-permute-start | bytes 12296 | tf_op jit(solution)/shard_map/ppermute | solution.py:54
  64.5 4.7 %collective-permute-start.3 = (f32[8,128]{1,0:T(8,128)S(1)}, f32[8,128]{1,0:T(8,128)S(1)}, u32[]{:S(2)}, u32[]{:S(2)}) collective-permute-start(f32[8,128]{1,0:T(8,128)S(1)} %shard_map.182.squares_0), channel_id=1, source_target_pairs={{0,1},{1,2},{2,3},{3,0},{4,5},{5,6},{6,7},{7,4},{8,9},{9,10},{10,1... | collective-permute-start | bytes 12296 | tf_op jit(solution)/shard_map/ppermute | solution.py:54
  64.5 4.7 %collective-permute-start.2 = (f32[8,128]{1,0:T(8,128)S(1)}, f32[8,128]{1,0:T(8,128)S(1)}, u32[]{:S(2)}, u32[]{:S(2)}) collective-permute-start(f32[8,128]{1,0:T(8,128)S(1)} %shard_map.182.squares_0), channel_id=1, source_target_pairs={{0,2},{1,3},{2,0},{3,1},{4,6},{5,7},{6,4},{7,5},{8,10},{9,11},{10,... | collective-permute-start | bytes 12296 | tf_op jit(solution)/shard_map/ppermute | solution.py:54

commit v4 on v3

--- a/solution.py
+++ b/solution.py
@@ -69,41 +69,65 @@
     return lax.ppermute(array, FS, pairs)
 
 
-LANES = 128
-HALF = LANES // 2
-
-
-def spread_kernel(factor_ref, out_ref, buf_ref, sems):
-    count = out_ref.shape[0]
-    arrival = pltpu.make_async_copy(factor_ref, buf_ref, sems.at[count])
-    arrival.start()
-    arrival.wait()
-    copies = [pltpu.make_async_copy(buf_ref, out_ref.at[i], sems.at[i]) for i in range(count)]
+def fetch(pairs, sems):
+    copies = [pltpu.make_async_copy(a, b, sems.at[i]) for i, (a, b) in enumerate(pairs)]
     for copy in copies:
         copy.start()
     for copy in copies:
         copy.wait()
 
 
-def spread(factor, count):
-    return run(
-        spread_kernel,
-        [HBM],
-        (factor,),
-        [far((count, *factor.shape), BF16)],
-        [pltpu.VMEM(factor.shape, BF16), pltpu.SemaphoreType.DMA((count + 1,))],
-        outs=[HBM],
-    )[0]
-
-
-def fold(q_ref, kv_ref, out_ref):
+LANES = 128
+HALF = LANES // 2
+
+
+def spread_kernel(
+    factor_ref, q_ref, kv_ref, qm_ref, km_ref, qs_ref, ks_ref, factor_out, rows_out, moments_out,
+    factor_buf, q_buf, kv_buf, qm_buf, km_buf, qs_buf, ks_buf, sems,
+):
+    fetch(
+        (
+            (factor_ref, factor_buf),
+            (q_ref, q_buf),
+            (kv_ref, kv_buf),
+            (qm_ref, qm_buf),
+            (km_ref, km_buf),
+            (qs_ref, qs_buf),
+            (ks_ref, ks_buf),
+        ),
+        sems,
+    )
+    factor = factor_buf[...]
+    for i in range(factor_out.shape[0]):
+        factor_out[i] = factor
+    q_width = q_ref.shape[1]
+    moments_out[0, :, :q_width] = qm_buf[...]
+    moments_out[0, :, q_width:] = km_buf[...]
+    moments_out[1, :, :q_width] = qs_buf[...]
+    moments_out[1, :, q_width:] = ks_buf[...]
     rows = q_ref.shape[0]
     quarter = rows // 4
-    q = q_ref[...].astype(BF16)
-    out_ref[0, :rows, :LANES] = q[:, :LANES]
-    out_ref[0, :rows, LANES:] = kv_ref[...].astype(BF16)
+    q = q_buf[...].astype(BF16)
+    rows_out[0, :rows, :LANES] = q[:, :LANES]
+    rows_out[0, :rows, LANES:] = kv_buf[...].astype(BF16)
     for g in range(4):
-        out_ref[0, rows:, HALF * g : HALF * (g + 1)] = q[quarter * g : quarter * (g + 1), LANES:]
+        rows_out[0, rows:, HALF * g : HALF * (g + 1)] = q[quarter * g : quarter * (g + 1), LANES:]
+
+
+def spread(factor, q, kv, qm, km, qs, ks, count):
+    rows, width = q.shape[0], q.shape[1] + kv.shape[1]
+    operands = (factor, q, kv, qm, km, qs, ks)
+    return run(
+        spread_kernel,
+        [HBM] * 7,
+        operands,
+        [
+            near((count, *factor.shape), BF16),
+            near((1, rows + rows // 4, 2 * LANES), BF16),
+            near((2, qm.shape[0], width)),
+        ],
+        [pltpu.VMEM(o.shape, o.dtype) for o in operands] + [pltpu.SemaphoreType.DMA((7,))],
+    )
 
 
 def stack_kernel(*refs):
@@ -122,13 +146,10 @@
 
 
 def gradient_kernel(
-    q_ref, kv_ref, x_ref, qw_ref, kvw_ref, qm_ref, km_ref, qs_ref, ks_ref,
-    out_ref, rows_ref, moments_ref, sum_ref, q_buf, kv_buf, x_buf,
-    qw_buf, kvw_buf, qm_buf, km_buf, qs_buf, ks_buf, sems, small_sems,
+    q_ref, kv_ref, x_ref, rows_ref, more_ref, out_ref, both_ref, sum_ref, q_buf, kv_buf, x_buf, sems
 ):
     depth, block, _ = x_buf.shape
     steps = x_ref.shape[0] // block
-    q_width = q_ref.shape[0]
 
     def copies(k):
         at, slot = pl.ds(k * block, block), k % depth
@@ -138,24 +159,11 @@
             pltpu.make_async_copy(x_ref.at[at, :], x_buf.at[slot], sems.at[slot, 2]),
         )
 
-    small = [
-        pltpu.make_async_copy(a, b, small_sems.at[i])
-        for i, (a, b) in enumerate(
-            (
-                (qw_ref, qw_buf),
-                (kvw_ref, kvw_buf),
-                (qm_ref, qm_buf),
-                (km_ref, km_buf),
-                (qs_ref, qs_buf),
-                (ks_ref, ks_buf),
-            )
-        )
-    ]
     for k in range(depth):
         for copy in copies(k):
             copy.start()
-    for copy in small:
-        copy.start()
+    both_ref[0] = rows_ref[0]
+    both_ref[1] = more_ref[0]
     for k in range(steps):
         slot = k % depth
         for copy in copies(k):
@@ -171,38 +179,24 @@
         if k + depth < steps:
             for copy in copies(k + depth):
                 copy.start()
-        if k == depth:
-            for copy in small:
-                copy.wait()
-            fold(qw_buf, kvw_buf, rows_ref)
-            moments_ref[0, :, :q_width] = qm_buf[...]
-            moments_ref[0, :, q_width:] = km_buf[...]
-            moments_ref[1, :, :q_width] = qs_buf[...]
-            moments_ref[1, :, q_width:] = ks_buf[...]
-
-
-def gradients(q_turned, kv, x, small, block=512, depth=4):
+
+
+def gradients(q_turned, kv, x, rows, more, block=512, depth=4):
     q_width, kv_width = q_turned.shape[0], kv.shape[1]
     width = q_width + kv_width
     tokens, model = x.shape
-    rows, half = small[0].shape[0], small[2].shape[0]
     return run(
         gradient_kernel,
-        [HBM] * (3 + len(small)),
-        (q_turned, kv, x, *small),
-        [
-            near((width, model), BF16),
-            near((1, rows + rows // 4, 2 * LANES), BF16),
-            near((2, half, width)),
-        ],
+        [HBM] * 3 + [VMEM] * 2,
+        (q_turned, kv, x, rows, more),
+        [near((width, model), BF16), near((2, *rows.shape[1:]), BF16)],
         [
             pltpu.VMEM((width, model), F32),
             pltpu.VMEM((depth, q_width, block), BF16),
             pltpu.VMEM((depth, block, kv_width), BF16),
             pltpu.VMEM((depth, block, model), BF16),
-        ]
-        + [pltpu.VMEM(a.shape, F32) for a in small]
-        + [pltpu.SemaphoreType.DMA((depth, 3)), pltpu.SemaphoreType.DMA((len(small),))],
+            pltpu.SemaphoreType.DMA((depth, 3)),
+        ],
         2 * width * tokens * model,
         24,
     )
@@ -229,47 +223,26 @@
     return partial, factor.reshape(count * 2 * rows, rank)
 
 
-def pair_kernel(parts_ref, moments_ref, out_ref):
-    rows = parts_ref.shape[1]
-    half = rows // 2
-    out_ref[:rows] = jnp.sum(parts_ref[...].astype(F32), axis=0)
-    out_ref[rows : rows + half] = moments_ref[0]
-    out_ref[rows + half :] = moments_ref[1]
-
-
-def pair_sums(parts, moments):
-    rows, width = parts.shape[1:]
-    return run(pair_kernel, [VMEM] * 2, (parts, moments), [near((2 * rows, width))])[0]
-
-
 def update(value, first, second):
     return 0.8 * first + 0.2 * value, 0.9 * second + 0.1 * value * value
 
 
-def direction_kernel(mine_ref, other_ref, out_ref, moments_ref):
-    core = lax.axis_index("core")
-    count, rows, _ = out_ref.shape
-    half = rows // 2
-    for ref, at in ((mine_ref, core * half), (other_ref, (1 - core) * half)):
-        at = pl.ds(pl.multiple_of(at, half), half)
-        moments_ref[0, at, :] = ref[rows : rows + half]
-        moments_ref[1, at, :] = ref[rows + half :]
-    value = mine_ref[:rows] + other_ref[:rows]
+def direction_kernel(parts_ref, moments_ref, out_ref, sums_ref):
+    value = jnp.sum(parts_ref[...].astype(F32), axis=0)
+    sums_ref[...] = value
     first, second = update(value, moments_ref[0], moments_ref[1])
     direction = (first / (jnp.sqrt(second) + 1e-08)).astype(BF16)
-    for i in range(count):
+    for i in range(out_ref.shape[0]):
         out_ref[i] = direction
 
 
-def direction_tiles(mine, other, count):
-    rows, width = mine.shape[0] // 2, mine.shape[1]
+def direction_tiles(parts, moments):
     return run(
         direction_kernel,
         [VMEM] * 2,
-        (mine, other),
-        [near((count, rows, width), BF16)],
-        [pltpu.VMEM((2, rows, width), F32)],
-    )[0]
+        (parts, moments),
+        [near(parts.shape, BF16), near(parts.shape[1:])],
+    )
 
 
 def stats_kernel(q_width):
@@ -337,14 +310,11 @@
 
 
 def steps_kernel(
-    dir_ref, factor_ref, own_ref, mine_ref, other_ref,
+    dir_ref, factor_ref, own_ref, sums_ref, moments_ref,
     q_ref, kv_ref, own_out, qm_out, km_out, qs_out, ks_out, qm_buf, km_buf, qs_buf, ks_buf, sems,
 ):
-    half, q_width = qm_buf.shape
-    rows = 2 * half
-    at = pl.ds(pl.multiple_of(lax.axis_index("core") * half, half), half)
-    value = mine_ref[at, :] + other_ref[at, :]
-    first, second = update(value, mine_ref[rows : rows + half], mine_ref[rows + half :])
+    q_width = qm_buf.shape[1]
+    first, second = update(sums_ref[...], moments_ref[0], moments_ref[1])
     qm_buf[...] = first[:, :q_width]
     km_buf[...] = first[:, q_width:]
     qs_buf[...] = second[:, :q_width]
@@ -367,13 +337,13 @@
         copy.wait()
 
 
-def unscaled_steps(directions, factor, own, mine, other, kept):
+def unscaled_steps(directions, factor, own, sums, moments, kept):
     model, width = factor.shape[0], directions.shape[1]
     q_width = kept[0].shape[1]
     return run(
         steps_kernel,
         [VMEM] * 5,
-        (directions, factor, own, mine, other),
+        (directions, factor, own, sums, moments),
         [near((q_width, model)), near((model, width - q_width)), near((own.shape[0], width))]
         + [far(k.shape) for k in kept],
         [pltpu.VMEM(k.shape, F32) for k in kept] + [pltpu.SemaphoreType.DMA((len(kept),))],
@@ -452,25 +422,25 @@
     q_width, kv_width = q_cot.shape[1], kv_cot.shape[1]
     width, rank_rows = q_width + kv_width, qm.shape[0]
     chips = lax.axis_size(ZY)
-    mine = exchange(spread(row_factor, chips), ZY)
-    grad, weight_rows, moments = gradients(
-        q_cot.T, kv_cot, x, (q_weight, kv_weight, qm, km, qs, ks)
-    )
-    mine, grad, weight_rows, moments = lax.optimization_barrier((mine, grad, weight_rows, moments))
+    factor_tiles, weight_rows, moments = spread(
+        row_factor, q_weight, kv_weight, qm, km, qs, ks, chips
+    )
     weight_more = swapped(weight_rows, "core", 1)
+    weight_across = shifted(weight_rows, "y", lax.axis_size("y") // 2)
+    mine = exchange(factor_tiles, ZY)
+    grad, weight_both = gradients(q_cot.T, kv_cot, x, weight_rows, weight_more)
+    mine, grad, weight_both, weight_rows = lax.optimization_barrier(
+        (mine, grad, weight_both, weight_rows)
+    )
     other = swapped(mine, "core", 1)
-    weight_across = shifted(weight_rows, "y", lax.axis_size("y") // 2)
-    weight_both = stacked((weight_rows, weight_more))
     weight_beside = turned(weight_both, "y")
     partial, factor = project(mine, other, grad)
-    parts = exchange(partial.reshape(chips, 2 * rank_rows, width), ZY)
+    parts = exchange(partial.reshape(fs_count, rank_rows, width), FS)
     weight_part = stacked((weight_rows, weight_beside, weight_across))
     weight_row = stacked((weight_part, swapped(weight_part, "core", 1)))
     weight_near = turned(weight_row, "z")
-    sums = pair_sums(parts, moments)
-    more = swapped(sums, "core", 1)
-    to_send = direction_tiles(sums, more, chips)
-    directions = exchange(to_send, ZY).reshape(fs_count * rank_rows, width)
+    to_send, sums = direction_tiles(parts, moments)
+    directions = exchange(to_send, FS).reshape(fs_count * rank_rows, width)
     weight_over = swapped(weight_near, "core", 1)
     weight_far = shifted(weight_part, "z", lax.axis_size("z") // 2)
     weight_last = swapped(weight_far, "core", 1)
@@ -481,7 +451,7 @@
     squares = stats(directions, q_width)
     squares = [squares] + [shifted(squares, "tp", k) for k in (2, 1, 3)]
     q_steps, kv_steps, own, *kept = unscaled_steps(
-        directions, factor, row_factor, sums, more, (qm, km, qs, ks)
+        directions, factor, row_factor, sums, moments, (qm, km, qs, ks)
     )
     count = rank_rows * fs_count * lax.axis_size("tp")
     q_new, kv_new, q_step, kv_step, q_copy, kv_copy = finish(

time: 72 us -> 69.8 us (0.969); the launches traced: 70.6 us -> 69.3 us
  starting transfers between devices: 35.3 us -> 32.9 us
  waiting for transfers between devices: 16.9 us -> 18 us
    all_to_all x3, waiting for transfers between devices: 11.1 us -> 14.4 us  [exchange(): return lax.all_to_all(tiles, axis, split_axis=0, concat_axis=0, tiled=True)]
    ppermute x6 -> x5, starting transfers between devices: 8.74 us -> 5.46 us  [swapped(): return lax.ppermute(array, axis, [(i, i ^ bit) for i in range(count)])]
    ppermute x6 -> x5, waiting for transfers between devices: 2.78 us -> 1.04 us  [swapped(): return lax.ppermute(array, axis, [(i, i ^ bit) for i in range(count)])]
    all_to_all x3, starting transfers between devices: 16.3 us -> 17.2 us  [exchange(): return lax.all_to_all(tiles, axis, split_axis=0, concat_axis=0, tiled=True)]
    pallas_call x12 -> x10, Pallas kernels: 16.9 us -> 16.8 us  [run(): pl.pallas_call(kernel, in_specs=list(specs), out_specs=outs or [VMEM] * l...]
  transfers between devices with their start and end apart: 16 -> 15, of which waited for: 8 -> 5; matrix products, arithmetic and copies ran while one was open for 0% -> 0% of each run, Pallas kernels for 20% -> 20%
where the time goes in v4:
time: 69.8 us; the launch traced here: 69.3 us
  starting transfers between devices  32.9 us (47%)
  waiting for transfers between devices  18 us (26%)
  Pallas kernels  16.8 us (24%)
  between operations  0.81 us (1%)
    all_to_all x3, starting transfers between devices, exchange(): return lax.all_to_all(tiles, axis, split_axis=0, concat_axis=0, tiled=True)  17.2 us
    pallas_call x10, Pallas kernels, run(): pl.pallas_call(kernel, in_specs=list(specs), out_specs=outs or [VMEM] * l...  16.8 us
    all_to_all x3, waiting for transfers between devices, exchange(): return lax.all_to_all(tiles, axis, split_axis=0, concat_axis=0, tiled=True)  14.4 us
    ppermute x5, starting transfers between devices, shifted(): lax.ppermute(array, axis, [(i, (i + k) % count) for i in range(count)])  9.1 us
    ppermute x5, starting transfers between devices, swapped(): return lax.ppermute(array, axis, [(i, i ^ bit) for i in range(count)])  5.46 us
    ppermute x5, waiting for transfers between devices, shifted(): lax.ppermute(array, axis, [(i, (i + k) % count) for i in range(count)])  2.53 us
  transfers between devices with their start and end apart: 15, of which 5 were waited for; matrix products, arithmetic and copies ran while one was open for 0% of the time, Pallas kernels for 20%

profile of v4, /device:TPU:1, one launch (start us, length us, event | category | flops | bytes accessed | tf_op | source)
XLA Modules:
  0.0 69.3 jit_solution(17796621012074848916)
XLA Ops:
  0.6 1.8 %shard_map.177 = (bf16[16,64,256]{2,1,0:T(8,128)(2,1)}, bf16[1,80,256]{2,1,0:T(8,128)(2,1)S(1)}, f32[2,8,320]{2,1,0:T(8,128)S(1)}) custom-call(bf16[64,256]{1,0:T(8,128)(2,1)} %own_ref.1, f32[64,192]{1,0:T(8,128)} %q_ref.3, f32[64,128]{1,0:T(8,128)} %kv_ref.5, f32[8,192]{1,0:T(8,128)} %qm_ref.1, f32[8,128]{1,0:T(8,128)} %km_ref.1, f32[8,192]{1,0:T(8,128)} %qs_ref.1, ...), custom_call_target="tpu_custom_call" | custom-call | tf_op jit(solution)/shard_map/pallas_call | solution.py:32
  2.4 1.5 %collective-permute-start = (bf16[1,80,256]{2,1,0:T(8,128)(2,1)S(1)}, bf16[1,80,256]{2,1,0:T(8,128)(2,1)S(1)}, u32[]{:S(2)}, u32[]{:S(2)}) collective-permute-start(bf16[1,80,256]{2,1,0:T(8,128)(2,1)S(1)} %get-tuple-element.52.rows_ref.refs_0_), channel_id=1, source_target_pairs={{0,4},{4,0},{1,5},{5,1},{2,6},{6,2},{3,7},{7,3},{8,12},{12,8},{9,1... | collective-permute-start | bytes 122888 | tf_op jit(solution)/shard_map/ppermute | solution.py:49
  3.9 7.9 %all-to-all-start = ((bf16[16,64,256]{2,1,0:T(8,128)(2,1)}), bf16[16,64,256]{2,1,0:T(8,128)(2,1)S(1)}, u32[]{:S(2)}, u32[]{:S(2)}) async-start(bf16[16,64,256]{2,1,0:T(8,128)(2,1)} %get-tuple-element.38), calls=%async_computation | async-start | bytes 1048576 | tf_op jit(solution)/shard_map/all_to_all | solution.py:44
  11.8 0.0 collective-permute-done.more_ref
  11.8 9.1 %shard_map.178 = (bf16[320,2048]{1,0:T(8,128)(2,1)S(1)}, bf16[2,80,256]{2,1,0:T(8,128)(2,1)S(1)}) custom-call(bf16[192,4608]{1,0:T(8,128)(2,1)} %bitcast.11, bf16[4608,128]{1,0:T(8,128)(2,1)} %kv_ref.4, bf16[4608,2048]{1,0:T(8,128)(2,1)} %x_ref.1, bf16[1,80,256]{2,1,0:T(8,128)(2,1)S(1)} %get-tuple-element.52.rows_ref.refs_0_, ...), custom_call_target="tpu_custom_call" | custom-call | flops 6039797760 | tf_op jit(solution)/shard_map/pallas_call | solution.py:32
  20.9 1.9 %all-to-all-done.mine_ref = bf16[16,64,256]{2,1,0:T(8,128)(2,1)S(1)} async-done(((bf16[16,64,256]{2,1,0:T(8,128)(2,1)}), bf16[16,64,256]{2,1,0:T(8,128)(2,1)S(1)}, u32[]{:S(2)}, u32[]{:S(2)}) %all-to-all-start) | async-done | bytes 524320 | tf_op jit(solution)/shard_map/all_to_all | solution.py:44
  22.8 0.3 collective-permute-start.5
  23.1 1.7 %collective-permute-start.1 = (bf16[16,64,256]{2,1,0:T(8,128)(2,1)S(1)}, bf16[16,64,256]{2,1,0:T(8,128)(2,1)S(1)}, u32[]{:S(2)}, u32[]{:S(2)}) collective-permute-start(bf16[16,64,256]{2,1,0:T(8,128)(2,1)S(1)} %all-to-all-done.mine_ref), channel_id=1, source_target_pairs={{0,4},{4,0},{1,5},{5,1},{2,6},{6,2},{3,7},{7,3},{8,12},{12,8},{9,1... | collective-permute-start | bytes 1572872 | tf_op jit(solution)/shard_map/ppermute | solution.py:49
  24.8 1.8 %collective-permute-start.6 = (bf16[1,80,256]{2,1,0:T(8,128)(2,1)S(1)}, bf16[1,80,256]{2,1,0:T(8,128)(2,1)S(1)}, u32[]{:S(2)}, u32[]{:S(2)}) collective-permute-start(bf16[1,80,256]{2,1,0:T(8,128)(2,1)S(1)} %get-tuple-element.52.rows_ref.refs_0_), channel_id=1, source_target_pairs={{0,16},{8,24},{16,0},{24,8},{1,17},{9,25},{17,1},{25,9},{2,18},{10... | collective-permute-start | bytes 122888 | tf_op jit(solution)/shard_map/ppermute | solution.py:54
  26.6 2.5 %collective-permute-done.6.refs_2_ = bf16[1,80,256]{2,1,0:T(8,128)(2,1)S(1)} collective-permute-done((bf16[1,80,256]{2,1,0:T(8,128)(2,1)S(1)}, bf16[1,80,256]{2,1,0:T(8,128)(2,1)S(1)}, u32[]{:S(2)}, u32[]{:S(2)}) %collective-permute-start.6) | collective-permute-done | bytes 40992 | tf_op jit(solution)/shard_map/ppermute | solution.py:54
  29.1 0.0 collective-permute-done.5.refs_1_
  29.2 1.2 %collective-permute-start.7 = (bf16[4,80,256]{2,1,0:T(8,128)(2,1)S(1)}, bf16[4,80,256]{2,1,0:T(8,128)(2,1)S(1)}, u32[]{:S(2)}, u32[]{:S(2)}) collective-permute-start(bf16[4,80,256]{2,1,0:T(8,128)(2,1)S(1)} %shard_map.183.refs_0_), channel_id=1, source_target_pairs={{0,4},{4,0},{1,5},{5,1},{2,6},{6,2},{3,7},{7,3},{8,12},{12,8},{9,1... | collective-permute-start | bytes 491528 | tf_op jit(solution)/shard_map/ppermute | solution.py:49
  30.4 1.0 %collective-permute-done.7.refs_1_ = bf16[4,80,256]{2,1,0:T(8,128)(2,1)S(1)} collective-permute-done((bf16[4,80,256]{2,1,0:T(8,128)(2,1)S(1)}, bf16[4,80,256]{2,1,0:T(8,128)(2,1)S(1)}, u32[]{:S(2)}, u32[]{:S(2)}) %collective-permute-start.7) | collective-permute-done | bytes 163872 | tf_op jit(solution)/shard_map/ppermute | solution.py:49
  31.4 0.0 copy-start.3
  31.5 0.9 %collective-permute-start.8 = (bf16[8,80,256]{2,1,0:T(8,128)(2,1)S(1)}, bf16[8,80,256]{2,1,0:T(8,128)(2,1)}, u32[]{:S(2)}, u32[]{:S(2)}) collective-permute-start(bf16[8,80,256]{2,1,0:T(8,128)(2,1)S(1)} %shard_map.184.here_ref), channel_id=1, source_target_pairs={{0,96},{4,36},{8,104},{12,44},{16,112},{20,52},{24,120},{28,60},{3... | collective-permute-start | bytes 983048 | tf_op jit(solution)/shard_map/ppermute | solution.py:69
  32.3 0.0 collective-permute-done.1.other_ref
  32.3 0.7 shard_map.179
  33.0 0.0 copy-start.1
  33.0 0.7 copy-done.1
  33.7 5.4 %all-to-all-start.1 = ((bf16[32,8,320]{2,1,0:T(8,128)(2,1)}), bf16[32,8,320]{2,1,0:T(8,128)(2,1)S(1)}, u32[]{:S(2)}, u32[]{:S(2)}) async-start(bf16[32,8,320]{2,1,0:T(8,128)(2,1)} %bitcast.10), calls=%async_computation.1 | async-start | bytes 393216 | tf_op jit(solution)/shard_map/all_to_all | solution.py:44
  39.1 3.0 %collective-permute-start.10 = (bf16[4,80,256]{2,1,0:T(8,128)(2,1)S(1)}, bf16[4,80,256]{2,1,0:T(8,128)(2,1)S(1)}, u32[]{:S(2)}, u32[]{:S(2)}) collective-permute-start(bf16[4,80,256]{2,1,0:T(8,128)(2,1)S(1)} %shard_map.183.refs_0_), channel_id=1, source_target_pairs={{0,64},{32,96},{64,0},{96,32},{1,65},{33,97},{65,1},{97,33},{2,66}... | collective-permute-start | bytes 491528 | tf_op jit(solution)/shard_map/ppermute | solution.py:54
  42.1 0.0 collective-permute-done.8.near_ref
  42.1 0.7 collective-permute-start.9
  42.8 4.6 %all-to-all-done.1.parts_ref = bf16[32,8,320]{2,1,0:T(8,128)(2,1)S(1)} async-done(((bf16[32,8,320]{2,1,0:T(8,128)(2,1)}), bf16[32,8,320]{2,1,0:T(8,128)(2,1)S(1)}, u32[]{:S(2)}, u32[]{:S(2)}) %all-to-all-start.1) | async-done | bytes 163872 | tf_op jit(solution)/shard_map/all_to_all | solution.py:44
  47.4 0.7 %shard_map.180 = (bf16[32,8,320]{2,1,0:T(8,128)(2,1)}, f32[8,320]{1,0:T(8,128)S(1)}) custom-call(bf16[32,8,320]{2,1,0:T(8,128)(2,1)S(1)} %all-to-all-done.1.parts_ref, f32[2,8,320]{2,1,0:T(8,128)S(1)} %get-tuple-element.45.moments_ref), custom_call_target="tpu_custom_call" | custom-call | tf_op jit(solution)/shard_map/pallas_call | solution.py:32
  48.2 0.0 copy-start
  48.2 0.0 copy-start.2
  48.2 3.9 %all-to-all-start.2 = ((bf16[32,8,320]{2,1,0:T(8,128)(2,1)}), bf16[32,8,320]{2,1,0:T(8,128)(2,1)S(1)}, u32[]{:S(2)}, u32[]{:S(2)}) async-start(bf16[32,8,320]{2,1,0:T(8,128)(2,1)} %get-tuple-element.46), calls=%async_computation.2 | async-start | bytes 393216 | tf_op jit(solution)/shard_map/all_to_all | solution.py:44
  52.1 0.0 collective-permute-done.10.far_ref
  52.1 0.4 collective-permute-start.11
  52.6 7.9 %all-to-all-done.2 = bf16[32,8,320]{2,1,0:T(8,128)(2,1)S(1)} async-done(((bf16[32,8,320]{2,1,0:T(8,128)(2,1)}), bf16[32,8,320]{2,1,0:T(8,128)(2,1)S(1)}, u32[]{:S(2)}, u32[]{:S(2)}) %all-to-all-start.2) | async-done | bytes 163872 | tf_op jit(solution)/shard_map/all_to_all | solution.py:44
  60.5 0.2 shard_map.181.squares_0
  60.6 2.5 %collective-permute-start.4 = (f32[8,128]{1,0:T(8,128)S(1)}, f32[8,128]{1,0:T(8,128)S(1)}, u32[]{:S(2)}, u32[]{:S(2)}) collective-permute-start(f32[8,128]{1,0:T(8,128)S(1)} %shard_map.181.squares_0), channel_id=1, source_target_pairs={{0,3},{1,0},{2,1},{3,2},{4,7},{5,4},{6,5},{7,6},{8,11},{9,8},{10,9... | collective-permute-start | bytes 12296 | tf_op jit(solution)/shard_map/ppermute | solution.py:54
  63.1 0.0 collective-permute-start.3
  63.1 1.7 %collective-permute-start.2 = (f32[8,128]{1,0:T(8,128)S(1)}, f32[8,128]{1,0:T(8,128)S(1)}, u32[]{:S(2)}, u32[]{:S(2)}) collective-permute-start(f32[8,128]{1,0:T(8,128)S(1)} %shard_map.181.squares_0), channel_id=1, source_target_pairs={{0,2},{1,3},{2,0},{3,1},{4,6},{5,7},{6,4},{7,5},{8,10},{9,11},{10,... | collective-permute-start | bytes 12296 | tf_op jit(solution)/shard_map/ppermute | solution.py:54
  64.9 0.0 copy-done.3
  64.9 1.4 %shard_map.182 = (f32[192,2048]{1,0:T(8,128)S(1)}, f32[2048,128]{1,0:T(8,128)S(1)}, f32[64,320]{1,0:T(8,128)S(1)}, f32[8,192]{1,0:T(8,128)}, f32[8,128]{1,0:T(8,...) custom-call(bf16[256,320]{1,0:T(8,128)(2,1)S(1)} %bitcast.7, bf16[2048,256]{1,0:T(8,128)(2,1)S(1)} %bitcast.8, ...), custom_call_target="tpu_custom_call" | custom-call | flops 335544320 | tf_op jit(solution)/shard_map/pallas_call | solution.py:32
  66.2 0.0 collective-permute-done.11.last_ref
  66.2 0.0 collective-permute-done.9.over_ref
  66.2 1.6 %shard_map.185 = (bf16[192,2048]{1,0:T(8,128)(2,1)S(1)}, bf16[4,4,2,64,128]{4,3,2,1,0:T(8,128)(2,1)S(1)}) custom-call(bf16[8,80,256]{2,1,0:T(8,128)(2,1)S(1)} %shard_map.184.here_ref, bf16[8,80,256]{2,1,0:T(8,128)(2,1)} %collective-permute-done.8.near_ref, bf16[8,80,256]{2,1,0:T(8,128)(2,1)S(1)} %collective-permute-done.9.over_ref, ...), custom_call_target="tpu_custom_call" | custom-call | tf_op jit(solution)/shard_map/pallas_call | solution.py:32
  67.8 0.0 collective-permute-done.4.squares_3
  67.8 0.0 collective-permute-done.3.squares_2
  67.8 0.0 collective-permute-done.2.squares_1
  67.9 0.0 copy-done
  67.9 0.0 copy-done.2
  67.9 1.4 %shard_map.186 = (f32[64,192]{1,0:T(8,128)}, f32[64,128]{1,0:T(8,128)}, f32[64,192]{1,0:T(8,128)}, f32[64,128]{1,0:T(8,128)}, bf16[192,2048]{1,0:T(8,128)(2,1)}, /*index=5*/bf16[2048,128]{1,0:T(8,128)(2,1)}) custom-call(f32[8,128]{1,0:T(8,128)S(1)} %shard_map.181.squares_0, f32[8,128]{1,0:T(8,128)S(1)} %collective-permute-done.2.squares_1, ...), custom_call_target="tpu_custom_call" | custom-call | tf_op jit(solution)/shard_map/pallas_call | solution.py:32
  (2 shorter events, 0.0 us)
Async XLA Ops:
  2.4 9.4 %collective-permute-start = (bf16[1,80,256]{2,1,0:T(8,128)(2,1)S(1)}, bf16[1,80,256]{2,1,0:T(8,128)(2,1)S(1)}, u32[]{:S(2)}, u32[]{:S(2)}) collective-permute-start(bf16[1,80,256]{2,1,0:T(8,128)(2,1)S(1)} %get-tuple-element.52.rows_ref.refs_0_), channel_id=1, source_target_pairs={{0,4},{4,0},{1,5},{5,1},{2,6},{6,2},{3,7},{7,3},{8,12},{12,8},{9,1... | collective-permute-start | bytes 122888 | tf_op jit(solution)/shard_map/ppermute | solution.py:49
  3.9 18.9 %all-to-all-start = ((bf16[16,64,256]{2,1,0:T(8,128)(2,1)}), bf16[16,64,256]{2,1,0:T(8,128)(2,1)S(1)}, u32[]{:S(2)}, u32[]{:S(2)}) async-start(bf16[16,64,256]{2,1,0:T(8,128)(2,1)} %get-tuple-element.38), calls=%async_computation | async-start | bytes 1048576 | tf_op jit(solution)/shard_map/all_to_all | solution.py:44
  22.8 6.3 %collective-permute-start.5 = (bf16[2,80,256]{2,1,0:T(8,128)(2,1)S(1)}, bf16[2,80,256]{2,1,0:T(8,128)(2,1)S(1)}, u32[]{:S(2)}, u32[]{:S(2)}) collective-permute-start(bf16[2,80,256]{2,1,0:T(8,128)(2,1)S(1)} %get-tuple-element.53), channel_id=1, source_target_pairs={{0,24},{4,12},{8,0},{12,20},{16,8},{20,28},{24,16},{28,4},{32,56},... | collective-permute-start | bytes 245768 | tf_op jit(solution)/shard_map/ppermute | solution.py:69
  23.1 9.3 %collective-permute-start.1 = (bf16[16,64,256]{2,1,0:T(8,128)(2,1)S(1)}, bf16[16,64,256]{2,1,0:T(8,128)(2,1)S(1)}, u32[]{:S(2)}, u32[]{:S(2)}) collective-permute-start(bf16[16,64,256]{2,1,0:T(8,128)(2,1)S(1)} %all-to-all-done.mine_ref), channel_id=1, source_target_pairs={{0,4},{4,0},{1,5},{5,1},{2,6},{6,2},{3,7},{7,3},{8,12},{12,8},{9,1... | collective-permute-start | bytes 1572872 | tf_op jit(solution)/shard_map/ppermute | solution.py:49
  24.8 4.4 %collective-permute-start.6 = (bf16[1,80,256]{2,1,0:T(8,128)(2,1)S(1)}, bf16[1,80,256]{2,1,0:T(8,128)(2,1)S(1)}, u32[]{:S(2)}, u32[]{:S(2)}) collective-permute-start(bf16[1,80,256]{2,1,0:T(8,128)(2,1)S(1)} %get-tuple-element.52.rows_ref.refs_0_), channel_id=1, source_target_pairs={{0,16},{8,24},{16,0},{24,8},{1,17},{9,25},{17,1},{25,9},{2,18},{10... | collective-permute-start | bytes 122888 | tf_op jit(solution)/shard_map/ppermute | solution.py:54
  29.2 2.3 %collective-permute-start.7 = (bf16[4,80,256]{2,1,0:T(8,128)(2,1)S(1)}, bf16[4,80,256]{2,1,0:T(8,128)(2,1)S(1)}, u32[]{:S(2)}, u32[]{:S(2)}) collective-permute-start(bf16[4,80,256]{2,1,0:T(8,128)(2,1)S(1)} %shard_map.183.refs_0_), channel_id=1, source_target_pairs={{0,4},{4,0},{1,5},{5,1},{2,6},{6,2},{3,7},{7,3},{8,12},{12,8},{9,1... | collective-permute-start | bytes 491528 | tf_op jit(solution)/shard_map/ppermute | solution.py:49
  31.4 33.4 %copy-start.3 = (bf16[64,256]{1,0:T(8,128)(2,1)S(1)}, bf16[64,256]{1,0:T(8,128)(2,1)}, u32[]{:S(2)}) copy-start(bf16[64,256]{1,0:T(8,128)(2,1)} %own_ref.1) | copy-start | bytes 98308
  31.5 10.7 %collective-permute-start.8 = (bf16[8,80,256]{2,1,0:T(8,128)(2,1)S(1)}, bf16[8,80,256]{2,1,0:T(8,128)(2,1)}, u32[]{:S(2)}, u32[]{:S(2)}) collective-permute-start(bf16[8,80,256]{2,1,0:T(8,128)(2,1)S(1)} %shard_map.184.here_ref), channel_id=1, source_target_pairs={{0,96},{4,36},{8,104},{12,44},{16,112},{20,52},{24,120},{28,60},{3... | collective-permute-start | bytes 983048 | tf_op jit(solution)/shard_map/ppermute | solution.py:69
  33.0 0.7 copy-start.1
  33.7 13.7 %all-to-all-start.1 = ((bf16[32,8,320]{2,1,0:T(8,128)(2,1)}), bf16[32,8,320]{2,1,0:T(8,128)(2,1)S(1)}, u32[]{:S(2)}, u32[]{:S(2)}) async-start(bf16[32,8,320]{2,1,0:T(8,128)(2,1)} %bitcast.10), calls=%async_computation.1 | async-start | bytes 393216 | tf_op jit(solution)/shard_map/all_to_all | solution.py:44
  39.1 13.1 %collective-permute-start.10 = (bf16[4,80,256]{2,1,0:T(8,128)(2,1)S(1)}, bf16[4,80,256]{2,1,0:T(8,128)(2,1)S(1)}, u32[]{:S(2)}, u32[]{:S(2)}) collective-permute-start(bf16[4,80,256]{2,1,0:T(8,128)(2,1)S(1)} %shard_map.183.refs_0_), channel_id=1, source_target_pairs={{0,64},{32,96},{64,0},{96,32},{1,65},{33,97},{65,1},{97,33},{2,66}... | collective-permute-start | bytes 491528 | tf_op jit(solution)/shard_map/ppermute | solution.py:54
  42.1 24.1 %collective-permute-start.9 = (bf16[8,80,256]{2,1,0:T(8,128)(2,1)}, bf16[8,80,256]{2,1,0:T(8,128)(2,1)S(1)}, u32[]{:S(2)}, u32[]{:S(2)}) collective-permute-start(bf16[8,80,256]{2,1,0:T(8,128)(2,1)} %collective-permute-done.8.near_ref), channel_id=1, source_target_pairs={{0,4},{4,0},{1,5},{5,1},{2,6},{6,2},{3,7},{7,3},{8,12},{12,8},{9,1... | collective-permute-start | bytes 983048 | tf_op jit(solution)/shard_map/ppermute | solution.py:49
  48.2 19.7 %copy-start = (f32[64,192]{1,0:T(8,128)S(1)}, f32[64,192]{1,0:T(8,128)}, u32[]{:S(2)}) copy-start(f32[64,192]{1,0:T(8,128)} %q_ref.3) | copy-start | bytes 147460
  48.2 19.7 %copy-start.2 = (f32[64,128]{1,0:T(8,128)S(1)}, f32[64,128]{1,0:T(8,128)}, u32[]{:S(2)}) copy-start(f32[64,128]{1,0:T(8,128)} %kv_ref.5) | copy-start | bytes 98308
  48.2 12.3 %all-to-all-start.2 = ((bf16[32,8,320]{2,1,0:T(8,128)(2,1)}), bf16[32,8,320]{2,1,0:T(8,128)(2,1)S(1)}, u32[]{:S(2)}, u32[]{:S(2)}) async-start(bf16[32,8,320]{2,1,0:T(8,128)(2,1)} %get-tuple-element.46), calls=%async_computation.2 | async-start | bytes 393216 | tf_op jit(solution)/shard_map/all_to_all | solution.py:44
  52.1 14.1 %collective-permute-start.11 = (bf16[4,80,256]{2,1,0:T(8,128)(2,1)S(1)}, bf16[4,80,256]{2,1,0:T(8,128)(2,1)S(1)}, u32[]{:S(2)}, u32[]{:S(2)}) collective-permute-start(bf16[4,80,256]{2,1,0:T(8,128)(2,1)S(1)} %collective-permute-done.10.far_ref), channel_id=1, source_target_pairs={{0,4},{4,0},{1,5},{5,1},{2,6},{6,2},{3,7},{7,3},{8,12},{12,8},{9,1... | collective-permute-start | bytes 491528 | tf_op jit(solution)/shard_map/ppermute | solution.py:49
  60.6 7.2 %collective-permute-start.4 = (f32[8,128]{1,0:T(8,128)S(1)}, f32[8,128]{1,0:T(8,128)S(1)}, u32[]{:S(2)}, u32[]{:S(2)}) collective-permute-start(f32[8,128]{1,0:T(8,128)S(1)} %shard_map.181.squares_0), channel_id=1, source_target_pairs={{0,3},{1,0},{2,1},{3,2},{4,7},{5,4},{6,5},{7,6},{8,11},{9,8},{10,9... | collective-permute-start | bytes 12296 | tf_op jit(solution)/shard_map/ppermute | solution.py:54
  63.1 4.7 %collective-permute-start.3 = (f32[8,128]{1,0:T(8,128)S(1)}, f32[8,128]{1,0:T(8,128)S(1)}, u32[]{:S(2)}, u32[]{:S(2)}) collective-permute-start(f32[8,128]{1,0:T(8,128)S(1)} %shard_map.181.squares_0), channel_id=1, source_target_pairs={{0,1},{1,2},{2,3},{3,0},{4,5},{5,6},{6,7},{7,4},{8,9},{9,10},{10,1... | collective-permute-start | bytes 12296 | tf_op jit(solution)/shard_map/ppermute | solution.py:54
  63.1 4.7 %collective-permute-start.2 = (f32[8,128]{1,0:T(8,128)S(1)}, f32[8,128]{1,0:T(8,128)S(1)}, u32[]{:S(2)}, u32[]{:S(2)}) collective-permute-start(f32[8,128]{1,0:T(8,128)S(1)} %shard_map.181.squares_0), channel_id=1, source_target_pairs={{0,2},{1,3},{2,0},{3,1},{4,6},{5,7},{6,4},{7,5},{8,10},{9,11},{10,... | collective-permute-start | bytes 12296 | tf_op jit(solution)/shard_map/ppermute | solution.py:54

commit v5 on v4

--- a/solution.py
+++ b/solution.py
@@ -69,14 +69,6 @@
     return lax.ppermute(array, FS, pairs)
 
 
-def fetch(pairs, sems):
-    copies = [pltpu.make_async_copy(a, b, sems.at[i]) for i, (a, b) in enumerate(pairs)]
-    for copy in copies:
-        copy.start()
-    for copy in copies:
-        copy.wait()
-
-
 LANES = 128
 HALF = LANES // 2
 
@@ -85,21 +77,27 @@
     factor_ref, q_ref, kv_ref, qm_ref, km_ref, qs_ref, ks_ref, factor_out, rows_out, moments_out,
     factor_buf, q_buf, kv_buf, qm_buf, km_buf, qs_buf, ks_buf, sems,
 ):
-    fetch(
-        (
-            (factor_ref, factor_buf),
-            (q_ref, q_buf),
-            (kv_ref, kv_buf),
-            (qm_ref, qm_buf),
-            (km_ref, km_buf),
-            (qs_ref, qs_buf),
-            (ks_ref, ks_buf),
-        ),
-        sems,
-    )
-    factor = factor_buf[...]
-    for i in range(factor_out.shape[0]):
-        factor_out[i] = factor
+    pairs = (
+        (factor_ref, factor_buf),
+        (q_ref, q_buf),
+        (kv_ref, kv_buf),
+        (qm_ref, qm_buf),
+        (km_ref, km_buf),
+        (qs_ref, qs_buf),
+        (ks_ref, ks_buf),
+    )
+    arrivals = [pltpu.make_async_copy(a, b, sems.at[i]) for i, (a, b) in enumerate(pairs)]
+    for copy in arrivals:
+        copy.start()
+    arrivals[0].wait()
+    sent = [
+        pltpu.make_async_copy(factor_buf, factor_out.at[i], sems.at[len(pairs) + i])
+        for i in range(factor_out.shape[0])
+    ]
+    for copy in sent:
+        copy.start()
+    for copy in arrivals[1:]:
+        copy.wait()
     q_width = q_ref.shape[1]
     moments_out[0, :, :q_width] = qm_buf[...]
     moments_out[0, :, q_width:] = km_buf[...]
@@ -112,6 +110,8 @@
     rows_out[0, :rows, LANES:] = kv_buf[...].astype(BF16)
     for g in range(4):
         rows_out[0, rows:, HALF * g : HALF * (g + 1)] = q[quarter * g : quarter * (g + 1), LANES:]
+    for copy in sent:
+        copy.wait()
 
 
 def spread(factor, q, kv, qm, km, qs, ks, count):
@@ -122,11 +122,12 @@
         [HBM] * 7,
         operands,
         [
-            near((count, *factor.shape), BF16),
+            far((count, *factor.shape), BF16),
             near((1, rows + rows // 4, 2 * LANES), BF16),
             near((2, qm.shape[0], width)),
         ],
-        [pltpu.VMEM(o.shape, o.dtype) for o in operands] + [pltpu.SemaphoreType.DMA((7,))],
+        [pltpu.VMEM(o.shape, o.dtype) for o in operands] + [pltpu.SemaphoreType.DMA((7 + count,))],
+        outs=[HBM, VMEM, VMEM],
     )
 
 

time: 69.8 us -> 69.7 us (level)
  no operation moved by 1% of the time
where the time goes in v5:
time: 69.7 us; the launch traced here: 69.2 us
  starting transfers between devices  32.9 us (47%)
  waiting for transfers between devices  18 us (26%)
  Pallas kernels  16.8 us (24%)
  between operations  0.81 us (1%)
    all_to_all x3, starting transfers between devices, exchange(): return lax.all_to_all(tiles, axis, split_axis=0, concat_axis=0, tiled=True)  17.2 us
    pallas_call x10, Pallas kernels, run(): pl.pallas_call(kernel, in_specs=list(specs), out_specs=outs or [VMEM] * l...  16.8 us
    all_to_all x3, waiting for transfers between devices, exchange(): return lax.all_to_all(tiles, axis, split_axis=0, concat_axis=0, tiled=True)  14.4 us
    ppermute x5, starting transfers between devices, shifted(): lax.ppermute(array, axis, [(i, (i + k) % count) for i in range(count)])  9.11 us
    ppermute x5, starting transfers between devices, swapped(): return lax.ppermute(array, axis, [(i, i ^ bit) for i in range(count)])  5.46 us
    ppermute x5, waiting for transfers between devices, shifted(): lax.ppermute(array, axis, [(i, (i + k) % count) for i in range(count)])  2.53 us
  transfers between devices with their start and end apart: 15, of which 5 were waited for; matrix products, arithmetic and copies ran while one was open for 0% of the time, Pallas kernels for 20%

profile of v5, /device:TPU:1, one launch (start us, length us, event | category | flops | bytes accessed | tf_op | source)
XLA Modules:
  0.0 69.2 jit_solution(9863065570331690121)
XLA Ops:
  0.6 1.7 %shard_map.177 = (bf16[16,64,256]{2,1,0:T(8,128)(2,1)}, bf16[1,80,256]{2,1,0:T(8,128)(2,1)S(1)}, f32[2,8,320]{2,1,0:T(8,128)S(1)}) custom-call(bf16[64,256]{1,0:T(8,128)(2,1)} %own_ref.1, f32[64,192]{1,0:T(8,128)} %q_ref.3, f32[64,128]{1,0:T(8,128)} %kv_ref.5, f32[8,192]{1,0:T(8,128)} %qm_ref.1, f32[8,128]{1,0:T(8,128)} %km_ref.1, f32[8,192]{1,0:T(8,128)} %qs_ref.1, ...), custom_call_target="tpu_custom_call" | custom-call | tf_op jit(solution)/shard_map/pallas_call | solution.py:32
  2.4 1.5 %collective-permute-start = (bf16[1,80,256]{2,1,0:T(8,128)(2,1)S(1)}, bf16[1,80,256]{2,1,0:T(8,128)(2,1)S(1)}, u32[]{:S(2)}, u32[]{:S(2)}) collective-permute-start(bf16[1,80,256]{2,1,0:T(8,128)(2,1)S(1)} %get-tuple-element.52.rows_ref.refs_0_), channel_id=1, source_target_pairs={{0,4},{4,0},{1,5},{5,1},{2,6},{6,2},{3,7},{7,3},{8,12},{12,8},{9,1... | collective-permute-start | bytes 122888 | tf_op jit(solution)/shard_map/ppermute | solution.py:49
  3.9 7.9 %all-to-all-start = ((bf16[16,64,256]{2,1,0:T(8,128)(2,1)}), bf16[16,64,256]{2,1,0:T(8,128)(2,1)S(1)}, u32[]{:S(2)}, u32[]{:S(2)}) async-start(bf16[16,64,256]{2,1,0:T(8,128)(2,1)} %get-tuple-element.38), calls=%async_computation | async-start | bytes 1048576 | tf_op jit(solution)/shard_map/all_to_all | solution.py:44
  11.7 0.0 collective-permute-done.more_ref
  11.7 9.1 %shard_map.178 = (bf16[320,2048]{1,0:T(8,128)(2,1)S(1)}, bf16[2,80,256]{2,1,0:T(8,128)(2,1)S(1)}) custom-call(bf16[192,4608]{1,0:T(8,128)(2,1)} %bitcast.11, bf16[4608,128]{1,0:T(8,128)(2,1)} %kv_ref.4, bf16[4608,2048]{1,0:T(8,128)(2,1)} %x_ref.1, bf16[1,80,256]{2,1,0:T(8,128)(2,1)S(1)} %get-tuple-element.52.rows_ref.refs_0_, ...), custom_call_target="tpu_custom_call" | custom-call | flops 6039797760 | tf_op jit(solution)/shard_map/pallas_call | solution.py:32
  20.9 1.9 %all-to-all-done.mine_ref = bf16[16,64,256]{2,1,0:T(8,128)(2,1)S(1)} async-done(((bf16[16,64,256]{2,1,0:T(8,128)(2,1)}), bf16[16,64,256]{2,1,0:T(8,128)(2,1)S(1)}, u32[]{:S(2)}, u32[]{:S(2)}) %all-to-all-start) | async-done | bytes 524320 | tf_op jit(solution)/shard_map/all_to_all | solution.py:44
  22.8 0.3 collective-permute-start.5
  23.1 1.7 %collective-permute-start.1 = (bf16[16,64,256]{2,1,0:T(8,128)(2,1)S(1)}, bf16[16,64,256]{2,1,0:T(8,128)(2,1)S(1)}, u32[]{:S(2)}, u32[]{:S(2)}) collective-permute-start(bf16[16,64,256]{2,1,0:T(8,128)(2,1)S(1)} %all-to-all-done.mine_ref), channel_id=1, source_target_pairs={{0,4},{4,0},{1,5},{5,1},{2,6},{6,2},{3,7},{7,3},{8,12},{12,8},{9,1... | collective-permute-start | bytes 1572872 | tf_op jit(solution)/shard_map/ppermute | solution.py:49
  24.7 1.8 %collective-permute-start.6 = (bf16[1,80,256]{2,1,0:T(8,128)(2,1)S(1)}, bf16[1,80,256]{2,1,0:T(8,128)(2,1)S(1)}, u32[]{:S(2)}, u32[]{:S(2)}) collective-permute-start(bf16[1,80,256]{2,1,0:T(8,128)(2,1)S(1)} %get-tuple-element.52.rows_ref.refs_0_), channel_id=1, source_target_pairs={{0,16},{8,24},{16,0},{24,8},{1,17},{9,25},{17,1},{25,9},{2,18},{10... | collective-permute-start | bytes 122888 | tf_op jit(solution)/shard_map/ppermute | solution.py:54
  26.6 2.5 %collective-permute-done.6.refs_2_ = bf16[1,80,256]{2,1,0:T(8,128)(2,1)S(1)} collective-permute-done((bf16[1,80,256]{2,1,0:T(8,128)(2,1)S(1)}, bf16[1,80,256]{2,1,0:T(8,128)(2,1)S(1)}, u32[]{:S(2)}, u32[]{:S(2)}) %collective-permute-start.6) | collective-permute-done | bytes 40992 | tf_op jit(solution)/shard_map/ppermute | solution.py:54
  29.1 0.0 collective-permute-done.5.refs_1_
  29.1 1.2 %collective-permute-start.7 = (bf16[4,80,256]{2,1,0:T(8,128)(2,1)S(1)}, bf16[4,80,256]{2,1,0:T(8,128)(2,1)S(1)}, u32[]{:S(2)}, u32[]{:S(2)}) collective-permute-start(bf16[4,80,256]{2,1,0:T(8,128)(2,1)S(1)} %shard_map.183.refs_0_), channel_id=1, source_target_pairs={{0,4},{4,0},{1,5},{5,1},{2,6},{6,2},{3,7},{7,3},{8,12},{12,8},{9,1... | collective-permute-start | bytes 491528 | tf_op jit(solution)/shard_map/ppermute | solution.py:49
  30.4 1.0 %collective-permute-done.7.refs_1_ = bf16[4,80,256]{2,1,0:T(8,128)(2,1)S(1)} collective-permute-done((bf16[4,80,256]{2,1,0:T(8,128)(2,1)S(1)}, bf16[4,80,256]{2,1,0:T(8,128)(2,1)S(1)}, u32[]{:S(2)}, u32[]{:S(2)}) %collective-permute-start.7) | collective-permute-done | bytes 163872 | tf_op jit(solution)/shard_map/ppermute | solution.py:49
  31.4 0.0 copy-start.3
  31.4 0.9 %collective-permute-start.8 = (bf16[8,80,256]{2,1,0:T(8,128)(2,1)S(1)}, bf16[8,80,256]{2,1,0:T(8,128)(2,1)}, u32[]{:S(2)}, u32[]{:S(2)}) collective-permute-start(bf16[8,80,256]{2,1,0:T(8,128)(2,1)S(1)} %shard_map.184.here_ref), channel_id=1, source_target_pairs={{0,96},{4,36},{8,104},{12,44},{16,112},{20,52},{24,120},{28,60},{3... | collective-permute-start | bytes 983048 | tf_op jit(solution)/shard_map/ppermute | solution.py:69
  32.3 0.0 collective-permute-done.1.other_ref
  32.3 0.7 shard_map.179
  33.0 0.0 copy-start.1
  33.0 0.7 copy-done.1
  33.7 5.4 %all-to-all-start.1 = ((bf16[32,8,320]{2,1,0:T(8,128)(2,1)}), bf16[32,8,320]{2,1,0:T(8,128)(2,1)S(1)}, u32[]{:S(2)}, u32[]{:S(2)}) async-start(bf16[32,8,320]{2,1,0:T(8,128)(2,1)} %bitcast.10), calls=%async_computation.1 | async-start | bytes 393216 | tf_op jit(solution)/shard_map/all_to_all | solution.py:44
  39.0 3.0 %collective-permute-start.10 = (bf16[4,80,256]{2,1,0:T(8,128)(2,1)S(1)}, bf16[4,80,256]{2,1,0:T(8,128)(2,1)S(1)}, u32[]{:S(2)}, u32[]{:S(2)}) collective-permute-start(bf16[4,80,256]{2,1,0:T(8,128)(2,1)S(1)} %shard_map.183.refs_0_), channel_id=1, source_target_pairs={{0,64},{32,96},{64,0},{96,32},{1,65},{33,97},{65,1},{97,33},{2,66}... | collective-permute-start | bytes 491528 | tf_op jit(solution)/shard_map/ppermute | solution.py:54
  42.1 0.0 collective-permute-done.8.near_ref
  42.1 0.7 collective-permute-start.9
  42.8 4.6 %all-to-all-done.1.parts_ref = bf16[32,8,320]{2,1,0:T(8,128)(2,1)S(1)} async-done(((bf16[32,8,320]{2,1,0:T(8,128)(2,1)}), bf16[32,8,320]{2,1,0:T(8,128)(2,1)S(1)}, u32[]{:S(2)}, u32[]{:S(2)}) %all-to-all-start.1) | async-done | bytes 163872 | tf_op jit(solution)/shard_map/all_to_all | solution.py:44
  47.4 0.7 %shard_map.180 = (bf16[32,8,320]{2,1,0:T(8,128)(2,1)}, f32[8,320]{1,0:T(8,128)S(1)}) custom-call(bf16[32,8,320]{2,1,0:T(8,128)(2,1)S(1)} %all-to-all-done.1.parts_ref, f32[2,8,320]{2,1,0:T(8,128)S(1)} %get-tuple-element.45.moments_ref), custom_call_target="tpu_custom_call" | custom-call | tf_op jit(solution)/shard_map/pallas_call | solution.py:32
  48.1 0.0 copy-start
  48.2 0.0 copy-start.2
  48.2 3.9 %all-to-all-start.2 = ((bf16[32,8,320]{2,1,0:T(8,128)(2,1)}), bf16[32,8,320]{2,1,0:T(8,128)(2,1)S(1)}, u32[]{:S(2)}, u32[]{:S(2)}) async-start(bf16[32,8,320]{2,1,0:T(8,128)(2,1)} %get-tuple-element.46), calls=%async_computation.2 | async-start | bytes 393216 | tf_op jit(solution)/shard_map/all_to_all | solution.py:44
  52.1 0.0 collective-permute-done.10.far_ref
  52.1 0.4 collective-permute-start.11
  52.5 7.9 %all-to-all-done.2 = bf16[32,8,320]{2,1,0:T(8,128)(2,1)S(1)} async-done(((bf16[32,8,320]{2,1,0:T(8,128)(2,1)}), bf16[32,8,320]{2,1,0:T(8,128)(2,1)S(1)}, u32[]{:S(2)}, u32[]{:S(2)}) %all-to-all-start.2) | async-done | bytes 163872 | tf_op jit(solution)/shard_map/all_to_all | solution.py:44
  60.4 0.2 shard_map.181.squares_0
  60.6 2.5 %collective-permute-start.4 = (f32[8,128]{1,0:T(8,128)S(1)}, f32[8,128]{1,0:T(8,128)S(1)}, u32[]{:S(2)}, u32[]{:S(2)}) collective-permute-start(f32[8,128]{1,0:T(8,128)S(1)} %shard_map.181.squares_0), channel_id=1, source_target_pairs={{0,3},{1,0},{2,1},{3,2},{4,7},{5,4},{6,5},{7,6},{8,11},{9,8},{10,9... | collective-permute-start | bytes 12296 | tf_op jit(solution)/shard_map/ppermute | solution.py:54
  63.1 0.0 collective-permute-start.3
  63.1 1.7 %collective-permute-start.2 = (f32[8,128]{1,0:T(8,128)S(1)}, f32[8,128]{1,0:T(8,128)S(1)}, u32[]{:S(2)}, u32[]{:S(2)}) collective-permute-start(f32[8,128]{1,0:T(8,128)S(1)} %shard_map.181.squares_0), channel_id=1, source_target_pairs={{0,2},{1,3},{2,0},{3,1},{4,6},{5,7},{6,4},{7,5},{8,10},{9,11},{10,... | collective-permute-start | bytes 12296 | tf_op jit(solution)/shard_map/ppermute | solution.py:54
  64.8 0.0 copy-done.3
  64.8 1.3 %shard_map.182 = (f32[192,2048]{1,0:T(8,128)S(1)}, f32[2048,128]{1,0:T(8,128)S(1)}, f32[64,320]{1,0:T(8,128)S(1)}, f32[8,192]{1,0:T(8,128)}, f32[8,128]{1,0:T(8,...) custom-call(bf16[256,320]{1,0:T(8,128)(2,1)S(1)} %bitcast.7, bf16[2048,256]{1,0:T(8,128)(2,1)S(1)} %bitcast.8, ...), custom_call_target="tpu_custom_call" | custom-call | flops 335544320 | tf_op jit(solution)/shard_map/pallas_call | solution.py:32
  66.2 0.0 collective-permute-done.11.last_ref
  66.2 0.0 collective-permute-done.9.over_ref
  66.2 1.6 %shard_map.185 = (bf16[192,2048]{1,0:T(8,128)(2,1)S(1)}, bf16[4,4,2,64,128]{4,3,2,1,0:T(8,128)(2,1)S(1)}) custom-call(bf16[8,80,256]{2,1,0:T(8,128)(2,1)S(1)} %shard_map.184.here_ref, bf16[8,80,256]{2,1,0:T(8,128)(2,1)} %collective-permute-done.8.near_ref, bf16[8,80,256]{2,1,0:T(8,128)(2,1)S(1)} %collective-permute-done.9.over_ref, ...), custom_call_target="tpu_custom_call" | custom-call | tf_op jit(solution)/shard_map/pallas_call | solution.py:32
  67.8 0.0 collective-permute-done.4.squares_3
  67.8 0.0 collective-permute-done.3.squares_2
  67.8 0.0 collective-permute-done.2.squares_1
  67.8 0.0 copy-done
  67.8 0.0 copy-done.2
  67.8 1.4 %shard_map.186 = (f32[64,192]{1,0:T(8,128)}, f32[64,128]{1,0:T(8,128)}, f32[64,192]{1,0:T(8,128)}, f32[64,128]{1,0:T(8,128)}, bf16[192,2048]{1,0:T(8,128)(2,1)}, /*index=5*/bf16[2048,128]{1,0:T(8,128)(2,1)}) custom-call(f32[8,128]{1,0:T(8,128)S(1)} %shard_map.181.squares_0, f32[8,128]{1,0:T(8,128)S(1)} %collective-permute-done.2.squares_1, ...), custom_call_target="tpu_custom_call" | custom-call | tf_op jit(solution)/shard_map/pallas_call | solution.py:32
  (2 shorter events, 0.0 us)
Async XLA Ops:
  2.4 9.4 %collective-permute-start = (bf16[1,80,256]{2,1,0:T(8,128)(2,1)S(1)}, bf16[1,80,256]{2,1,0:T(8,128)(2,1)S(1)}, u32[]{:S(2)}, u32[]{:S(2)}) collective-permute-start(bf16[1,80,256]{2,1,0:T(8,128)(2,1)S(1)} %get-tuple-element.52.rows_ref.refs_0_), channel_id=1, source_target_pairs={{0,4},{4,0},{1,5},{5,1},{2,6},{6,2},{3,7},{7,3},{8,12},{12,8},{9,1... | collective-permute-start | bytes 122888 | tf_op jit(solution)/shard_map/ppermute | solution.py:49
  3.9 18.9 %all-to-all-start = ((bf16[16,64,256]{2,1,0:T(8,128)(2,1)}), bf16[16,64,256]{2,1,0:T(8,128)(2,1)S(1)}, u32[]{:S(2)}, u32[]{:S(2)}) async-start(bf16[16,64,256]{2,1,0:T(8,128)(2,1)} %get-tuple-element.38), calls=%async_computation | async-start | bytes 1048576 | tf_op jit(solution)/shard_map/all_to_all | solution.py:44
  22.8 6.3 %collective-permute-start.5 = (bf16[2,80,256]{2,1,0:T(8,128)(2,1)S(1)}, bf16[2,80,256]{2,1,0:T(8,128)(2,1)S(1)}, u32[]{:S(2)}, u32[]{:S(2)}) collective-permute-start(bf16[2,80,256]{2,1,0:T(8,128)(2,1)S(1)} %get-tuple-element.53), channel_id=1, source_target_pairs={{0,24},{4,12},{8,0},{12,20},{16,8},{20,28},{24,16},{28,4},{32,56},... | collective-permute-start | bytes 245768 | tf_op jit(solution)/shard_map/ppermute | solution.py:69
  23.1 9.3 %collective-permute-start.1 = (bf16[16,64,256]{2,1,0:T(8,128)(2,1)S(1)}, bf16[16,64,256]{2,1,0:T(8,128)(2,1)S(1)}, u32[]{:S(2)}, u32[]{:S(2)}) collective-permute-start(bf16[16,64,256]{2,1,0:T(8,128)(2,1)S(1)} %all-to-all-done.mine_ref), channel_id=1, source_target_pairs={{0,4},{4,0},{1,5},{5,1},{2,6},{6,2},{3,7},{7,3},{8,12},{12,8},{9,1... | collective-permute-start | bytes 1572872 | tf_op jit(solution)/shard_map/ppermute | solution.py:49
  24.7 4.4 %collective-permute-start.6 = (bf16[1,80,256]{2,1,0:T(8,128)(2,1)S(1)}, bf16[1,80,256]{2,1,0:T(8,128)(2,1)S(1)}, u32[]{:S(2)}, u32[]{:S(2)}) collective-permute-start(bf16[1,80,256]{2,1,0:T(8,128)(2,1)S(1)} %get-tuple-element.52.rows_ref.refs_0_), channel_id=1, source_target_pairs={{0,16},{8,24},{16,0},{24,8},{1,17},{9,25},{17,1},{25,9},{2,18},{10... | collective-permute-start | bytes 122888 | tf_op jit(solution)/shard_map/ppermute | solution.py:54
  29.1 2.3 %collective-permute-start.7 = (bf16[4,80,256]{2,1,0:T(8,128)(2,1)S(1)}, bf16[4,80,256]{2,1,0:T(8,128)(2,1)S(1)}, u32[]{:S(2)}, u32[]{:S(2)}) collective-permute-start(bf16[4,80,256]{2,1,0:T(8,128)(2,1)S(1)} %shard_map.183.refs_0_), channel_id=1, source_target_pairs={{0,4},{4,0},{1,5},{5,1},{2,6},{6,2},{3,7},{7,3},{8,12},{12,8},{9,1... | collective-permute-start | bytes 491528 | tf_op jit(solution)/shard_map/ppermute | solution.py:49
  31.4 33.4 %copy-start.3 = (bf16[64,256]{1,0:T(8,128)(2,1)S(1)}, bf16[64,256]{1,0:T(8,128)(2,1)}, u32[]{:S(2)}) copy-start(bf16[64,256]{1,0:T(8,128)(2,1)} %own_ref.1) | copy-start | bytes 98308
  31.4 10.7 %collective-permute-start.8 = (bf16[8,80,256]{2,1,0:T(8,128)(2,1)S(1)}, bf16[8,80,256]{2,1,0:T(8,128)(2,1)}, u32[]{:S(2)}, u32[]{:S(2)}) collective-permute-start(bf16[8,80,256]{2,1,0:T(8,128)(2,1)S(1)} %shard_map.184.here_ref), channel_id=1, source_target_pairs={{0,96},{4,36},{8,104},{12,44},{16,112},{20,52},{24,120},{28,60},{3... | collective-permute-start | bytes 983048 | tf_op jit(solution)/shard_map/ppermute | solution.py:69
  33.0 0.7 copy-start.1
  33.7 13.7 %all-to-all-start.1 = ((bf16[32,8,320]{2,1,0:T(8,128)(2,1)}), bf16[32,8,320]{2,1,0:T(8,128)(2,1)S(1)}, u32[]{:S(2)}, u32[]{:S(2)}) async-start(bf16[32,8,320]{2,1,0:T(8,128)(2,1)} %bitcast.10), calls=%async_computation.1 | async-start | bytes 393216 | tf_op jit(solution)/shard_map/all_to_all | solution.py:44
  39.0 13.1 %collective-permute-start.10 = (bf16[4,80,256]{2,1,0:T(8,128)(2,1)S(1)}, bf16[4,80,256]{2,1,0:T(8,128)(2,1)S(1)}, u32[]{:S(2)}, u32[]{:S(2)}) collective-permute-start(bf16[4,80,256]{2,1,0:T(8,128)(2,1)S(1)} %shard_map.183.refs_0_), channel_id=1, source_target_pairs={{0,64},{32,96},{64,0},{96,32},{1,65},{33,97},{65,1},{97,33},{2,66}... | collective-permute-start | bytes 491528 | tf_op jit(solution)/shard_map/ppermute | solution.py:54
  42.1 24.1 %collective-permute-start.9 = (bf16[8,80,256]{2,1,0:T(8,128)(2,1)}, bf16[8,80,256]{2,1,0:T(8,128)(2,1)S(1)}, u32[]{:S(2)}, u32[]{:S(2)}) collective-permute-start(bf16[8,80,256]{2,1,0:T(8,128)(2,1)} %collective-permute-done.8.near_ref), channel_id=1, source_target_pairs={{0,4},{4,0},{1,5},{5,1},{2,6},{6,2},{3,7},{7,3},{8,12},{12,8},{9,1... | collective-permute-start | bytes 983048 | tf_op jit(solution)/shard_map/ppermute | solution.py:49
  48.1 19.7 %copy-start = (f32[64,192]{1,0:T(8,128)S(1)}, f32[64,192]{1,0:T(8,128)}, u32[]{:S(2)}) copy-start(f32[64,192]{1,0:T(8,128)} %q_ref.3) | copy-start | bytes 147460
  48.2 19.7 %copy-start.2 = (f32[64,128]{1,0:T(8,128)S(1)}, f32[64,128]{1,0:T(8,128)}, u32[]{:S(2)}) copy-start(f32[64,128]{1,0:T(8,128)} %kv_ref.5) | copy-start | bytes 98308
  48.2 12.3 %all-to-all-start.2 = ((bf16[32,8,320]{2,1,0:T(8,128)(2,1)}), bf16[32,8,320]{2,1,0:T(8,128)(2,1)S(1)}, u32[]{:S(2)}, u32[]{:S(2)}) async-start(bf16[32,8,320]{2,1,0:T(8,128)(2,1)} %get-tuple-element.46), calls=%async_computation.2 | async-start | bytes 393216 | tf_op jit(solution)/shard_map/all_to_all | solution.py:44
  52.1 14.1 %collective-permute-start.11 = (bf16[4,80,256]{2,1,0:T(8,128)(2,1)S(1)}, bf16[4,80,256]{2,1,0:T(8,128)(2,1)S(1)}, u32[]{:S(2)}, u32[]{:S(2)}) collective-permute-start(bf16[4,80,256]{2,1,0:T(8,128)(2,1)S(1)} %collective-permute-done.10.far_ref), channel_id=1, source_target_pairs={{0,4},{4,0},{1,5},{5,1},{2,6},{6,2},{3,7},{7,3},{8,12},{12,8},{9,1... | collective-permute-start | bytes 491528 | tf_op jit(solution)/shard_map/ppermute | solution.py:49
  60.6 7.2 %collective-permute-start.4 = (f32[8,128]{1,0:T(8,128)S(1)}, f32[8,128]{1,0:T(8,128)S(1)}, u32[]{:S(2)}, u32[]{:S(2)}) collective-permute-start(f32[8,128]{1,0:T(8,128)S(1)} %shard_map.181.squares_0), channel_id=1, source_target_pairs={{0,3},{1,0},{2,1},{3,2},{4,7},{5,4},{6,5},{7,6},{8,11},{9,8},{10,9... | collective-permute-start | bytes 12296 | tf_op jit(solution)/shard_map/ppermute | solution.py:54
  63.1 4.7 %collective-permute-start.3 = (f32[8,128]{1,0:T(8,128)S(1)}, f32[8,128]{1,0:T(8,128)S(1)}, u32[]{:S(2)}, u32[]{:S(2)}) collective-permute-start(f32[8,128]{1,0:T(8,128)S(1)} %shard_map.181.squares_0), channel_id=1, source_target_pairs={{0,1},{1,2},{2,3},{3,0},{4,5},{5,6},{6,7},{7,4},{8,9},{9,10},{10,1... | collective-permute-start | bytes 12296 | tf_op jit(solution)/shard_map/ppermute | solution.py:54
  63.1 4.7 %collective-permute-start.2 = (f32[8,128]{1,0:T(8,128)S(1)}, f32[8,128]{1,0:T(8,128)S(1)}, u32[]{:S(2)}, u32[]{:S(2)}) collective-permute-start(f32[8,128]{1,0:T(8,128)S(1)} %shard_map.181.squares_0), channel_id=1, source_target_pairs={{0,2},{1,3},{2,0},{3,1},{4,6},{5,7},{6,4},{7,5},{8,10},{9,11},{10,... | collective-permute-start | bytes 12296 | tf_op jit(solution)/shard_map/ppermute | solution.py:54
